TPU v7x, 256 devices: a whole 4x4x8 slice. The times are simulated.
256 devices in a mesh: sp: 64 (over z, y, core), tp: 4 (over x).
Axes of the slice: x: 4, y: 4, z: 8, core: 2. Of those that a mesh axis runs over, the one named last changes fastest.
Arguments:
- query: bfloat16 [16384, 1536], P('sp', 'tp'), may hold values from -6 to 6
- forget_preact: bfloat16 [16384, 1536], P('sp', 'tp'), may hold values from -6 to 6
- value_input: bfloat16 [16384, 1536], P('sp', 'tp'), may hold values from -6 to 6
- output_gate: bfloat16 [16384, 1536], P('sp', 'tp'), may hold values from -6 to 6
- forget_minimum: float32 [1536], P('tp'), may hold values from 0.88 to 1
- extra_log_decay: float32 [12, 16384], P('tp', 'sp'), may hold values from -0.7 to 0
- head_norm_gain: float32 [1536], P('tp'), may hold values from 0.1 to 1.9
- output_weight: bfloat16 [1536, 3072], P(None, 'tp'), may hold values from -0.15625 to 0.15625
- stream: bfloat16 [16384, 3072], P(('sp', 'tp')), may hold values from -6 to 6
- feedforward_gain: float32 [3072], replicated, may hold values from 0.1 to 1.9
- routes: int32 [16384, 2], P('sp'), may hold values from 0 to 63, all different within a row; in each aligned block of 64 rows (0 to 63, 64 to 127, ...) at most 4 rows name the same one
- router_weight: float32 [16384, 2], P(('sp', 'tp')), may hold values from 0.05 to 1
- expert_gate_weight: bfloat16 [64, 3072, 1024], P('sp', None, 'tp'), may hold values from -0.109375 to 0.109375
- expert_up_weight: bfloat16 [64, 3072, 1024], P('sp', None, 'tp'), may hold values from -0.109375 to 0.109375
- expert_down_weight: bfloat16 [64, 1024, 3072], P('sp', 'tp'), may hold values from -0.1875 to 0.1875
Outputs:
- result: bfloat16 [16384, 3072], P(('sp', 'tp'))
Inputs may be any that keep to these rules, and one draw needn't show every extreme that they name: `routes`: each row names 2 different experts; in each aligned block of 64 rows no expert is named by more than 4 rows, a bound that some block reaches.
All inputs are finite; a program needn't handle non-finite values.
Results may differ from a plain program's by a relative error of at most 0.01.
Values may be sent and summed in bfloat16 or wider, within the bound.
No kernel may reach another device: no remote copies, remote signals or barrier semaphores. Data moves between devices by JAX's collectives and lax.ppermute only.
A program may use at most 64 MiB of HBM per device.

v0:
```python
import jax
import jax.numpy as jnp
from jax import lax
from jax.sharding import Mesh
from jax.sharding import PartitionSpec as P

STATE_ROW_COUNT = 128
VALUE_CHANNELS = 128
SPAN = 64
TOPK = 2
SP = ("sp_0", "sp_1", "sp_2")
SP_TP = ("sp_0", "sp_1", "sp_2", "tp")


epsilon = 1e-06
top_precision = lax.Precision.HIGHEST


def nothing_yet(value, identity):
    return jax.tree.map(
        lambda part, zero: jnp.zeros_like(part) + jnp.asarray(zero, part.dtype), value, identity
    )


def entering(value, axes, combine, identity):
    before = start = nothing_yet(value, identity)
    running = value
    for axis in reversed(axes):
        devices, mine = (lax.axis_size(axis), lax.axis_index(axis))
        pieces = jax.tree.map(
            lambda part, kind: lax.all_gather(part.astype(kind), axis),
            running,
            (jnp.bfloat16, jnp.bfloat16),
        )
        inside, running = (start, start)
        for k in range(devices):
            passed = k < mine
            running = combine(
                running, jax.tree.map(lambda part, own: part[k].astype(own.dtype), pieces, value)
            )
            inside = jax.tree.map(lambda new, old: jnp.where(passed, new, old), running, inside)
        before = combine(inside, before)
    return before


def sent_to_all(value, axis):
    devices = lax.axis_size(axis)
    return lax.all_to_all(
        jnp.broadcast_to(value[None], (devices, *value.shape)), axis, 0, 0, tiled=True
    )


def laid_out(parts, dim):
    parts = jnp.moveaxis(parts, 0, dim)
    dims = parts.shape
    return parts.reshape(*dims[:dim], dims[dim] * dims[dim + 1], *dims[dim + 2 :])


def gathered_copies(value, axis, dim):
    parts = sent_to_all(value, axis)
    return laid_out(parts, dim)


def block_step(current_state, block_inputs):
    query_block, weight_blk, value_block, decay_blk = block_inputs
    running_decay = jnp.cumsum(decay_blk, axis=1)
    intermediate = jnp.einsum(
        "yro,yow->yrw", query_block * jnp.exp(running_decay), current_state, precision=top_precision
    )
    causal = lax.broadcasted_iota(jnp.int32, (SPAN, SPAN), 0) >= lax.broadcasted_iota(
        jnp.int32, (SPAN, SPAN), 1
    )
    log_gap = running_decay[:, :, None, :] - running_decay[:, None, :, :]
    decay_table = jnp.exp(jnp.where(causal[None, :, :, None], log_gap, -jnp.inf))
    scores = jnp.einsum(
        "htk,hsk,htsk->hts", query_block, weight_blk, decay_table, precision=top_precision
    )
    output = intermediate + jnp.einsum("hts,hsv->htv", scores, value_block, precision=top_precision)
    final_decay = running_decay[:, -1:, :]
    scaled_rows = weight_blk * jnp.exp(final_decay - running_decay)
    following_state = jnp.exp(final_decay[:, 0, :])[:, :, None] * current_state + jnp.einsum(
        "xme,xmc->xec", scaled_rows, value_block, precision=top_precision
    )
    return (following_state, output)


def gate_factors(query, forget_preact, forget_minimum, extra_log_decay):
    query_activated = jax.nn.silu(query.astype(jnp.float32))
    incoming_weight = (1.0 - forget_minimum) * jax.nn.sigmoid(-forget_preact.astype(jnp.float32))
    spike_columns = jnp.repeat(jnp.transpose(extra_log_decay), STATE_ROW_COUNT, axis=1)
    decay_logarithm = jnp.log1p(-incoming_weight) + spike_columns
    return (query_activated, incoming_weight, decay_logarithm)


def head_blocks(array_in, head_total):
    rows_in = array_in.shape[0]
    return array_in.reshape(rows_in // SPAN, SPAN, head_total, -1).transpose(0, 2, 1, 3)


def unblock(block_outs, window_rows, head_total):
    return block_outs.transpose(0, 2, 1, 3).reshape(window_rows, head_total, VALUE_CHANNELS)


def head_output(mixed, head_norm_gain, output_gate):
    normalized = mixed * lax.rsqrt(jnp.mean(mixed * mixed, axis=-1, keepdims=True) + epsilon)
    flat_rows = normalized.reshape(mixed.shape[0], -1)
    return (flat_rows * head_norm_gain * jax.nn.silu(output_gate.astype(jnp.float32))).astype(
        jnp.bfloat16
    )


def rms_norm(residual, gain):
    scale_row = lax.rsqrt(jnp.mean(residual * residual, axis=-1, keepdims=True) + epsilon)
    return (residual * scale_row * gain).astype(jnp.bfloat16)


def combine_states(earlier, later):
    return (earlier[0] + later[0], jnp.exp(later[0])[:, :, None] * earlier[1] + later[1])


def carry_in(total_decay, local_state):
    identity = (jnp.zeros_like(total_decay), jnp.zeros_like(local_state))
    return entering((total_decay, local_state), SP, combine_states, identity)[1]


def dispatch_table(slot_ids, window_rows, quarter_rows):
    groups = slot_ids.shape[0]
    slot_grid = lax.broadcasted_iota(jnp.int32, (groups, window_rows, slot_ids.shape[1]), 1)
    hits = (slot_grid == slot_ids[:, None, :]).astype(jnp.bfloat16)
    return jnp.sum(hits.reshape(groups, window_rows, quarter_rows, TOPK), axis=3)


def per_device(
    query,
    forget_preact,
    value_input,
    output_gate,
    forget_minimum,
    extra_log_decay,
    head_norm_gain,
    output_weight,
    stream,
    feedforward_gain,
    routes,
    router_weight,
    expert_gate_weight,
    expert_up_weight,
    expert_down_weight,
):
    head_total = query.shape[1] // STATE_ROW_COUNT
    window_rows = query.shape[0]
    tp_size = lax.axis_size("tp")
    sp_size = lax.axis_size(SP)
    query_activated, incoming_weight, decay_logarithm = gate_factors(
        query, forget_preact, forget_minimum, extra_log_decay
    )
    value_rows = value_input.astype(jnp.float32)
    blocks = (
        head_blocks(query_activated, head_total),
        head_blocks(incoming_weight, head_total),
        head_blocks(value_rows, head_total),
        head_blocks(decay_logarithm, head_total),
    )
    running_decay = jnp.cumsum(decay_logarithm, axis=0)
    total_decay = running_decay[-1].reshape(head_total, STATE_ROW_COUNT)
    scaled_rows = (incoming_weight * jnp.exp(running_decay[-1:] - running_decay)).reshape(
        window_rows, head_total, STATE_ROW_COUNT
    )
    local_state = jnp.einsum(
        "pyr,pyc->yrc",
        scaled_rows,
        value_rows.reshape(window_rows, head_total, VALUE_CHANNELS),
        precision=top_precision,
    )
    carried = carry_in(total_decay, local_state)
    _, block_outs = lax.scan(block_step, carried, blocks)
    mixed = unblock(block_outs, window_rows, head_total)
    hidden = head_output(mixed, head_norm_gain, output_gate)
    projected = jnp.dot(
        gathered_copies(hidden, "tp", 1), output_weight, preferred_element_type=jnp.float32
    )
    mix_rows = lax.all_to_all(
        projected.astype(jnp.bfloat16), "tp", split_axis=0, concat_axis=1, tiled=True
    )
    residual = stream.astype(jnp.float32) + mix_rows.astype(jnp.float32)
    normed = rms_norm(residual, feedforward_gain)
    quarter_rows = stream.shape[0]
    capacity = window_rows // sp_size
    pick_ids = routes.reshape(tp_size, quarter_rows * TOPK)
    onehot = (pick_ids[:, :, None] == jnp.arange(sp_size, dtype=jnp.int32)[None, None, :]).astype(
        jnp.int32
    )
    rank_ids = jnp.sum((jnp.cumsum(onehot, axis=1) - 1) * onehot, axis=2)
    slot_ids = pick_ids * capacity + rank_ids
    own_index = lax.axis_index("tp")
    own_slots = lax.dynamic_slice_in_dim(slot_ids, own_index, 1, 0)
    send_table = dispatch_table(own_slots, window_rows, quarter_rows)[0]
    sendbuf = jnp.dot(send_table, normed, preferred_element_type=jnp.float32).astype(jnp.bfloat16)
    received = lax.all_to_all(
        sendbuf.reshape(sp_size, capacity, -1), SP, split_axis=0, concat_axis=0, tiled=True
    )
    arrived = lax.all_gather(received[None], "tp", axis=0, tiled=True)
    flat_rows = arrived.reshape(-1, arrived.shape[-1])
    gate_act = jnp.dot(flat_rows, expert_gate_weight[0], preferred_element_type=jnp.float32)
    up_act = jnp.dot(flat_rows, expert_up_weight[0], preferred_element_type=jnp.float32)
    inner_act = (jax.nn.silu(gate_act) * up_act).astype(jnp.bfloat16)
    summed = lax.psum_scatter(
        jnp.dot(inner_act, expert_down_weight[0], preferred_element_type=jnp.float32)
        .reshape(arrived.shape)
        .astype(jnp.bfloat16),
        "tp",
        scatter_dimension=0,
        tiled=True,
    )
    returned = lax.all_to_all(summed, SP, split_axis=1, concat_axis=1, tiled=True)
    results = returned.reshape(window_rows, -1)
    picked = jnp.take(results, own_slots.reshape(-1), axis=0).reshape(quarter_rows, TOPK, -1)
    route_weight = router_weight / jnp.sum(router_weight, axis=1, keepdims=True)
    routed_sum = jnp.sum(route_weight[:, :, None] * picked.astype(jnp.float32), axis=1)
    return (residual + routed_sum).astype(jnp.bfloat16)


def solution(mesh):
    torus = Mesh(mesh.devices.reshape(8, 4, 2, mesh.shape["tp"]), ("sp_0", "sp_1", "sp_2", "tp"))
    placed = (
        P(SP, "tp"),
        P(SP, "tp"),
        P(SP, "tp"),
        P(SP, "tp"),
        P("tp"),
        P("tp", SP),
        P("tp"),
        P(None, "tp"),
        P(SP_TP, None),
        P(),
        P(SP, None),
        P(SP_TP, None),
        P(SP, None, "tp"),
        P(SP, None, "tp"),
        P(SP, "tp", None),
    )
    return jax.shard_map(
        per_device, mesh=torus, in_specs=placed, out_specs=P(SP_TP, None), check_vma=False
    )
```

profile of v0, /device:TPU:1, one launch (start us, length us, event | category | flops | bytes accessed | tf_op | source)
XLA Modules:
  0.0 459.0 jit_solution(5915146488147493368)
XLA Ops:
  6.5 1.2 copy.172
  8.4 1.7 divide_multiply_fusion
  11.3 1.2 fusion.100
  13.3 1.2 copy.175
  16.9 4.7 %all_gather.29 = bf16[2,3,128]{2,1,0:T(4,128)(2,1)S(1)} all-gather(bf16[1,3,128]{2,1,0:T(4,128)(2,1)S(1)} %bitcast.289), channel_id=1, replica_groups=mesh['sp_0'=8,'sp_1'=4,'sp_2'=2,'tp'=4] {'sp_2'}, dimensions={0}, use_global_device_ids=true | all-gather | bytes 2304 | tf_op jit(solution)/shard_map/all_gather | solution.py:31
  22.2 6.3 %all_gather.30 = bf16[4,3,128]{2,1,0:T(4,128)(2,1)S(1)} all-gather(bf16[1,3,128]{2,1,0:T(4,128)(2,1)S(1)} %get-tuple-element.125), channel_id=1, replica_groups=mesh['sp_0'=8,'sp_1'=4,'sp_2'=2,'tp'=4] {'sp_1'}, dimensions={0}, use_global_device_ids=true | all-gather | bytes 3840 | tf_op jit(solution)/shard_map/all_gather | solution.py:31
  28.9 3.9 all-gather
  33.0 9.6 %all_gather.34 = bf16[4,3,128,128]{3,2,1,0:T(8,128)(2,1)S(1)} all-gather(bf16[1,3,128,128]{3,2,1,0:T(8,128)(2,1)S(1)} %fusion.65), channel_id=1, replica_groups=mesh['sp_0'=8,'sp_1'=4,'sp_2'=2,'tp'=4] {'sp_1'}, dimensions={0}, use_global_device_ids=true | all-gather | bytes 491520 | tf_op jit(solution)/shard_map/all_gather | solution.py:31
  43.5 26.2 %all_gather.35 = bf16[8,3,128,128]{3,2,1,0:T(8,128)(2,1)} all-gather(bf16[1,3,128,128]{3,2,1,0:T(8,128)(2,1)S(1)} %fusion.60), channel_id=1, replica_groups=mesh['sp_0'=8,'sp_1'=4,'sp_2'=2,'tp'=4] {'sp_0'}, dimensions={0}, use_global_device_ids=true | all-gather | bytes 884736 | tf_op jit(solution)/shard_map/all_gather | solution.py:31
  69.7 12.0 %all_gather.31 = bf16[8,3,128]{2,1,0:T(4,128)(2,1)S(1)} all-gather(bf16[1,3,128]{2,1,0:T(4,128)(2,1)S(1)} %get-tuple-element.120), channel_id=1, replica_groups=mesh['sp_0'=8,'sp_1'=4,'sp_2'=2,'tp'=4] {'sp_0'}, dimensions={0}, use_global_device_ids=true | all-gather | bytes 6912 | tf_op jit(solution)/shard_map/all_gather | solution.py:31
  82.4 1.1 reshape.398
  84.3 1.9 copy.179
  86.2 1.1 reshape.399
  90.3 2.0 reshape.401
  93.3 1.8 copy.184
  95.1 2.1 fusion.46
  97.2 38.7 %while.12 = (s32[]{:T(128)}, f32[3,128,128]{2,1,0:T(8,128)S(1)}, f32[4,3,64,128]{3,2,1,0:T(8,128)}, f32[4,3,64,128]{3,2,1,0:T(8,128)}, f32[4,3,64,128]{3,2,1,0:T...) while((s32[]{:T(128)}, f32[3,128,128]{2,1,0:T(8,128)S(1)}, ...), condition=%wide.region_4.5_spmd, body=%wide.region_2.4_spmd.sunk | while | flops 103972864 | bytes 18455716 | solution.py:176
  98.3 1.2 select_exponential_fusion.2
  99.5 5.5 %fusion.125 = f32[3,64,64]{1,2,0:T(8,128)S(1)} fusion(f32[3,64,64,128]{3,2,1,0:T(8,128)S(1)} %select_exponential_fusion.2, f32[3,128,64]{1,2,0:T(8,128)S(1)} %get-tuple-element.173, f32[3,128,64]{1,2,0:T(8,128)S(1)} %dynamic-slice_bitcast_fusion.6), kind=kLoop, calls=%fused_computation.2.clone.1 | loop fusion | flops 4706304 | bytes 6537216 | tf_op jit(solution)/shard_map/while/body/eval_jaxpr/htk,hsk,htsk->hts/dot_general | solution.py:75
  108.0 1.2 select_exponential_fusion.2
  109.2 5.5 %fusion.125 = f32[3,64,64]{1,2,0:T(8,128)S(1)} fusion(f32[3,64,64,128]{3,2,1,0:T(8,128)S(1)} %select_exponential_fusion.2, f32[3,128,64]{1,2,0:T(8,128)S(1)} %get-tuple-element.173, f32[3,128,64]{1,2,0:T(8,128)S(1)} %dynamic-slice_bitcast_fusion.6), kind=kLoop, calls=%fused_computation.2.clone.1 | loop fusion | flops 4706304 | bytes 6537216 | tf_op jit(solution)/shard_map/while/body/eval_jaxpr/htk,hsk,htsk->hts/dot_general | solution.py:75
  117.6 1.2 select_exponential_fusion.2
  118.9 5.5 %fusion.125 = f32[3,64,64]{1,2,0:T(8,128)S(1)} fusion(f32[3,64,64,128]{3,2,1,0:T(8,128)S(1)} %select_exponential_fusion.2, f32[3,128,64]{1,2,0:T(8,128)S(1)} %get-tuple-element.173, f32[3,128,64]{1,2,0:T(8,128)S(1)} %dynamic-slice_bitcast_fusion.6), kind=kLoop, calls=%fused_computation.2.clone.1 | loop fusion | flops 4706304 | bytes 6537216 | tf_op jit(solution)/shard_map/while/body/eval_jaxpr/htk,hsk,htsk->hts/dot_general | solution.py:75
  127.3 1.2 select_exponential_fusion.2
  128.6 5.5 %fusion.125 = f32[3,64,64]{1,2,0:T(8,128)S(1)} fusion(f32[3,64,64,128]{3,2,1,0:T(8,128)S(1)} %select_exponential_fusion.2, f32[3,128,64]{1,2,0:T(8,128)S(1)} %get-tuple-element.173, f32[3,128,64]{1,2,0:T(8,128)S(1)} %dynamic-slice_bitcast_fusion.6), kind=kLoop, calls=%fused_computation.2.clone.1 | loop fusion | flops 4706304 | bytes 6537216 | tf_op jit(solution)/shard_map/while/body/eval_jaxpr/htk,hsk,htsk->hts/dot_general | solution.py:75
  136.0 1.2 multiply_reduce_fusion.2
  137.1 1.3 copy.205
  141.2 4.2 all-to-all-start
  146.4 7.4 %all-to-all-done = bf16[4,256,384]{1,2,0:T(8,128)(2,1)} async-done(((bf16[4,256,384]{1,2,0:T(8,128)(2,1)}), bf16[4,256,384]{1,2,0:T(8,128)(2,1)}, u32[]{:S(2)}, u32[]{:S(2)}) %all-to-all-start) | async-done | bytes 786464 | tf_op jit(solution)/shard_map/all_to_all | solution.py:48
  153.8 2.7 convolution_convert_fusion.2
  156.5 3.8 all-to-all-start.1
  160.8 8.3 %all-to-all-done.1 = bf16[4,64,768]{2,1,0:T(8,128)(2,1)S(1)} async-done(((bf16[4,64,768]{2,1,0:T(8,128)(2,1)}), bf16[4,64,768]{2,1,0:T(8,128)(2,1)S(1)}, u32[]{:S(2)}, u32[]{:S(2)}) %all-to-all-start.1) | async-done | bytes 393248 | tf_op jit(solution)/shard_map/all_to_all | solution.py:182
  170.0 1.5 reshape.406
  171.6 59.1 %all_to_all.28 = bf16[64,4,3072]{2,1,0:T(4,128)(2,1)} all-to-all(bf16[64,4,3072]{2,1,0:T(4,128)(2,1)} %reshape.406), channel_id=1, replica_groups=mesh['sp_0'=8,'sp_1'=4,'sp_2'=2,'tp'=4] {'sp_0','sp_1','sp_2'}, dimensions={0} | all-to-all | bytes 3145728 | tf_op jit(solution)/shard_map/all_to_all | solution.py:199
  230.7 63.3 %all-gather.4.cloned.1.call-done = bf16[256,4,3072]{2,1,0:T(4,128)(2,1)} async-done(((bf16[64,4,3072]{2,1,0:T(4,128)(2,1)}), bf16[256,4,3072]{2,1,0:T(4,128)(2,1)}) %all-gather.4.cloned.1.call-update) | async-done | bytes 6291472 | tf_op jit(solution)/shard_map/all_gather | solution.py:202
  294.0 10.7 %reshape.407 = bf16[1024,3072]{1,0:T(8,128)(2,1)} reshape(bf16[256,4,3072]{2,1,0:T(4,128)(2,1)} %all-gather.4.cloned.1.call-done) | data formatting | bytes 12582912 | tf_op jit(solution)/shard_map/reshape | solution.py:203
  304.7 4.7 %fusion.21 = f32[1024,256]{1,0:T(8,128)S(1)} fusion(bf16[1024,3072]{1,0:T(8,128)(2,1)} %reshape.407, bf16[1,3072,256]{2,1,0:T(8,128)(2,1)S(1)} %copy-done.14), kind=kOutput, calls=%fused_computation.35 | convolution fusion | flops 1610612736 | bytes 8912896 | tf_op jit(solution)/shard_map/dot_general | solution.py:204
  309.7 2.6 fusion.26
  312.3 1.2 dot_general.44
  313.5 4.5 convolution_convert_fusion
  318.0 67.4 %reduce-scatter.2.cloned.1.call-done = bf16[1,64,4,3072]{3,1,2,0:T(8,128)(2,1)} async-done(((bf16[4,64,4,3072]{3,1,2,0:T(8,128)(2,1)}), bf16[1,64,4,3072]{3,1,2,0:T(8,128)(2,1)}) %reduce-scatter.2.cloned.1.call-update) | async-done | bytes 1572880 | tf_op jit(solution)/shard_map/reduce_scatter | solution.py:207
  385.4 3.8 copy.195
  389.2 11.1 %all-to-all-start.3 = ((bf16[1,64,4,3072]{3,2,0,1:T(4,128)(2,1)}), bf16[1,64,4,3072]{3,2,0,1:T(4,128)(2,1)}, u32[]{:S(2)}, u32[]{:S(2)}) async-start(bf16[1,64,4,3072]{3,2,0,1:T(4,128)(2,1)} %copy.195), calls=%async_computation.4 | async-start | bytes 3145728 | tf_op jit(solution)/shard_map/all_to_all | solution.py:215
  401.1 38.2 %all-to-all-done.3 = bf16[1,64,4,3072]{3,2,0,1:T(4,128)(2,1)} async-done(((bf16[1,64,4,3072]{3,2,0,1:T(4,128)(2,1)}), bf16[1,64,4,3072]{3,2,0,1:T(4,128)(2,1)}, u32[]{:S(2)}, u32[]{:S(2)}) %all-to-all-start.3) | async-done | bytes 1572896 | tf_op jit(solution)/shard_map/all_to_all | solution.py:215
  439.3 2.7 reshape.408
  442.0 1.9 gather_fusion
  443.9 3.0 gather.7
  446.9 4.3 multiply_reduce_fusion
  (145 shorter events, 31.3 us)
Async XLA Ops:
  6.5 147.3 %copy-start = (bf16[1536,768]{1,0:T(8,128)(2,1)S(1)}, bf16[1536,768]{1,0:T(8,128)(2,1)}, u32[]{:S(2)}) copy-start(bf16[1536,768]{1,0:T(8,128)(2,1)} %param.24) | copy-start | bytes 7077892
  10.3 5.5 %copy-start.7 = (bf16[256,384]{1,0:T(8,128)(2,1)S(1)}, bf16[256,384]{1,0:T(8,128)(2,1)}, u32[]{:S(2)}) copy-start(bf16[256,384]{1,0:T(8,128)(2,1)} %param.19) | copy-start | bytes 589828
  42.7 39.7 %copy-start.9 = (f32[3,128]{1,0:T(4,128)}, f32[3,128]{1,0:T(4,128)S(1)}, u32[]{:S(2)}) copy-start(f32[3,128]{1,0:T(4,128)S(1)} %fusion.95) | copy-start | bytes 4612
  43.2 39.1 %copy-start.8 = (f32[3,128]{1,0:T(4,128)}, f32[3,128]{1,0:T(4,128)S(1)}, u32[]{:S(2)}) copy-start(f32[3,128]{1,0:T(4,128)S(1)} %get-tuple-element.122) | copy-start | bytes 4612
  98.3 1.2 copy-start.3
  99.5 5.8 %copy-start.4 = (f32[4,3,64,128]{3,2,1,0:T(8,128)S(1)}, f32[4,3,64,128]{3,2,1,0:T(8,128)}, u32[]{:S(2)}) copy-start(f32[4,3,64,128]{3,2,1,0:T(8,128)} %get-tuple-element.197) | copy-start | bytes 1179652 | tf_op jit(solution)/shard_map/while
  107.9 1.2 copy-start.3
  109.2 5.8 %copy-start.4 = (f32[4,3,64,128]{3,2,1,0:T(8,128)S(1)}, f32[4,3,64,128]{3,2,1,0:T(8,128)}, u32[]{:S(2)}) copy-start(f32[4,3,64,128]{3,2,1,0:T(8,128)} %get-tuple-element.197) | copy-start | bytes 1179652 | tf_op jit(solution)/shard_map/while
  117.6 1.2 copy-start.3
  118.9 5.8 %copy-start.4 = (f32[4,3,64,128]{3,2,1,0:T(8,128)S(1)}, f32[4,3,64,128]{3,2,1,0:T(8,128)}, u32[]{:S(2)}) copy-start(f32[4,3,64,128]{3,2,1,0:T(8,128)} %get-tuple-element.197) | copy-start | bytes 1179652 | tf_op jit(solution)/shard_map/while
  127.3 1.2 copy-start.3
  128.6 5.8 %copy-start.4 = (f32[4,3,64,128]{3,2,1,0:T(8,128)S(1)}, f32[4,3,64,128]{3,2,1,0:T(8,128)}, u32[]{:S(2)}) copy-start(f32[4,3,64,128]{3,2,1,0:T(8,128)} %get-tuple-element.197) | copy-start | bytes 1179652 | tf_op jit(solution)/shard_map/while
  135.9 4.2 copy-start.12
  138.5 7.0 %copy-start.13 = (s32[256,2]{0,1:T(2,128)S(1)}, s32[256,2]{0,1:T(2,128)}, u32[]{:S(2)}) copy-start(s32[256,2]{0,1:T(2,128)} %param.27) | copy-start | bytes 6148
  141.2 12.6 %all-to-all-start = ((bf16[4,256,384]{1,2,0:T(8,128)(2,1)}), bf16[4,256,384]{1,2,0:T(8,128)(2,1)}, u32[]{:S(2)}, u32[]{:S(2)}) async-start(bf16[4,256,384]{1,2,0:T(8,128)(2,1)} %broadcast_in_dim.43), calls=%async_computation | async-start | bytes 1572864 | tf_op jit(solution)/shard_map/all_to_all | solution.py:48
  156.5 12.7 %copy-start.5 = (bf16[64,3072]{1,0:T(8,128)(2,1)S(1)}, bf16[64,3072]{1,0:T(8,128)(2,1)}, u32[]{:S(2)}) copy-start(bf16[64,3072]{1,0:T(8,128)(2,1)} %param.25) | copy-start | bytes 1179652
  156.5 12.9 %copy-start.10 = (f32[3072]{0:T(1024)S(1)}, f32[3072]{0:T(1024)}, u32[]{:S(2)}) copy-start(f32[3072]{0:T(1024)} %param.26) | copy-start | bytes 36868
  156.5 12.5 %all-to-all-start.1 = ((bf16[4,64,768]{2,1,0:T(8,128)(2,1)}), bf16[4,64,768]{2,1,0:T(8,128)(2,1)S(1)}, u32[]{:S(2)}, u32[]{:S(2)}) async-start(bf16[4,64,768]{2,1,0:T(8,128)(2,1)} %bitcast.56), calls=%async_computation.1 | async-start | bytes 786432 | tf_op jit(solution)/shard_map/all_to_all | solution.py:182
  160.3 133.6 %all-gather.4.cloned.1.call-start = ((), (), s32[]{:S(2)}) async-start(), calls=%async_computation.6 | async-start | bytes 7864320 | tf_op jit(solution)/shard_map/all_gather | solution.py:202
  230.7 74.0 %copy-start.14 = (bf16[1,3072,256]{2,1,0:T(8,128)(2,1)S(1)}, bf16[1,3072,256]{2,1,0:T(8,128)(2,1)}, u32[]{:S(2)}) copy-start(bf16[1,3072,256]{2,1,0:T(8,128)(2,1)} %param.29) | copy-start | bytes 4718596
  230.7 154.7 %reduce-scatter.2.cloned.1.call-start = ((), (), s32[]{:S(2)}) async-start(), calls=%async_computation.5 | async-start | bytes 7864320 | tf_op jit(solution)/shard_map/reduce_scatter | solution.py:207
  304.7 4.7 %copy-start.2 = (bf16[1024,3072]{1,0:T(8,128)(2,1)S(1)}, bf16[1024,3072]{1,0:T(8,128)(2,1)}, u32[]{:S(2)}) copy-start(bf16[1024,3072]{1,0:T(8,128)(2,1)} %reshape.407) | copy-start | bytes 18874372
  304.7 5.0 %copy-start.15 = (bf16[1,3072,256]{2,1,0:T(8,128)(2,1)S(1)}, bf16[1,3072,256]{2,1,0:T(8,128)(2,1)}, u32[]{:S(2)}) copy-start(bf16[1,3072,256]{2,1,0:T(8,128)(2,1)} %param.30) | copy-start | bytes 4718596
  309.7 3.8 copy-start.6
  389.2 11.1 %copy-start.11 = (f32[64,2]{0,1:T(2,128)S(1)}, f32[64,2]{0,1:T(2,128)}, u32[]{:S(2)}) copy-start(f32[64,2]{0,1:T(2,128)} %param.28) | copy-start | bytes 1540
  389.2 50.0 %all-to-all-start.3 = ((bf16[1,64,4,3072]{3,2,0,1:T(4,128)(2,1)}), bf16[1,64,4,3072]{3,2,0,1:T(4,128)(2,1)}, u32[]{:S(2)}, u32[]{:S(2)}) async-start(bf16[1,64,4,3072]{3,2,0,1:T(4,128)(2,1)} %copy.195), calls=%async_computation.4 | async-start | bytes 3145728 | tf_op jit(solution)/shard_map/all_to_all | solution.py:215
  443.9 8.2 %copy-start.1 = (bf16[1536,768]{1,0:T(8,128)(2,1)S(1)}, bf16[1536,768]{1,0:T(8,128)(2,1)}, u32[]{:S(2)}) copy-start(bf16[1536,768]{1,0:T(8,128)(2,1)} %param.24) | copy-start | bytes 7077892
Sparse Core Ops, SparseCore 0:
  230.8 63.1 all-gather.3
  318.1 67.2 reduce-scatter.1
where the time goes:
time: 461 us; the launch traced here: 459 us
  waiting for transfers between devices  185 us (40%)
  blocking collectives  122 us (26%)
  local copies, waits for them, and re-layouts  53.4 us (12%)
  other arithmetic  43 us (9%)
  matrix products  22.8 us (5%)
  starting transfers between devices  19.1 us (4%)
  between operations  13.8 us (3%)
    reduce_scatter x1, waiting for transfers between devices, per_device(): lax.psum_scatter(jnp.dot(inner_act, expert_down_weight[0], preferred_elem...  67.4 us
    all_gather x1, waiting for transfers between devices, per_device(): arrived = lax.all_gather(received[None], 'tp', axis=0, tiled=True)  63.3 us
    all_gather x6, blocking collectives, entering(): lax.all_gather(part.astype(kind), axis)  62.7 us
    all_to_all x1, blocking collectives, per_device(): lax.all_to_all(sendbuf.reshape(sp_size, capacity, -1), SP, split_axis=0,...  59.1 us
    all_to_all x1, waiting for transfers between devices, per_device(): lax.all_to_all(summed, SP, split_axis=1, concat_axis=1, tiled=True)  38.2 us
    dot_general x4, other arithmetic, block_step(): jnp.einsum('htk,hsk,htsk->hts', query_block, weight_blk, decay_table, pre...  21.9 us
    all_to_all x1, starting transfers between devices, per_device(): lax.all_to_all(summed, SP, split_axis=1, concat_axis=1, tiled=True)  11.1 us
    reshape x1, local copies, waits for them, and re-layouts, per_device(): flat_rows = arrived.reshape(-1, arrived.shape[-1])  10.7 us
  transfers between devices with their start and end apart: 5, of which 5 were waited for; matrix products, arithmetic and copies ran while one was open for 0% of the time, Pallas kernels for 0%

commit v1 on v0

v1 whole, which is shorter than its diff:
```python
import jax
import jax.numpy as jnp
from jax import lax
from jax.experimental import pallas as pl
from jax.experimental.pallas import tpu as pltpu
from jax.sharding import Mesh
from jax.sharding import PartitionSpec as P

LANES = 128
SPAN = 64
TOPK = 2
PLANE = ("sp_1", "sp_2")
SP = ("sp_0", "sp_1", "sp_2")
TP = ("tp_0", "tp_1")
SP_TP = SP + TP
ROW_PAIRS = ((1, 2), (2, 1), (3, 0), (0, 3))

f32 = jnp.float32
bf16 = jnp.bfloat16
epsilon = 1e-06
exact = lax.Precision.HIGHEST


def dot(a, b, dims=((1,), (0,)), precision=None):
    return lax.dot_general(a, b, (dims, ((), ())), precision=precision, preferred_element_type=f32)


def split(value):
    high = value.astype(bf16)
    return high, (value - high.astype(f32)).astype(bf16)


def silu(value):
    return value * jax.nn.sigmoid(value)


def call(kernel, out_shape, *operands, smem=()):
    specs = [
        pl.BlockSpec(memory_space=pltpu.SMEM if k in smem else pltpu.VMEM)
        for k in range(len(operands))
    ]
    outs = jax.tree.map(lambda _: pl.BlockSpec(memory_space=pltpu.VMEM), out_shape)
    return pl.pallas_call(
        kernel,
        out_shape=out_shape,
        in_specs=specs,
        out_specs=outs,
        compiler_params=pltpu.CompilerParams(vmem_limit_bytes=48 * 1024 * 1024),
    )(*operands)


def decays(forget_ref, floor_ref, extra_ref, table):
    weight = (1.0 - floor_ref[...]) * jax.nn.sigmoid(-forget_ref[...].astype(f32))
    single = jnp.log1p(-weight)
    summed = dot(table, single, precision=exact)
    extra = extra_ref[...]
    extra_summed = dot(table, extra, ((1,), (1,)), precision=exact)
    return weight, summed, extra_summed


def state_kernel(forget_ref, value_ref, floor_ref, extra_ref, out_ref):
    rows, width = forget_ref.shape
    heads = width // LANES
    pieces = out_ref.shape[0]
    piece = LANES // pieces
    at = lax.broadcasted_iota(jnp.int32, (rows, rows), 0)
    other = lax.broadcasted_iota(jnp.int32, (rows, rows), 1)
    after = (other > at).astype(f32)
    weight, tail, extra_tail = decays(forget_ref, floor_ref, extra_ref, after)
    first = jnp.log1p(-weight[:1])
    row_at = lax.broadcasted_iota(jnp.int32, (16, LANES), 0)
    decay_rows = jnp.zeros((16, LANES), f32)
    for h in range(heads):
        lanes = slice(h * LANES, (h + 1) * LANES)
        rest = tail[:, lanes] + extra_tail[:, h : h + 1]
        total = rest[:1] + first[:, lanes] + extra_ref[h : h + 1, 0:1]
        high = total.astype(bf16).astype(f32)
        decay_rows = jnp.where(row_at == h, high, decay_rows)
        decay_rows = jnp.where(row_at == heads + h, total - high, decay_rows)
        scaled_high, scaled_low = split(weight[:, lanes] * jnp.exp(rest))
        value = value_ref[:, lanes]
        state = dot(value, scaled_high, ((0,), (0,))) + dot(value, scaled_low, ((0,), (0,)))
        for p in range(pieces):
            out_ref[p, h * piece : (h + 1) * piece, :] = state[p * piece : (p + 1) * piece].astype(bf16)
    for p in range(pieces):
        out_ref[p, heads * piece :, :] = decay_rows.astype(bf16)


def read_piece(ref, j, heads, piece):
    states = [ref[j, h * piece : (h + 1) * piece, :].astype(f32) for h in range(heads)]
    rows = ref[j, heads * piece :, :].astype(f32)
    totals = [rows[h : h + 1] + rows[heads + h : heads + h + 1] for h in range(heads)]
    return states, totals


def plane_kernel(heads, in_ref, out_ref, before_ref, passed_ref):
    members = in_ref.shape[0]
    piece = before_ref.shape[1] // heads
    running = [jnp.zeros((piece, LANES), f32) for _ in range(heads)]
    total = [jnp.zeros((1, LANES), f32) for _ in range(heads)]
    passed_ref[...] = jnp.zeros(passed_ref.shape, f32)
    for j in range(members):
        states, decay = read_piece(in_ref, j, heads, piece)
        for h in range(heads):
            before_ref[j, h * piece : (h + 1) * piece, :] = running[h]
            passed_ref[j, h : h + 1, :] = total[h]
            running[h] = jnp.exp(decay[h]) * running[h] + states[h]
            total[h] = total[h] + decay[h]
    row_at = lax.broadcasted_iota(jnp.int32, (16, LANES), 0)
    decay_rows = jnp.zeros((16, LANES), f32)
    for h in range(heads):
        high = total[h].astype(bf16).astype(f32)
        decay_rows = jnp.where(row_at == h, high, decay_rows)
        decay_rows = jnp.where(row_at == heads + h, total[h] - high, decay_rows)
    for k in range(out_ref.shape[0]):
        for h in range(heads):
            out_ref[k, h * piece : (h + 1) * piece, :] = running[h].astype(bf16)
        out_ref[k, heads * piece :, :] = decay_rows.astype(bf16)


def carry_kernel(heads, place_ref, in_ref, before_ref, passed_ref, out_ref):
    piece = before_ref.shape[1] // heads
    place = place_ref[0]
    running = [jnp.zeros((piece, LANES), f32) for _ in range(heads)]
    for k in range(in_ref.shape[0]):
        states, decay = read_piece(in_ref, k, heads, piece)
        for h in range(heads):
            following = jnp.exp(decay[h]) * running[h] + states[h]
            running[h] = jnp.where(k < place, following, running[h])
    for j in range(out_ref.shape[0]):
        for h in range(heads):
            rows = slice(h * piece, (h + 1) * piece)
            out_ref[j, rows, :] = (
                jnp.exp(passed_ref[j, h : h + 1, :]) * running[h] + before_ref[j, rows, :]
            ).astype(bf16)


def local_kernel(query_ref, forget_ref, value_ref, floor_ref, extra_ref, out_ref, late_ref):
    rows, width = query_ref.shape
    at = lax.broadcasted_iota(jnp.int32, (rows, rows), 0)
    other = lax.broadcasted_iota(jnp.int32, (rows, rows), 1)
    upto = ((other <= at) & (at // SPAN == other // SPAN)).astype(f32)
    weight, summed, extra_summed = decays(forget_ref, floor_ref, extra_ref, upto)
    query = silu(query_ref[...].astype(f32))
    causal = lax.broadcasted_iota(jnp.int32, (SPAN, SPAN), 0) >= lax.broadcasted_iota(
        jnp.int32, (SPAN, SPAN), 1
    )
    for h in range(width // LANES):
        lanes = slice(h * LANES, (h + 1) * LANES)
        running = summed[:, lanes] + extra_summed[:, h : h + 1]
        asked = query[:, lanes] * jnp.exp(running)
        state = jnp.zeros((LANES, LANES), f32)
        passed = jnp.zeros((1, LANES), f32)
        for b in range(rows // SPAN):
            part = slice(b * SPAN, (b + 1) * SPAN)
            decay = running[part]
            final = decay[SPAN - 1 :]
            asked_now = asked[part].astype(bf16)
            value = value_ref[part, lanes]
            given = weight[part, lanes]
            scores = dot(asked_now, (given * jnp.exp(-decay)).astype(bf16), ((1,), (1,)))
            scores = jnp.where(causal, scores, 0.0).astype(bf16)
            out = dot(scores, value)
            if b:
                out = out + dot(asked_now, state.astype(bf16), ((1,), (1,)))
            out_ref[part, lanes] = out
            late_ref[part, lanes] = (asked[part] * jnp.exp(passed)).astype(bf16)
            passed = passed + final
            kept = (given * jnp.exp(final - decay)).astype(bf16)
            state = state * jnp.exp(final) + dot(value, kept, ((0,), (0,)))


def head_kernel(local_ref, late_ref, carry_ref, gain_ref, gate_ref, out_ref):
    width = local_ref.shape[1]
    heads = width // LANES
    piece = carry_ref.shape[1] // heads
    for h in range(heads):
        lanes = slice(h * LANES, (h + 1) * LANES)
        carried = jnp.concatenate(
            [carry_ref[p, h * piece : (h + 1) * piece, :] for p in range(carry_ref.shape[0])], axis=0
        )
        mixed = local_ref[:, lanes] + dot(late_ref[:, lanes], carried, ((1,), (1,)))
        scale = lax.rsqrt(jnp.mean(mixed * mixed, axis=-1, keepdims=True) + epsilon)
        gate = silu(gate_ref[:, lanes].astype(f32))
        hidden = (mixed * scale * gain_ref[:, lanes] * gate).astype(bf16)
        for k in range(out_ref.shape[0]):
            out_ref[k, :, lanes] = hidden


def slots_in_row(column_ref, row_ref, capacity):
    tokens = column_ref.shape[0]
    earlier = lax.broadcasted_iota(jnp.int32, (tokens, tokens), 0) < lax.broadcasted_iota(
        jnp.int32, (tokens, tokens), 1
    )
    slots = []
    for j in range(TOPK):
        mine = row_ref[j : j + 1, :]
        rank = jnp.zeros((1, tokens), f32)
        for i in range(j + 1):
            same = column_ref[:, i : i + 1] == mine
            if i == j:
                same = same & earlier
            rank = rank + jnp.sum(same.astype(f32), axis=0, keepdims=True)
        slots.append(mine * capacity + rank.astype(jnp.int32))
    return slots


def slots_in_column(column_ref, row_ref, capacity):
    tokens = column_ref.shape[0]
    earlier = lax.broadcasted_iota(jnp.int32, (tokens, tokens), 1) < lax.broadcasted_iota(
        jnp.int32, (tokens, tokens), 0
    )
    slots = []
    for j in range(TOPK):
        mine = column_ref[:, j : j + 1]
        rank = jnp.zeros((tokens, 1), f32)
        for i in range(j + 1):
            same = row_ref[i : i + 1, :] == mine
            if i == j:
                same = same & earlier
            rank = rank + jnp.sum(same.astype(f32), axis=1, keepdims=True)
        slots.append(mine * capacity + rank.astype(jnp.int32))
    return slots


def dispatch_kernel(capacity, mix_ref, stream_ref, gain_ref, column_ref, row_ref, residual_ref, *send_refs):
    tokens, width = stream_ref.shape
    blocks, _, block = mix_ref.shape
    square = jnp.zeros((tokens, 1), f32)
    for k in range(blocks):
        lanes = slice(k * block, (k + 1) * block)
        residual = stream_ref[:, lanes].astype(f32) + mix_ref[k].astype(f32)
        residual_ref[:, lanes] = residual
        square = square + jnp.sum(residual * residual, axis=1, keepdims=True)
    scale = lax.rsqrt(square / width + epsilon)
    slots = slots_in_row(column_ref, row_ref, capacity)
    slot_at = lax.broadcasted_iota(jnp.int32, (send_refs[0].shape[0], tokens), 0)
    table = ((slot_at == slots[0]) | (slot_at == slots[1])).astype(f32).astype(bf16)
    part = width // len(send_refs)
    for k, send_ref in enumerate(send_refs):
        lanes = slice(k * part, (k + 1) * part)
        normed = (residual_ref[:, lanes] * scale * gain_ref[:, lanes]).astype(bf16)
        send_ref[...] = dot(table, normed).astype(bf16)


def combine_kernel(capacity, results_ref, residual_ref, column_ref, row_ref, weight_ref, out_ref):
    tokens = residual_ref.shape[0]
    slots = slots_in_column(column_ref, row_ref, capacity)
    weight = weight_ref[...]
    weight = weight / jnp.sum(weight, axis=1, keepdims=True)
    slot_at = lax.broadcasted_iota(jnp.int32, (tokens, results_ref.shape[0]), 1)
    table = jnp.zeros((tokens, results_ref.shape[0]), f32)
    for j in range(TOPK):
        table = table + jnp.where(slot_at == slots[j], weight[:, j : j + 1], 0.0)
    high, low = split(table)
    results = results_ref[...]
    out_ref[...] = (residual_ref[...] + (dot(high, results) + dot(low, results))).astype(bf16)


def spread(value, axes):
    return lax.all_to_all(value, axes, split_axis=0, concat_axis=0, tiled=True)


def per_device(
    query,
    forget_preact,
    value_input,
    output_gate,
    forget_minimum,
    extra_log_decay,
    head_norm_gain,
    output_weight,
    stream,
    feedforward_gain,
    routes,
    router_weight,
    expert_gate_weight,
    expert_up_weight,
    expert_down_weight,
):
    window_rows, width = query.shape
    heads = width // LANES
    tp_size = lax.axis_size(TP)
    sp_size = lax.axis_size(SP)
    plane = lax.axis_size(PLANE)
    planes = lax.axis_size("sp_0")
    quarter_rows, model_width = stream.shape
    capacity = window_rows // sp_size
    piece = LANES // plane

    both = jnp.stack([expert_gate_weight[0], expert_up_weight[0]])
    paired = lax.all_gather(both, "tp_1")
    down = lax.all_gather(expert_down_weight[0], TP)

    floor = forget_minimum.reshape(1, -1)
    message = jax.ShapeDtypeStruct((plane, heads * piece + 16, LANES), bf16)
    states = call(state_kernel, message, forget_preact, value_input, floor, extra_log_decay)
    states = spread(states, PLANE)
    totals, before, passed = call(
        lambda *refs: plane_kernel(heads, *refs),
        (
            jax.ShapeDtypeStruct((planes, heads * piece + 16, LANES), bf16),
            jax.ShapeDtypeStruct((plane, heads * piece, LANES), f32),
            jax.ShapeDtypeStruct((plane, 8, LANES), f32),
        ),
        states,
    )
    totals = spread(totals, "sp_0")
    local, late = call(
        local_kernel,
        (
            jax.ShapeDtypeStruct((window_rows, width), f32),
            jax.ShapeDtypeStruct((window_rows, width), bf16),
        ),
        query,
        forget_preact,
        value_input,
        floor,
        extra_log_decay,
    )
    place = lax.axis_index("sp_0").astype(jnp.int32).reshape(1)
    carried = call(
        lambda *refs: carry_kernel(heads, *refs),
        jax.ShapeDtypeStruct((plane, heads * piece, LANES), bf16),
        place,
        totals,
        before,
        passed,
        smem=(0,),
    )
    carried = spread(carried, PLANE)
    hidden = call(
        head_kernel,
        jax.ShapeDtypeStruct((tp_size, window_rows, width), bf16),
        local,
        late,
        carried,
        head_norm_gain.reshape(1, -1),
        output_gate,
    )
    hidden = spread(hidden, TP)
    projected = jnp.einsum(
        "ptc,pcd->td",
        hidden,
        output_weight.reshape(tp_size, width, -1),
        preferred_element_type=f32,
    ).astype(bf16)
    mix = spread(projected.reshape(tp_size, quarter_rows, -1), TP)

    own = lax.dynamic_slice_in_dim(routes, lax.axis_index(TP) * quarter_rows, quarter_rows, 0)
    own_rows = own.T
    halves = 2
    half = model_width // halves
    residual, *sends = call(
        lambda *refs: dispatch_kernel(capacity, *refs),
        (jax.ShapeDtypeStruct((quarter_rows, model_width), f32),)
        + (jax.ShapeDtypeStruct((window_rows, half), bf16),) * halves,
        mix,
        stream,
        feedforward_gain.reshape(1, -1),
        own,
        own_rows,
    )
    hidden_part = expert_gate_weight.shape[2]
    acts = 0.0
    for k, send in enumerate(sends):
        received = spread(send.reshape(sp_size, capacity, half), SP).reshape(window_rows, half)
        others = lax.ppermute(received, TP, ROW_PAIRS)
        rows = jnp.stack([received, others])
        weights = lax.slice_in_dim(paired, k * half, (k + 1) * half, axis=2)
        acts = acts + jnp.einsum("std,pgdf->gstpf", rows, weights, preferred_element_type=f32)
    inner = (silu(acts[0]) * acts[1]).astype(bf16)
    mine, theirs = inner[0], inner[1]
    rest = lax.ppermute(theirs, TP, ROW_PAIRS)
    first_half = lax.axis_index("tp_0") == 0
    inner = jnp.concatenate(
        [jnp.where(first_half, mine, rest), jnp.where(first_half, rest, mine)], axis=1
    ).reshape(window_rows, tp_size * hidden_part)
    expert_out = jnp.dot(
        inner, down.reshape(tp_size * hidden_part, model_width), preferred_element_type=f32
    ).astype(bf16)
    returned = spread(expert_out.reshape(sp_size, capacity, model_width), SP)
    return call(
        lambda *refs: combine_kernel(capacity, *refs),
        jax.ShapeDtypeStruct((quarter_rows, model_width), bf16),
        returned.reshape(window_rows, model_width),
        residual,
        own,
        own_rows,
        router_weight,
    )


def solution(mesh):
    torus = Mesh(mesh.devices.reshape(8, 4, 2, 2, 2), SP_TP)
    placed = (
        P(SP, TP),
        P(SP, TP),
        P(SP, TP),
        P(SP, TP),
        P(TP),
        P(TP, SP),
        P(TP),
        P(None, TP),
        P(SP_TP, None),
        P(),
        P(SP, None),
        P(SP_TP, None),
        P(SP, None, TP),
        P(SP, None, TP),
        P(SP, TP, None),
    )
    return jax.shard_map(
        per_device, mesh=torus, in_specs=placed, out_specs=P(SP_TP, None), check_vma=False
    )
```

time: 461 us -> 301 us (0.65)
  blocking collectives: 122 us -> 35.4 us
  waiting for transfers between devices: 185 us -> 142 us
  other arithmetic: 43 us -> 5.26 us
  starting transfers between devices: 19.1 us -> 45.9 us
  local copies, waits for them, and re-layouts: 53.4 us -> 35.2 us
  Pallas kernels: 0 us -> 8.57 us
  matrix products: 22.8 us -> 14.4 us
    reduce_scatter x1 -> x0, waiting for transfers between devices: 67.4 us -> none  [per_device(): lax.psum_scatter(jnp.dot(inner_act, expert_down_weight[0], preferred_elem...]
    all_gather x1 -> x2, waiting for transfers between devices: 63.3 us -> 0.02 us  [the longest x1 0.02 us: per_device(): down = lax.all_gather(expert_down_weight[0], TP)]
    all_gather x6 -> x0, blocking collectives: 62.7 us -> none  [entering(): lax.all_gather(part.astype(kind), axis)]
    all_to_all x3 -> x6, waiting for transfers between devices: 53.9 us -> 101 us  [spread(): return lax.all_to_all(value, axes, split_axis=0, concat_axis=0, tiled=True)]
    ppermute x0 -> x3, waiting for transfers between devices: none -> 39.7 us  [the longest x2 32.6 us: per_device(): others = lax.ppermute(received, TP, ROW_PAIRS)]
    all_to_all x3 -> x6, starting transfers between devices: 19.1 us -> 43.1 us  [spread(): return lax.all_to_all(value, axes, split_axis=0, concat_axis=0, tiled=True)]
    all_to_all x1 -> x2, blocking collectives: 59.1 us -> 35.4 us  [spread(): return lax.all_to_all(value, axes, split_axis=0, concat_axis=0, tiled=True)]
    dot_general x4 -> x0, other arithmetic: 21.9 us -> none  [block_step(): jnp.einsum('htk,hsk,htsk->hts', query_block, weight_blk, decay_table, pre...]
  transfers between devices with their start and end apart: 5 -> 11, of which waited for: 5 -> 9; matrix products, arithmetic and copies ran while one was open for 0% -> 10% of each run, Pallas kernels for 0% -> 2%
where the time goes in v1:
time: 301 us; the launch traced here: 300 us
  waiting for transfers between devices  142 us (47%)
  starting transfers between devices  45.9 us (15%)
  blocking collectives  35.4 us (12%)
  local copies, waits for them, and re-layouts  35.2 us (12%)
  matrix products  14.4 us (5%)
  between operations  13.6 us (5%)
  Pallas kernels  8.57 us (3%)
  other arithmetic  5.26 us (2%)
    all_to_all x6, waiting for transfers between devices, spread(): return lax.all_to_all(value, axes, split_axis=0, concat_axis=0, tiled=True)  101 us
    all_to_all x6, starting transfers between devices, spread(): return lax.all_to_all(value, axes, split_axis=0, concat_axis=0, tiled=True)  43.1 us
    all_to_all x2, blocking collectives, spread(): return lax.all_to_all(value, axes, split_axis=0, concat_axis=0, tiled=True)  35.4 us
    ppermute x2, waiting for transfers between devices, per_device(): others = lax.ppermute(received, TP, ROW_PAIRS)  32.6 us
    all_gather x1, local copies, waits for them, and re-layouts, per_device(): paired = lax.all_gather(both, 'tp_1')  8.76 us
    pallas_call x7, Pallas kernels, call(): pl.pallas_call(kernel, out_shape=out_shape, in_specs=specs, out_specs=out...  8.57 us
    unnamed x47, local copies, waits for them, and re-layouts  7.83 us
    ppermute x1, waiting for transfers between devices, per_device(): rest = lax.ppermute(theirs, TP, ROW_PAIRS)  7.09 us
  transfers between devices with their start and end apart: 11, of which 9 were waited for; matrix products, arithmetic and copies ran while one was open for 10% of the time, Pallas kernels for 2%

profile of v1, /device:TPU:1, one launch (start us, length us, event | category | flops | bytes accessed | tf_op | source)
XLA Modules:
  0.0 300.0 jit_solution(5442101591472961547)
XLA Ops:
  6.5 4.0 %pad_maximum_fusion = bf16[2,3072,256]{2,1,0:T(8,128)(2,1)} fusion(bf16[1,3072,256]{2,1,0:T(8,128)(2,1)} %param.28, bf16[1,3072,256]{2,1,0:T(8,128)(2,1)} %param.27), kind=kLoop, calls=%fused_computation.6 | loop fusion | flops 1572864 | bytes 6291456 | tf_op jit(solution)/shard_map/stack | solution.py:291
  11.5 1.4 shard_map.146
  13.0 11.0 %all_to_all.40.refs_0_ = bf16[8,64,128]{2,1,0:T(8,128)(2,1)S(1)} all-to-all(bf16[8,64,128]{2,1,0:T(8,128)(2,1)S(1)} %shard_map.146), channel_id=1, replica_groups=mesh['sp_0'=8,'sp_1'=4,'sp_2'=2,'tp_0'=2,'tp_1'=2] {'sp_1','sp_2'}, dimensions={0} | all-to-all | bytes 262144 | tf_op jit(solution)/shard_map/all_to_all | solution.py:261
  24.7 8.2 %all-to-all-start.1 = ((bf16[8,64,128]{2,1,0:T(8,128)(2,1)}), bf16[8,64,128]{2,1,0:T(8,128)(2,1)S(1)}, u32[]{:S(2)}, u32[]{:S(2)}) async-start(bf16[8,64,128]{2,1,0:T(8,128)(2,1)} %get-tuple-element.15), calls=%async_computation.1 | async-start | bytes 262144 | tf_op jit(solution)/shard_map/all_to_all | solution.py:261
  32.8 7.9 %all-to-all-done.1.refs_1_ = bf16[8,64,128]{2,1,0:T(8,128)(2,1)S(1)} async-done(((bf16[8,64,128]{2,1,0:T(8,128)(2,1)}), bf16[8,64,128]{2,1,0:T(8,128)(2,1)S(1)}, u32[]{:S(2)}, u32[]{:S(2)}) %all-to-all-start.1) | async-done | bytes 131104 | tf_op jit(solution)/shard_map/all_to_all | solution.py:261
  40.7 0.7 shard_map.148
  41.4 5.6 %all-to-all-start.2 = ((bf16[8,48,128]{2,1,0:T(8,128)(2,1)}), bf16[8,48,128]{2,1,0:T(8,128)(2,1)S(1)}, u32[]{:S(2)}, u32[]{:S(2)}) async-start(bf16[8,48,128]{2,1,0:T(8,128)(2,1)} %shard_map.148), calls=%async_computation.2 | async-start | bytes 196608 | tf_op jit(solution)/shard_map/all_to_all | solution.py:261
  47.0 2.9 shard_map.145
  50.7 1.4 all-to-all-done.2.carry_ref
  52.0 0.9 copy-done.11
  53.0 0.9 copy-done.13
  54.3 24.4 %all_to_all.41 = bf16[4,256,384]{2,1,0:T(8,128)(2,1)S(1)} all-to-all(bf16[4,256,384]{2,1,0:T(8,128)(2,1)S(1)} %shard_map.149), channel_id=1, replica_groups=mesh['sp_0'=8,'sp_1'=4,'sp_2'=2,'tp_0'=2,'tp_1'=2] {'tp_0','tp_1'}, dimensions={0} | all-to-all | bytes 1572864 | tf_op jit(solution)/shard_map/all_to_all | solution.py:261
  78.7 1.5 fusion.7
  80.2 3.5 %all-to-all-start.4 = ((bf16[4,64,768]{2,1,0:T(8,128)(2,1)}), bf16[4,64,768]{2,1,0:T(8,128)(2,1)S(1)}, u32[]{:S(2)}, u32[]{:S(2)}) async-start(bf16[4,64,768]{2,1,0:T(8,128)(2,1)} %bitcast.6), calls=%async_computation.4 | async-start | bytes 786432 | tf_op jit(solution)/shard_map/all_to_all | solution.py:261
  83.8 0.7 copy.24.refs_3_.refs_2_
  84.6 11.2 %all-to-all-done.4.refs_0_ = bf16[4,64,768]{2,1,0:T(8,128)(2,1)S(1)} async-done(((bf16[4,64,768]{2,1,0:T(8,128)(2,1)}), bf16[4,64,768]{2,1,0:T(8,128)(2,1)S(1)}, u32[]{:S(2)}, u32[]{:S(2)}) %all-to-all-start.4) | async-done | bytes 393248 | tf_op jit(solution)/shard_map/all_to_all | solution.py:261
  95.8 1.0 copy-done.7
  96.8 0.8 copy-done.8
  97.6 0.8 shard_map.150
  98.4 0.9 copy-done.2
  99.3 0.9 copy-done.5
  100.2 2.4 reshape.46
  102.6 7.7 %all-to-all-start.6 = ((bf16[64,4,1536]{2,1,0:T(4,128)(2,1)}), bf16[64,4,1536]{2,1,0:T(4,128)(2,1)}, u32[]{:S(2)}, u32[]{:S(2)}) async-start(bf16[64,4,1536]{2,1,0:T(4,128)(2,1)} %reshape.46), calls=%async_computation.6 | async-start | bytes 1572864 | tf_op jit(solution)/shard_map/all_to_all | solution.py:261
  110.3 1.1 reshape.44
  111.3 22.1 %all-to-all-done.6 = bf16[64,4,1536]{2,1,0:T(4,128)(2,1)} async-done(((bf16[64,4,1536]{2,1,0:T(4,128)(2,1)}), bf16[64,4,1536]{2,1,0:T(4,128)(2,1)}, u32[]{:S(2)}, u32[]{:S(2)}) %all-to-all-start.6) | async-done | bytes 786464 | tf_op jit(solution)/shard_map/all_to_all | solution.py:261
  133.4 5.8 %all-to-all-start.5 = ((bf16[64,4,1536]{2,1,0:T(4,128)(2,1)}), bf16[64,4,1536]{2,1,0:T(4,128)(2,1)S(1)}, u32[]{:S(2)}, u32[]{:S(2)}) async-start(bf16[64,4,1536]{2,1,0:T(4,128)(2,1)} %reshape.44), calls=%async_computation.5 | async-start | bytes 1572864 | tf_op jit(solution)/shard_map/all_to_all | solution.py:261
  139.3 2.3 reshape.47
  141.6 0.9 collective-permute-start.1
  142.4 19.8 %all-to-all-done.5 = bf16[64,4,1536]{2,1,0:T(4,128)(2,1)S(1)} async-done(((bf16[64,4,1536]{2,1,0:T(4,128)(2,1)}), bf16[64,4,1536]{2,1,0:T(4,128)(2,1)S(1)}, u32[]{:S(2)}, u32[]{:S(2)}) %all-to-all-start.5) | async-done | bytes 786464 | tf_op jit(solution)/shard_map/all_to_all | solution.py:261
  162.3 1.1 reshape.45
  163.3 0.9 collective-permute-start
  164.2 2.3 stack_reshape.7
  166.5 1.1 stack_reshape.6
  167.6 8.8 %copy.23 = bf16[4,3072,256]{1,2,0:T(8,128)(2,1)} copy(bf16[4,3072,256]{2,1,0:T(8,128)(2,1)} %all-gather.6.cloned.1.call-done) | data formatting | bytes 12582912 | tf_op jit(solution)/shard_map/all_gather | solution.py:292
  176.3 3.0 %collective-permute-done.1 = bf16[256,1536]{1,0:T(8,128)(2,1)} collective-permute-done((bf16[256,1536]{1,0:T(8,128)(2,1)}, bf16[256,1536]{1,0:T(8,128)(2,1)}, u32[]{:S(2)}, u32[]{:S(2)}) %collective-permute-start.1) | collective-permute-done | bytes 786464 | tf_op jit(solution)/shard_map/ppermute | solution.py:368
  179.4 4.1 %fusion.1 = f32[2,2,256,2,256]{4,2,3,1,0:T(8,128)S(1)} fusion(bf16[2,2,3072,256]{2,3,1,0:T(8,128)(2,1)} %bitcast.70, bf16[1,256,1536]{2,1,0:T(8,128)(2,1)} %bitcast.14, bf16[1,256,1536]{2,1,0:T(8,128)(2,1)S(1)} %copy-done.18), kind=kOutput, calls=%fused_computation.3 | convolution fusion | flops 1613758464 | bytes 6815744 | tf_op jit(solution)/shard_map/std,pgdf->gstpf/dot_general | solution.py:371
  183.5 29.6 %collective-permute-done = bf16[256,1536]{1,0:T(8,128)(2,1)} collective-permute-done((bf16[256,1536]{1,0:T(8,128)(2,1)}, bf16[256,1536]{1,0:T(8,128)(2,1)}, u32[]{:S(2)}, u32[]{:S(2)}) %collective-permute-start) | collective-permute-done | bytes 786464 | tf_op jit(solution)/shard_map/ppermute | solution.py:368
  213.1 3.0 add_bitcast_fusion
  216.4 1.0 collective-permute-start.2
  217.4 7.1 %collective-permute-done.2 = bf16[256,2,256]{0,2,1:T(8,128)(2,1)} collective-permute-done((bf16[256,2,256]{0,2,1:T(8,128)(2,1)S(1)}, bf16[256,2,256]{0,2,1:T(8,128)(2,1)}, u32[]{:S(2)}, u32[]{:S(2)}) %collective-permute-start.2) | collective-permute-done | bytes 262176 | tf_op jit(solution)/shard_map/ppermute | solution.py:374
  224.4 1.0 broadcast_select_fusion.1
  225.5 5.8 %fusion = bf16[256,3072]{1,0:T(8,128)(2,1)} fusion(bf16[4,256,3072]{2,1,0:T(8,128)(2,1)} %all-gather.4.cloned.1.call-done, bf16[256,2,256]{0,2,1:T(8,128)(2,1)S(1)} %get-tuple-element.22, bf16[256,2,256]{0,2,1:T(8,128)(2,1)S(1)} %get-tuple-element.21), kind=kOutput, calls=%fused_computation.1 | convolution fusion | flops 1611661312 | bytes 8388608 | tf_op jit(solution)/shard_map/dot_general | solution.py:379
  231.3 3.9 %reshape.48 = bf16[64,4,3072]{2,1,0:T(4,128)(2,1)} reshape(bf16[256,3072]{1,0:T(8,128)(2,1)} %fusion) | data formatting | bytes 3145728 | tf_op jit(solution)/shard_map/reshape | solution.py:382
  235.2 12.3 %all-to-all-start.7 = ((bf16[64,4,3072]{2,1,0:T(4,128)(2,1)}), bf16[64,4,3072]{2,1,0:T(4,128)(2,1)}, u32[]{:S(2)}, u32[]{:S(2)}) async-start(bf16[64,4,3072]{2,1,0:T(4,128)(2,1)} %reshape.48), calls=%async_computation.7 | async-start | bytes 3145728 | tf_op jit(solution)/shard_map/all_to_all | solution.py:261
  247.6 38.9 %all-to-all-done.7 = bf16[64,4,3072]{2,1,0:T(4,128)(2,1)} async-done(((bf16[64,4,3072]{2,1,0:T(4,128)(2,1)}), bf16[64,4,3072]{2,1,0:T(4,128)(2,1)}, u32[]{:S(2)}, u32[]{:S(2)}) %all-to-all-start.7) | async-done | bytes 1572896 | tf_op jit(solution)/shard_map/all_to_all | solution.py:261
  286.4 3.7 %reshape.49.refs_0_ = bf16[256,3072]{1,0:T(8,128)(2,1)} reshape(bf16[64,4,3072]{2,1,0:T(4,128)(2,1)} %all-to-all-done.7) | data formatting | bytes 3145728 | tf_op jit(solution)/shard_map/reshape | solution.py:386
  290.2 1.4 copy-done.1
  291.6 1.6 shard_map.151
  (54 shorter events, 3.4 us)
Async XLA Ops:
  6.5 72.2 %copy-start = (bf16[1536,768]{1,0:T(8,128)(2,1)S(1)}, bf16[1536,768]{1,0:T(8,128)(2,1)}, u32[]{:S(2)}) copy-start(bf16[1536,768]{1,0:T(8,128)(2,1)} %param.22) | copy-start | bytes 7077892
  6.5 161.0 %all-gather.6.cloned.1.call-start = ((), (), s32[]{:S(2)}) async-start(), calls=%async_computation.9 | async-start | bytes 9437184 | tf_op jit(solution)/shard_map/all_gather | solution.py:292
  10.5 0.8 copy-start.19
  10.5 0.9 copy-start.3
  10.5 1.0 copy-start.4
  10.5 1.0 copy-start.14
  10.5 36.5 %copy-start.10 = (bf16[256,384]{1,0:T(8,128)(2,1)S(1)}, bf16[256,384]{1,0:T(8,128)(2,1)}, u32[]{:S(2)}) copy-start(bf16[256,384]{1,0:T(8,128)(2,1)} %query_ref.1) | copy-start | bytes 589828
  10.5 40.1 %copy-start.20 = (f32[384]{0:T(512)S(1)}, f32[384]{0:T(512)}, u32[]{:S(2)}) copy-start(f32[384]{0:T(512)} %param.21) | copy-start | bytes 4612
  10.6 214.9 %all-gather.4.cloned.1.call-start = ((), (), s32[]{:S(2)}) async-start(), calls=%async_computation.8 | async-start | bytes 7864320 | tf_op jit(solution)/shard_map/all_gather | solution.py:293
  24.7 16.0 %all-to-all-start.1 = ((bf16[8,64,128]{2,1,0:T(8,128)(2,1)}), bf16[8,64,128]{2,1,0:T(8,128)(2,1)S(1)}, u32[]{:S(2)}, u32[]{:S(2)}) async-start(bf16[8,64,128]{2,1,0:T(8,128)(2,1)} %get-tuple-element.15), calls=%async_computation.1 | async-start | bytes 262144 | tf_op jit(solution)/shard_map/all_to_all | solution.py:261
  41.4 10.6 %all-to-all-start.2 = ((bf16[8,48,128]{2,1,0:T(8,128)(2,1)}), bf16[8,48,128]{2,1,0:T(8,128)(2,1)S(1)}, u32[]{:S(2)}, u32[]{:S(2)}) async-start(bf16[8,48,128]{2,1,0:T(8,128)(2,1)} %shard_map.148), calls=%async_computation.2 | async-start | bytes 196608 | tf_op jit(solution)/shard_map/all_to_all | solution.py:261
  50.0 0.7 copy-start.12
  52.0 0.9 copy-start.11
  53.0 0.9 copy-start.13
  78.7 5.0 %copy-start.21 = (s32[256,2]{0,1:T(2,128)S(1)}, s32[256,2]{0,1:T(2,128)}, u32[]{:S(2)}) copy-start(s32[256,2]{0,1:T(2,128)} %param.25) | copy-start | bytes 6148
  78.7 17.1 %copy-start.15 = (f32[3072]{0:T(1024)S(1)}, f32[3072]{0:T(1024)}, u32[]{:S(2)}) copy-start(f32[3072]{0:T(1024)} %param.24) | copy-start | bytes 36868
  80.2 15.6 %all-to-all-start.4 = ((bf16[4,64,768]{2,1,0:T(8,128)(2,1)}), bf16[4,64,768]{2,1,0:T(8,128)(2,1)S(1)}, u32[]{:S(2)}, u32[]{:S(2)}) async-start(bf16[4,64,768]{2,1,0:T(8,128)(2,1)} %bitcast.6), calls=%async_computation.4 | async-start | bytes 786432 | tf_op jit(solution)/shard_map/all_to_all | solution.py:261
  95.8 1.0 copy-start.7
  96.8 0.8 copy-start.8
  98.4 0.9 copy-start.2
  99.3 0.9 copy-start.5
  102.6 30.8 %all-to-all-start.6 = ((bf16[64,4,1536]{2,1,0:T(4,128)(2,1)}), bf16[64,4,1536]{2,1,0:T(4,128)(2,1)}, u32[]{:S(2)}, u32[]{:S(2)}) async-start(bf16[64,4,1536]{2,1,0:T(4,128)(2,1)} %reshape.46), calls=%async_computation.6 | async-start | bytes 1572864 | tf_op jit(solution)/shard_map/all_to_all | solution.py:261
  133.4 28.9 %all-to-all-start.5 = ((bf16[64,4,1536]{2,1,0:T(4,128)(2,1)}), bf16[64,4,1536]{2,1,0:T(4,128)(2,1)S(1)}, u32[]{:S(2)}, u32[]{:S(2)}) async-start(bf16[64,4,1536]{2,1,0:T(4,128)(2,1)} %reshape.44), calls=%async_computation.5 | async-start | bytes 1572864 | tf_op jit(solution)/shard_map/all_to_all | solution.py:261
  141.6 37.8 %collective-permute-start.1 = (bf16[256,1536]{1,0:T(8,128)(2,1)}, bf16[256,1536]{1,0:T(8,128)(2,1)}, u32[]{:S(2)}, u32[]{:S(2)}) collective-permute-start(bf16[256,1536]{1,0:T(8,128)(2,1)} %reshape.47), channel_id=1, source_target_pairs={{1,2},{2,1},{3,0},{0,3},{5,6},{6,5},{7,4},{4,7},{9,10},{10,9},{11,... | collective-permute-start | bytes 2359304 | tf_op jit(solution)/shard_map/ppermute | solution.py:368
  163.3 49.7 %collective-permute-start = (bf16[256,1536]{1,0:T(8,128)(2,1)}, bf16[256,1536]{1,0:T(8,128)(2,1)}, u32[]{:S(2)}, u32[]{:S(2)}) collective-permute-start(bf16[256,1536]{1,0:T(8,128)(2,1)} %reshape.45), channel_id=1, source_target_pairs={{1,2},{2,1},{3,0},{0,3},{5,6},{6,5},{7,4},{4,7},{9,10},{10,9},{11,... | collective-permute-start | bytes 2359304 | tf_op jit(solution)/shard_map/ppermute | solution.py:368
  167.6 11.8 %copy-start.18 = (bf16[1,256,1536]{2,1,0:T(8,128)(2,1)S(1)}, bf16[1,256,1536]{2,1,0:T(8,128)(2,1)}, u32[]{:S(2)}) copy-start(bf16[1,256,1536]{2,1,0:T(8,128)(2,1)} %stack_reshape.7) | copy-start | bytes 2359300
  179.3 33.7 %copy-start.16 = (bf16[4,3072,256]{1,2,0:T(8,128)(2,1)S(1)}, bf16[4,3072,256]{1,2,0:T(8,128)(2,1)}, u32[]{:S(2)}) copy-start(bf16[4,3072,256]{1,2,0:T(8,128)(2,1)} %copy.23) | copy-start | bytes 18874372
  179.4 33.7 %copy-start.17 = (bf16[1,256,1536]{2,1,0:T(8,128)(2,1)S(1)}, bf16[1,256,1536]{2,1,0:T(8,128)(2,1)}, u32[]{:S(2)}) copy-start(bf16[1,256,1536]{2,1,0:T(8,128)(2,1)} %stack_reshape.6) | copy-start | bytes 2359300
  216.4 8.1 %collective-permute-start.2 = (bf16[256,2,256]{0,2,1:T(8,128)(2,1)S(1)}, bf16[256,2,256]{0,2,1:T(8,128)(2,1)}, u32[]{:S(2)}, u32[]{:S(2)}) collective-permute-start(bf16[256,2,256]{0,2,1:T(8,128)(2,1)S(1)} %slice_bitcast_fusion.8), channel_id=1, source_target_pairs={{1,2},{2,1},{3,0},{0,3},{5,6},{6,5},{7,4},{4,7},{9,10},{10,9},{11,... | collective-permute-start | bytes 786440 | tf_op jit(solution)/shard_map/ppermute | solution.py:374
  235.1 12.3 %copy-start.22 = (f32[64,2]{0,1:T(2,128)S(1)}, f32[64,2]{0,1:T(2,128)}, u32[]{:S(2)}) copy-start(f32[64,2]{0,1:T(2,128)} %param.26) | copy-start | bytes 1540
  235.2 51.3 %all-to-all-start.7 = ((bf16[64,4,3072]{2,1,0:T(4,128)(2,1)}), bf16[64,4,3072]{2,1,0:T(4,128)(2,1)}, u32[]{:S(2)}, u32[]{:S(2)}) async-start(bf16[64,4,3072]{2,1,0:T(4,128)(2,1)} %reshape.48), calls=%async_computation.7 | async-start | bytes 3145728 | tf_op jit(solution)/shard_map/all_to_all | solution.py:261
  247.5 42.7 %copy-start.6 = (f32[64,3072]{1,0:T(8,128)S(1)}, f32[64,3072]{1,0:T(8,128)}, u32[]{:S(2)}) copy-start(f32[64,3072]{1,0:T(8,128)} %copy-done.5) | copy-start | bytes 2359300
  247.5 42.7 %copy-start.9 = (s32[64,2]{1,0:T(8,128)S(1)}, s32[64,2]{1,0:T(8,128)}, u32[]{:S(2)}) copy-start(s32[64,2]{1,0:T(8,128)} %copy.24.refs_3_.refs_2_) | copy-start | bytes 1540
  290.2 1.4 copy-start.1
Sparse Core Ops, SparseCore 0:
  10.7 101.6 all-gather.5
  114.2 102.8 all-gather.3

commit v2 on v1

--- a/solution.py
+++ b/solution.py
@@ -6,14 +6,19 @@
 from jax.sharding import Mesh
 from jax.sharding import PartitionSpec as P
 
+
 LANES = 128
 SPAN = 64
+PARTS = 2
+DOWN_LANES = 512
 TOPK = 2
 PLANE = ("sp_1", "sp_2")
 SP = ("sp_0", "sp_1", "sp_2")
 TP = ("tp_0", "tp_1")
 SP_TP = SP + TP
 ROW_PAIRS = ((1, 2), (2, 1), (3, 0), (0, 3))
+WEIGHT_PAIRS = ((0, 1), (1, 0), (2, 3), (3, 2))
+FIRST_SHARE = (2, 3)
 
 f32 = jnp.float32
 bf16 = jnp.bfloat16
@@ -34,18 +39,20 @@
     return value * jax.nn.sigmoid(value)
 
 
-def call(kernel, out_shape, *operands, smem=()):
-    specs = [
-        pl.BlockSpec(memory_space=pltpu.SMEM if k in smem else pltpu.VMEM)
-        for k in range(len(operands))
-    ]
-    outs = jax.tree.map(lambda _: pl.BlockSpec(memory_space=pltpu.VMEM), out_shape)
+def call(kernel, out_shape, *operands, kinds="", scratch=(), mib=12):
+    spaces = {
+        "v": pl.BlockSpec(memory_space=pltpu.VMEM),
+        "h": pl.BlockSpec(memory_space=pltpu.HBM),
+        "s": pl.BlockSpec(memory_space=pltpu.SMEM),
+    }
+    kinds = kinds or "v" * len(operands)
     return pl.pallas_call(
         kernel,
         out_shape=out_shape,
-        in_specs=specs,
-        out_specs=outs,
-        compiler_params=pltpu.CompilerParams(vmem_limit_bytes=48 * 1024 * 1024),
+        in_specs=[spaces[kind] for _, kind in zip(operands, kinds, strict=True)],
+        out_specs=jax.tree.map(lambda _: spaces["v"], out_shape),
+        scratch_shapes=scratch,
+        compiler_params=pltpu.CompilerParams(vmem_limit_bytes=mib * 1024 * 1024),
     )(*operands)
 
 
@@ -135,7 +142,7 @@
             ).astype(bf16)
 
 
-def local_kernel(query_ref, forget_ref, value_ref, floor_ref, extra_ref, out_ref, late_ref):
+def local_kernel(query_ref, forget_ref, value_ref, floor_ref, extra_ref, out_ref):
     rows, width = query_ref.shape
     at = lax.broadcasted_iota(jnp.int32, (rows, rows), 0)
     other = lax.broadcasted_iota(jnp.int32, (rows, rows), 1)
@@ -163,15 +170,15 @@
             out = dot(scores, value)
             if b:
                 out = out + dot(asked_now, state.astype(bf16), ((1,), (1,)))
-            out_ref[part, lanes] = out
-            late_ref[part, lanes] = (asked[part] * jnp.exp(passed)).astype(bf16)
+            out_ref[0, part, lanes] = out
+            out_ref[1, part, lanes] = asked[part] * jnp.exp(passed)
             passed = passed + final
             kept = (given * jnp.exp(final - decay)).astype(bf16)
             state = state * jnp.exp(final) + dot(value, kept, ((0,), (0,)))
 
 
-def head_kernel(local_ref, late_ref, carry_ref, gain_ref, gate_ref, out_ref):
-    width = local_ref.shape[1]
+def head_kernel(local_ref, carry_ref, gain_ref, gate_ref, out_ref):
+    width = local_ref.shape[2]
     heads = width // LANES
     piece = carry_ref.shape[1] // heads
     for h in range(heads):
@@ -179,7 +186,8 @@
         carried = jnp.concatenate(
             [carry_ref[p, h * piece : (h + 1) * piece, :] for p in range(carry_ref.shape[0])], axis=0
         )
-        mixed = local_ref[:, lanes] + dot(late_ref[:, lanes], carried, ((1,), (1,)))
+        late = local_ref[1, :, lanes].astype(bf16)
+        mixed = local_ref[0, :, lanes] + dot(late, carried, ((1,), (1,)))
         scale = lax.rsqrt(jnp.mean(mixed * mixed, axis=-1, keepdims=True) + epsilon)
         gate = silu(gate_ref[:, lanes].astype(f32))
         hidden = (mixed * scale * gain_ref[:, lanes] * gate).astype(bf16)
@@ -201,7 +209,7 @@
             if i == j:
                 same = same & earlier
             rank = rank + jnp.sum(same.astype(f32), axis=0, keepdims=True)
-        slots.append(mine * capacity + rank.astype(jnp.int32))
+        slots.append(mine * (PARTS * capacity) + rank.astype(jnp.int32))
     return slots
 
 
@@ -219,8 +227,24 @@
             if i == j:
                 same = same & earlier
             rank = rank + jnp.sum(same.astype(f32), axis=1, keepdims=True)
-        slots.append(mine * capacity + rank.astype(jnp.int32))
+        slots.append(mine * (PARTS * capacity) + rank.astype(jnp.int32))
     return slots
+
+
+def spread_table(rows, columns, capacity, part):
+    row = lax.broadcasted_iota(jnp.int32, (rows, columns), 0)
+    column = lax.broadcasted_iota(jnp.int32, (rows, columns), 1)
+    stride = PARTS * capacity
+    wanted = (column // capacity) * stride + part * capacity + column % capacity
+    return (row == wanted).astype(f32).astype(bf16)
+
+
+def gather_table(rows, columns, capacity, part):
+    row = lax.broadcasted_iota(jnp.int32, (rows, columns), 0)
+    column = lax.broadcasted_iota(jnp.int32, (rows, columns), 1)
+    stride = PARTS * capacity
+    wanted = (row // capacity) * stride + part * capacity + row % capacity
+    return (column == wanted).astype(f32).astype(bf16)
 
 
 def dispatch_kernel(capacity, mix_ref, stream_ref, gain_ref, column_ref, row_ref, residual_ref, *send_refs):
@@ -235,12 +259,91 @@
     scale = lax.rsqrt(square / width + epsilon)
     slots = slots_in_row(column_ref, row_ref, capacity)
     slot_at = lax.broadcasted_iota(jnp.int32, (send_refs[0].shape[0], tokens), 0)
-    table = ((slot_at == slots[0]) | (slot_at == slots[1])).astype(f32).astype(bf16)
-    part = width // len(send_refs)
-    for k, send_ref in enumerate(send_refs):
-        lanes = slice(k * part, (k + 1) * part)
-        normed = (residual_ref[:, lanes] * scale * gain_ref[:, lanes]).astype(bf16)
-        send_ref[...] = dot(table, normed).astype(bf16)
+    tables = [
+        ((slot_at == slots[0] + q * capacity) | (slot_at == slots[1] + q * capacity))
+        .astype(f32)
+        .astype(bf16)
+        for q in range(PARTS)
+    ]
+    start = 0
+    for send_ref in send_refs:
+        part = send_ref.shape[1]
+        send = jnp.zeros(send_ref.shape, f32)
+        for q in range(PARTS):
+            lanes = slice(start, start + part)
+            start += part
+            normed = (residual_ref[:, lanes] * scale * gain_ref[:, lanes]).astype(bf16)
+            send = send + dot(tables[q], normed)
+        send_ref[...] = send.astype(bf16)
+
+
+def gate_up(own_ref, others_ref, weight_refs, capacity):
+    rows, part = own_ref.shape
+    tables = [gather_table(rows // PARTS, rows, capacity, q) for q in range(PARTS)]
+    laid = [
+        jnp.concatenate([dot(table, ref[...]).astype(bf16) for table in tables], axis=1)
+        for ref in (own_ref, others_ref)
+    ]
+    for j, weight_ref in enumerate(weight_refs):
+        weight = weight_ref[: PARTS * part, :]
+        for i in range(2):
+            yield i, j, dot(laid[i], weight)
+
+
+def first_kernel(
+    capacity, own_ref, others_ref, gate_ref, gate_too_ref, up_pair_ref, parts_ref, acts_ref, kept_ref
+):
+    place = parts_ref[0] % 2
+    weight_refs = (gate_ref, up_pair_ref.at[place], gate_too_ref, up_pair_ref.at[1 - place])
+    for i, j, product in gate_up(own_ref, others_ref, weight_refs, capacity):
+        acts_ref[i, j] = product
+    left = kept_ref.shape[1]
+    for j, weight_ref in enumerate(weight_refs):
+        kept_ref[j] = weight_ref[weight_ref.shape[0] - left :, :]
+
+
+def second_kernel(capacity, own_ref, others_ref, kept_ref, acts_ref, mine_ref, theirs_ref):
+    outs = (mine_ref, theirs_ref)
+    width = kept_ref.shape[2]
+    gates = {}
+    weight_refs = [kept_ref.at[j] for j in range(kept_ref.shape[0])]
+    for i, j, product in gate_up(own_ref, others_ref, weight_refs, capacity):
+        product = product + acts_ref[i, j]
+        if j % 2 == 0:
+            gates[i] = silu(product)
+        else:
+            lanes = slice(j // 2 * width, (j // 2 + 1) * width)
+            outs[i][:, lanes] = (gates[i] * product).astype(bf16)
+
+
+def down_kernel(capacity, parts_ref, mine_ref, rest_ref, weights_ref, out_ref):
+    width = weights_ref.shape[1]
+    inner = [ref[:, k * width : (k + 1) * width] for ref in (mine_ref, rest_ref) for k in range(2)]
+    rows = mine_ref.shape[0]
+    block = out_ref.shape[1]
+    part = weights_ref.shape[2] // PARTS
+    out = jnp.zeros(out_ref.shape, f32)
+    for q in range(PARTS):
+        lanes = pl.ds(pl.multiple_of(q * part + pl.program_id(0) * block, LANES), block)
+        product = dot(inner[0], weights_ref[parts_ref[0], :, lanes])
+        for k in range(1, len(inner)):
+            product = product + dot(inner[k], weights_ref[parts_ref[k], :, lanes])
+        out = out + dot(spread_table(PARTS * rows, rows, capacity, q), product.astype(bf16))
+    out_ref[...] = out.astype(bf16)
+
+
+def project_down(capacity, parts, mine, rest, weights):
+    rows = mine.shape[0]
+    part = weights.shape[2] // PARTS
+    whole = pl.BlockSpec(memory_space=pltpu.VMEM)
+    return pl.pallas_call(
+        lambda *refs: down_kernel(capacity, *refs),
+        grid=(part // DOWN_LANES,),
+        out_shape=jax.ShapeDtypeStruct((PARTS * rows, part), bf16),
+        in_specs=[pl.BlockSpec(memory_space=pltpu.SMEM), whole, whole, whole],
+        out_specs=pl.BlockSpec((PARTS * rows, DOWN_LANES), lambda k: (0, k)),
+        compiler_params=pltpu.CompilerParams(vmem_limit_bytes=12 * 1024 * 1024),
+    )(parts, mine, rest, weights)
 
 
 def combine_kernel(capacity, results_ref, residual_ref, column_ref, row_ref, weight_ref, out_ref):
@@ -248,20 +351,24 @@
     slots = slots_in_column(column_ref, row_ref, capacity)
     weight = weight_ref[...]
     weight = weight / jnp.sum(weight, axis=1, keepdims=True)
-    slot_at = lax.broadcasted_iota(jnp.int32, (tokens, results_ref.shape[0]), 1)
-    table = jnp.zeros((tokens, results_ref.shape[0]), f32)
-    for j in range(TOPK):
-        table = table + jnp.where(slot_at == slots[j], weight[:, j : j + 1], 0.0)
-    high, low = split(table)
-    results = results_ref[...]
-    out_ref[...] = (residual_ref[...] + (dot(high, results) + dot(low, results))).astype(bf16)
+    count, part = results_ref.shape
+    for q in range(PARTS):
+        slot_at = lax.broadcasted_iota(jnp.int32, (tokens, count), 1) - q * capacity
+        table = jnp.zeros((tokens, count), f32)
+        for j in range(TOPK):
+            table = table + jnp.where(slot_at == slots[j], weight[:, j : j + 1], 0.0)
+        high, low = split(table)
+        results = results_ref[...]
+        lanes = slice(q * part, (q + 1) * part)
+        routed = dot(high, results) + dot(low, results)
+        out_ref[:, lanes] = (residual_ref[:, lanes] + routed).astype(bf16)
 
 
 def spread(value, axes):
     return lax.all_to_all(value, axes, split_axis=0, concat_axis=0, tiled=True)
 
 
-def per_device(
+def layer(
     query,
     forget_preact,
     value_input,
@@ -288,13 +395,15 @@
     capacity = window_rows // sp_size
     piece = LANES // plane
 
-    both = jnp.stack([expert_gate_weight[0], expert_up_weight[0]])
-    paired = lax.all_gather(both, "tp_1")
     down = lax.all_gather(expert_down_weight[0], TP)
+
+    up_pair = lax.all_gather(expert_up_weight[0], "tp_1")
 
     floor = forget_minimum.reshape(1, -1)
     message = jax.ShapeDtypeStruct((plane, heads * piece + 16, LANES), bf16)
-    states = call(state_kernel, message, forget_preact, value_input, floor, extra_log_decay)
+    states = call(
+        state_kernel, message, forget_preact, value_input, floor, extra_log_decay
+    )
     states = spread(states, PLANE)
     totals, before, passed = call(
         lambda *refs: plane_kernel(heads, *refs),
@@ -306,12 +415,9 @@
         states,
     )
     totals = spread(totals, "sp_0")
-    local, late = call(
+    local = call(
         local_kernel,
-        (
-            jax.ShapeDtypeStruct((window_rows, width), f32),
-            jax.ShapeDtypeStruct((window_rows, width), bf16),
-        ),
+        jax.ShapeDtypeStruct((2, window_rows, width), f32),
         query,
         forget_preact,
         value_input,
@@ -326,14 +432,13 @@
         totals,
         before,
         passed,
-        smem=(0,),
+        kinds="svvv",
     )
     carried = spread(carried, PLANE)
     hidden = call(
         head_kernel,
         jax.ShapeDtypeStruct((tp_size, window_rows, width), bf16),
         local,
-        late,
         carried,
         head_norm_gain.reshape(1, -1),
         output_gate,
@@ -346,15 +451,19 @@
         preferred_element_type=f32,
     ).astype(bf16)
     mix = spread(projected.reshape(tp_size, quarter_rows, -1), TP)
+    gate_weight, mix = lax.optimization_barrier((expert_gate_weight[0], mix))
+    gate_weight_too = lax.ppermute(gate_weight, TP, WEIGHT_PAIRS)
 
     own = lax.dynamic_slice_in_dim(routes, lax.axis_index(TP) * quarter_rows, quarter_rows, 0)
     own_rows = own.T
-    halves = 2
-    half = model_width // halves
+    first_depth = model_width * FIRST_SHARE[0] // FIRST_SHARE[1]
+    packed = [
+        jax.ShapeDtypeStruct((window_rows * PARTS, depth // PARTS), bf16)
+        for depth in (first_depth, model_width - first_depth)
+    ]
     residual, *sends = call(
         lambda *refs: dispatch_kernel(capacity, *refs),
-        (jax.ShapeDtypeStruct((quarter_rows, model_width), f32),)
-        + (jax.ShapeDtypeStruct((window_rows, half), bf16),) * halves,
+        (jax.ShapeDtypeStruct((quarter_rows, model_width), f32), *packed),
         mix,
         stream,
         feedforward_gain.reshape(1, -1),
@@ -362,28 +471,48 @@
         own_rows,
     )
     hidden_part = expert_gate_weight.shape[2]
-    acts = 0.0
-    for k, send in enumerate(sends):
-        received = spread(send.reshape(sp_size, capacity, half), SP).reshape(window_rows, half)
-        others = lax.ppermute(received, TP, ROW_PAIRS)
-        rows = jnp.stack([received, others])
-        weights = lax.slice_in_dim(paired, k * half, (k + 1) * half, axis=2)
-        acts = acts + jnp.einsum("std,pgdf->gstpf", rows, weights, preferred_element_type=f32)
-    inner = (silu(acts[0]) * acts[1]).astype(bf16)
-    mine, theirs = inner[0], inner[1]
+    rows = []
+    for send in sends:
+        received = spread(send.reshape(sp_size, PARTS * capacity, -1), SP).reshape(send.shape)
+        rows.append((received, lax.ppermute(received, TP, ROW_PAIRS)))
+    count = 4
+    place = lax.axis_index(TP).astype(jnp.int32)
+    parts = jnp.stack([place, place ^ 1, 3 - place, (3 - place) ^ 1])
+    acts, kept = call(
+        lambda *refs: first_kernel(capacity, *refs),
+        (
+            jax.ShapeDtypeStruct((2, count, window_rows, hidden_part), f32),
+            jax.ShapeDtypeStruct((count, model_width - first_depth, hidden_part), bf16),
+        ),
+        *rows[0],
+        gate_weight,
+        gate_weight_too,
+        up_pair,
+        parts,
+        kinds="vvvvvs",
+        mib=16,
+    )
+    acts, down = lax.optimization_barrier((acts, down))
+    mine, theirs = call(
+        lambda *refs: second_kernel(capacity, *refs),
+        (jax.ShapeDtypeStruct((window_rows, 2 * hidden_part), bf16),) * 2,
+        *rows[1],
+        kept,
+        acts,
+    )
     rest = lax.ppermute(theirs, TP, ROW_PAIRS)
-    first_half = lax.axis_index("tp_0") == 0
-    inner = jnp.concatenate(
-        [jnp.where(first_half, mine, rest), jnp.where(first_half, rest, mine)], axis=1
-    ).reshape(window_rows, tp_size * hidden_part)
-    expert_out = jnp.dot(
-        inner, down.reshape(tp_size * hidden_part, model_width), preferred_element_type=f32
-    ).astype(bf16)
-    returned = spread(expert_out.reshape(sp_size, capacity, model_width), SP)
+    expert_out = project_down(
+        capacity,
+        parts,
+        mine,
+        rest,
+        down,
+    )
+    returned = spread(expert_out.reshape(sp_size, PARTS * capacity, -1), SP)
     return call(
         lambda *refs: combine_kernel(capacity, *refs),
         jax.ShapeDtypeStruct((quarter_rows, model_width), bf16),
-        returned.reshape(window_rows, model_width),
+        returned.reshape(expert_out.shape),
         residual,
         own,
         own_rows,
@@ -411,5 +540,5 @@
         P(SP, TP, None),
     )
     return jax.shard_map(
-        per_device, mesh=torus, in_specs=placed, out_specs=P(SP_TP, None), check_vma=False
-    )
+        layer, mesh=torus, in_specs=placed, out_specs=P(SP_TP, None), check_vma=False
+    )

time: 301 us -> 265 us (0.88)
  waiting for transfers between devices: 142 us -> 124 us
  local copies, waits for them, and re-layouts: 35.2 us -> 18.1 us
  Pallas kernels: 8.57 us -> 24.1 us
  matrix products: 14.4 us -> 1.52 us
  starting transfers between devices: 45.9 us -> 51.2 us
  other arithmetic: 5.26 us -> 0.08 us
  blocking collectives: 35.4 us -> 31.6 us
    ppermute x3 -> x4, waiting for transfers between devices: 39.7 us -> 23.3 us  [the longest x1 17.2 us: layer(): gate_weight_too = lax.ppermute(gate_weight, TP, WEIGHT_PAIRS)]
    pallas_call x7 -> x10, Pallas kernels: 8.57 us -> 24.1 us  [the longest x9 20 us: call(): pl.pallas_call(kernel, out_shape=out_shape, in_specs=[spaces[kind] for _,...]
    reshape x8 -> x2, local copies, waits for them, and re-layouts: 14.4 us -> 0.01 us  [the longest x1 0.01 us: layer(): head_norm_gain.reshape(1, -1)]
    dot_general x4 -> x1, matrix products: 14.4 us -> 1.52 us  [layer(): jnp.einsum('ptc,pcd->td', hidden, output_weight.reshape(tp_size, width, -...]
    unnamed x47 -> x49, local copies, waits for them, and re-layouts: 7.83 us -> 17.8 us
    all_gather x1 -> x0, local copies, waits for them, and re-layouts: 8.76 us -> none  [per_device(): paired = lax.all_gather(both, 'tp_1')]
    all_to_all x6, starting transfers between devices: 43.1 us -> 47.1 us  [spread(): return lax.all_to_all(value, axes, split_axis=0, concat_axis=0, tiled=True)]
    another operation x1, other arithmetic: 3.95 us -> 0.08 us  [layer(): parts = jnp.stack([place, place ^ 1, 3 - place, 3 - place ^ 1])]
  transfers between devices with their start and end apart: 11 -> 12, of which waited for: 9 -> 8; matrix products, arithmetic and copies ran while one was open for 10% -> 1% of each run, Pallas kernels for 2% -> 5%
where the time goes in v2:
time: 265 us; the launch traced here: 264 us
  waiting for transfers between devices  124 us (47%)
  starting transfers between devices  51.2 us (19%)
  blocking collectives  31.6 us (12%)
  Pallas kernels  24.1 us (9%)
  local copies, waits for them, and re-layouts  18.1 us (7%)
  between operations  13.6 us (5%)
    all_to_all x6, waiting for transfers between devices, spread(): return lax.all_to_all(value, axes, split_axis=0, concat_axis=0, tiled=True)  98.8 us
    all_to_all x6, starting transfers between devices, spread(): return lax.all_to_all(value, axes, split_axis=0, concat_axis=0, tiled=True)  47.1 us
    all_to_all x2, blocking collectives, spread(): return lax.all_to_all(value, axes, split_axis=0, concat_axis=0, tiled=True)  31.6 us
    pallas_call x9, Pallas kernels, call(): pl.pallas_call(kernel, out_shape=out_shape, in_specs=[spaces[kind] for _,...  20 us
    unnamed x49, local copies, waits for them, and re-layouts  17.8 us
    ppermute x1, waiting for transfers between devices, layer(): gate_weight_too = lax.ppermute(gate_weight, TP, WEIGHT_PAIRS)  17.2 us
    ppermute x1, waiting for transfers between devices, layer(): rest = lax.ppermute(theirs, TP, ROW_PAIRS)  6.14 us
  transfers between devices with their start and end apart: 12, of which 8 were waited for; matrix products, arithmetic and copies ran while one was open for 1% of the time, Pallas kernels for 5%

profile of v2, /device:TPU:1, one launch (start us, length us, event | category | flops | bytes accessed | tf_op | source)
XLA Modules:
  0.0 263.7 jit_solution(3174370701784756867)
XLA Ops:
  6.6 0.7 all-gather.3.cloned.1.call-update
  7.3 0.7 all-gather.5.cloned.1.call-update
  8.1 1.4 shard_map.146
  9.5 11.0 %all_to_all.40.refs_0_ = bf16[8,64,128]{2,1,0:T(8,128)(2,1)S(1)} all-to-all(bf16[8,64,128]{2,1,0:T(8,128)(2,1)S(1)} %shard_map.146), channel_id=1, replica_groups=mesh['sp_0'=8,'sp_1'=4,'sp_2'=2,'tp_0'=2,'tp_1'=2] {'sp_1','sp_2'}, dimensions={0} | all-to-all | bytes 262144 | tf_op jit(solution)/shard_map/all_to_all | solution.py:368
  20.5 0.7 shard_map.147
  21.2 8.2 %all-to-all-start.1 = ((bf16[8,64,128]{2,1,0:T(8,128)(2,1)}), bf16[8,64,128]{2,1,0:T(8,128)(2,1)S(1)}, u32[]{:S(2)}, u32[]{:S(2)}) async-start(bf16[8,64,128]{2,1,0:T(8,128)(2,1)} %get-tuple-element.19), calls=%async_computation.1 | async-start | bytes 262144 | tf_op jit(solution)/shard_map/all_to_all | solution.py:368
  29.4 7.9 %all-to-all-done.1.refs_1_ = bf16[8,64,128]{2,1,0:T(8,128)(2,1)S(1)} async-done(((bf16[8,64,128]{2,1,0:T(8,128)(2,1)}), bf16[8,64,128]{2,1,0:T(8,128)(2,1)S(1)}, u32[]{:S(2)}, u32[]{:S(2)}) %all-to-all-start.1) | async-done | bytes 131104 | tf_op jit(solution)/shard_map/all_to_all | solution.py:368
  37.3 0.7 shard_map.148
  38.0 6.2 %all-to-all-start.2 = ((bf16[8,48,128]{2,1,0:T(8,128)(2,1)}), bf16[8,48,128]{2,1,0:T(8,128)(2,1)}, u32[]{:S(2)}, u32[]{:S(2)}) async-start(bf16[8,48,128]{2,1,0:T(8,128)(2,1)} %shard_map.148), calls=%async_computation.2 | async-start | bytes 196608 | tf_op jit(solution)/shard_map/all_to_all | solution.py:368
  44.2 0.9 copy-done.16
  45.1 2.9 %shard_map.145.local_ref = f32[2,256,384]{2,1,0:T(8,128)S(1)} custom-call(bf16[256,384]{1,0:T(8,128)(2,1)S(1)} %copy-done.16, bf16[256,384]{1,0:T(8,128)(2,1)S(1)} %copy-done.12, bf16[256,384]{1,0:T(8,128)(2,1)S(1)} %copy-done.13, f32[1,384]{1,0:T(1,128)S(1)} %reshape.36.floor_ref, f32[3,256]{1,0:T(4,128)S(1)} %copy-done.18), custom_call_target="tpu_custom_call" | custom-call | tf_op jit(solution)/shard_map/pallas_call | solution.py:49
  48.1 1.2 all-to-all-done.2.carry_ref
  49.3 0.9 copy-done.17
  50.2 1.3 shard_map.149
  51.5 20.6 %all_to_all.41 = bf16[4,256,384]{2,1,0:T(8,128)(2,1)S(1)} all-to-all(bf16[4,256,384]{2,1,0:T(8,128)(2,1)S(1)} %shard_map.149), channel_id=1, replica_groups=mesh['sp_0'=8,'sp_1'=4,'sp_2'=2,'tp_0'=2,'tp_1'=2] {'tp_0','tp_1'}, dimensions={0} | all-to-all | bytes 1572864 | tf_op jit(solution)/shard_map/all_to_all | solution.py:368
  72.2 1.5 fusion
  73.7 3.5 %all-to-all-start.4 = ((bf16[4,64,768]{2,1,0:T(8,128)(2,1)}), bf16[4,64,768]{2,1,0:T(8,128)(2,1)S(1)}, u32[]{:S(2)}, u32[]{:S(2)}) async-start(bf16[4,64,768]{2,1,0:T(8,128)(2,1)} %bitcast.8), calls=%async_computation.4 | async-start | bytes 786432 | tf_op jit(solution)/shard_map/all_to_all | solution.py:368
  77.2 0.1 copy.19.refs_3_.refs_2_
  77.4 6.4 %all-to-all-done.4.refs_0_ = bf16[4,64,768]{2,1,0:T(8,128)(2,1)S(1)} async-done(((bf16[4,64,768]{2,1,0:T(8,128)(2,1)}), bf16[4,64,768]{2,1,0:T(8,128)(2,1)S(1)}, u32[]{:S(2)}, u32[]{:S(2)}) %all-to-all-start.4) | async-done | bytes 393248 | tf_op jit(solution)/shard_map/all_to_all | solution.py:368
  83.8 1.2 shard_map.150
  85.1 1.0 copy-done.9
  86.1 0.9 copy-done.10
  87.0 0.8 copy-done.14
  87.8 10.3 %all-to-all-start.6 = ((bf16[64,8,1024]{2,1,0:T(8,128)(2,1)}), bf16[64,8,1024]{2,1,0:T(8,128)(2,1)S(1)}, u32[]{:S(2)}, u32[]{:S(2)}) async-start(bf16[64,8,1024]{2,1,0:T(8,128)(2,1)} %bitcast.29), calls=%async_computation.6 | async-start | bytes 2097152 | tf_op jit(solution)/shard_map/all_to_all | solution.py:368
  98.1 0.4 collective-permute-start.2
  98.5 27.8 %all-to-all-done.6 = bf16[64,8,1024]{2,1,0:T(8,128)(2,1)S(1)} async-done(((bf16[64,8,1024]{2,1,0:T(8,128)(2,1)}), bf16[64,8,1024]{2,1,0:T(8,128)(2,1)S(1)}, u32[]{:S(2)}, u32[]{:S(2)}) %all-to-all-start.6) | async-done | bytes 1048608 | tf_op jit(solution)/shard_map/all_to_all | solution.py:368
  126.3 6.5 %all-to-all-start.5 = ((bf16[64,8,512]{2,1,0:T(8,128)(2,1)}), bf16[64,8,512]{2,1,0:T(8,128)(2,1)}, u32[]{:S(2)}, u32[]{:S(2)}) async-start(bf16[64,8,512]{2,1,0:T(8,128)(2,1)} %bitcast.30), calls=%async_computation.5 | async-start | bytes 1048576 | tf_op jit(solution)/shard_map/all_to_all | solution.py:368
  132.7 1.0 collective-permute-start.1
  133.7 16.6 %all-to-all-done.5 = bf16[64,8,512]{2,1,0:T(8,128)(2,1)} async-done(((bf16[64,8,512]{2,1,0:T(8,128)(2,1)}), bf16[64,8,512]{2,1,0:T(8,128)(2,1)}, u32[]{:S(2)}, u32[]{:S(2)}) %all-to-all-start.5) | async-done | bytes 524320 | tf_op jit(solution)/shard_map/all_to_all | solution.py:368
  150.3 0.9 collective-permute-start
  151.3 17.2 %collective-permute-done.2.refs_3_ = bf16[3072,256]{1,0:T(8,128)(2,1)} collective-permute-done((bf16[3072,256]{1,0:T(8,128)(2,1)}, bf16[3072,256]{1,0:T(8,128)(2,1)}, u32[]{:S(2)}, u32[]{:S(2)}) %collective-permute-start.2) | collective-permute-done | bytes 1572896 | tf_op jit(solution)/shard_map/ppermute | solution.py:455
  168.5 1.9 copy-done.3
  170.4 1.4 copy-done.8
  171.8 5.2 %shard_map.151 = (f32[2,4,256,256]{3,2,1,0:T(8,128)S(1)}, bf16[4,1024,256]{2,1,0:T(8,128)(2,1)S(1)}) custom-call(bf16[512,1024]{1,0:T(8,128)(2,1)S(1)} %bitcast.26, bf16[512,1024]{1,0:T(8,128)(2,1)} %collective-permute-done.1.refs_1_, bf16[3072,256]{1,0:T(8,128)(2,1)S(1)} %bitcast.28, bf16[3072,256]{1,0:T(8,128)(2,1)} %collective-permute-done.2.refs_3_, ...), custom_call_target="tpu_custom_call" | custom-call | tf_op jit(solution)/shard_map/pallas_call | solution.py:49
  177.0 1.3 copy-done.4
  178.3 1.4 copy-done.6
  179.7 1.6 copy-done.5
  181.3 1.6 copy-done.7
  182.9 3.0 %shard_map.152 = (bf16[256,512]{1,0:T(8,128)(2,1)S(1)}, bf16[256,512]{1,0:T(8,128)(2,1)S(1)}) custom-call(bf16[512,512]{1,0:T(8,128)(2,1)} %bitcast.12.refs_0_, bf16[512,512]{1,0:T(8,128)(2,1)} %collective-permute-done.refs_1_, bf16[4,1024,256]{2,1,0:T(8,128)(2,1)S(1)} %copy-done.7, f32[2,4,256,256]{3,2,1,0:T(8,128)S(1)} %copy-done.5), custom_call_target="tpu_custom_call" | custom-call | tf_op jit(solution)/shard_map/pallas_call | solution.py:49
  185.9 1.8 collective-permute-start.3
  187.7 6.1 %collective-permute-done.3.refs_2_ = bf16[256,512]{1,0:T(8,128)(2,1)S(1)} collective-permute-done((bf16[256,512]{1,0:T(8,128)(2,1)S(1)}, bf16[256,512]{1,0:T(8,128)(2,1)S(1)}, u32[]{:S(2)}, u32[]{:S(2)}) %collective-permute-start.3) | collective-permute-done | bytes 262176 | tf_op jit(solution)/shard_map/ppermute | solution.py:503
  193.8 2.8 %copy-done.2 = bf16[4,256,3072]{2,1,0:T(8,128)(2,1)S(1)} copy-done((bf16[4,256,3072]{2,1,0:T(8,128)(2,1)S(1)}, bf16[4,256,3072]{2,1,0:T(8,128)(2,1)}, u32[]{:S(2)}) %copy-start.2) | copy-done | bytes 6291480
  196.6 4.0 %shard_map.153 = bf16[512,1536]{1,0:T(8,128)(2,1)S(1)} custom-call(s32[4]{0:T(128)S(1)} %pad_add_fusion.refs_5_.refs_0_, bf16[256,512]{1,0:T(8,128)(2,1)S(1)} %get-tuple-element.29.refs_1_, bf16[256,512]{1,0:T(8,128)(2,1)S(1)} %collective-permute-done.3.refs_2_, bf16[4,256,3072]{2,1,0:T(8,128)(2,1)S(1)} %copy-done.2), custom_call_target="tpu_custom_call" | custom-call | tf_op jit(solution)/shard_map/pallas_call | solution.py:339
  200.7 1.1 copy-done.1
  201.8 12.5 %all-to-all-start.7 = ((bf16[64,8,1536]{2,1,0:T(8,128)(2,1)}), bf16[64,8,1536]{2,1,0:T(8,128)(2,1)}, u32[]{:S(2)}, u32[]{:S(2)}) async-start(bf16[64,8,1536]{2,1,0:T(8,128)(2,1)} %bitcast.24), calls=%async_computation.7 | async-start | bytes 3145728 | tf_op jit(solution)/shard_map/all_to_all | solution.py:368
  214.3 0.1 copy.21.refs_4_
  214.4 38.9 %all-to-all-done.7 = bf16[64,8,1536]{2,1,0:T(8,128)(2,1)} async-done(((bf16[64,8,1536]{2,1,0:T(8,128)(2,1)}), bf16[64,8,1536]{2,1,0:T(8,128)(2,1)}, u32[]{:S(2)}, u32[]{:S(2)}) %all-to-all-start.7) | async-done | bytes 1572896 | tf_op jit(solution)/shard_map/all_to_all | solution.py:368
  253.3 3.6 %shard_map.154 = bf16[64,3072]{1,0:T(8,128)(2,1)} custom-call(bf16[512,1536]{1,0:T(8,128)(2,1)} %bitcast.16.refs_0_, f32[64,3072]{1,0:T(8,128)S(1)} %copy-done.11, s32[64,2]{1,0:T(8,128)S(1)} %copy.19.refs_3_.refs_2_, s32[2,64]{1,0:T(2,128)S(1)} %fusion.3.refs_4_.refs_3_, f32[64,2]{1,0:T(8,128)S(1)} %copy.21.refs_4_), custom_call_target="tpu_custom_call" | custom-call | tf_op jit(solution)/shard_map/pallas_call | solution.py:49
  (46 shorter events, 0.4 us)
Async XLA Ops:
  6.5 65.6 %copy-start = (bf16[1536,768]{1,0:T(8,128)(2,1)S(1)}, bf16[1536,768]{1,0:T(8,128)(2,1)}, u32[]{:S(2)}) copy-start(bf16[1536,768]{1,0:T(8,128)(2,1)} %param.22) | copy-start | bytes 7077892
  6.5 1.5 copy-start.20
  6.5 1.5 copy-start.12
  6.5 1.5 copy-start.13
  6.5 1.5 copy-start.18
  6.5 161.9 %all-gather.3.cloned.1.call-start = ((), (), s32[]{:S(2)}) async-start(), calls=%async_computation.8 | async-start | bytes 4718592 | tf_op jit(solution)/shard_map/all_gather | solution.py:400
  7.3 40.8 %copy-start.21 = (f32[384]{0:T(512)S(1)}, f32[384]{0:T(512)}, u32[]{:S(2)}) copy-start(f32[384]{0:T(512)} %param.21) | copy-start | bytes 4612
  7.3 172.4 %all-gather.5.cloned.1.call-start = ((), (), s32[]{:S(2)}) async-start(), calls=%async_computation.9 | async-start | bytes 7864320 | tf_op jit(solution)/shard_map/all_gather | solution.py:398
  21.2 16.0 %all-to-all-start.1 = ((bf16[8,64,128]{2,1,0:T(8,128)(2,1)}), bf16[8,64,128]{2,1,0:T(8,128)(2,1)S(1)}, u32[]{:S(2)}, u32[]{:S(2)}) async-start(bf16[8,64,128]{2,1,0:T(8,128)(2,1)} %get-tuple-element.19), calls=%async_computation.1 | async-start | bytes 262144 | tf_op jit(solution)/shard_map/all_to_all | solution.py:368
  38.0 11.3 %all-to-all-start.2 = ((bf16[8,48,128]{2,1,0:T(8,128)(2,1)}), bf16[8,48,128]{2,1,0:T(8,128)(2,1)}, u32[]{:S(2)}, u32[]{:S(2)}) async-start(bf16[8,48,128]{2,1,0:T(8,128)(2,1)} %shard_map.148), calls=%async_computation.2 | async-start | bytes 196608 | tf_op jit(solution)/shard_map/all_to_all | solution.py:368
  44.2 0.9 copy-start.16
  49.3 0.9 copy-start.17
  72.2 5.0 %copy-start.22 = (s32[256,2]{0,1:T(2,128)S(1)}, s32[256,2]{0,1:T(2,128)}, u32[]{:S(2)}) copy-start(s32[256,2]{0,1:T(2,128)} %param.25) | copy-start | bytes 6148
  72.2 11.7 %copy-start.15 = (bf16[64,3072]{1,0:T(8,128)(2,1)S(1)}, bf16[64,3072]{1,0:T(8,128)(2,1)}, u32[]{:S(2)}) copy-start(bf16[64,3072]{1,0:T(8,128)(2,1)} %refs_1_.1) | copy-start | bytes 1179652
  72.2 11.7 %copy-start.19 = (f32[3072]{0:T(1024)S(1)}, f32[3072]{0:T(1024)}, u32[]{:S(2)}) copy-start(f32[3072]{0:T(1024)} %param.24) | copy-start | bytes 36868
  73.7 10.1 %all-to-all-start.4 = ((bf16[4,64,768]{2,1,0:T(8,128)(2,1)}), bf16[4,64,768]{2,1,0:T(8,128)(2,1)S(1)}, u32[]{:S(2)}, u32[]{:S(2)}) async-start(bf16[4,64,768]{2,1,0:T(8,128)(2,1)} %bitcast.8), calls=%async_computation.4 | async-start | bytes 786432 | tf_op jit(solution)/shard_map/all_to_all | solution.py:368
  85.1 1.0 copy-start.9
  86.1 0.9 copy-start.10
  87.0 0.8 copy-start.14
  87.8 38.5 %all-to-all-start.6 = ((bf16[64,8,1024]{2,1,0:T(8,128)(2,1)}), bf16[64,8,1024]{2,1,0:T(8,128)(2,1)S(1)}, u32[]{:S(2)}, u32[]{:S(2)}) async-start(bf16[64,8,1024]{2,1,0:T(8,128)(2,1)} %bitcast.29), calls=%async_computation.6 | async-start | bytes 2097152 | tf_op jit(solution)/shard_map/all_to_all | solution.py:368
  98.1 70.4 %collective-permute-start.2 = (bf16[3072,256]{1,0:T(8,128)(2,1)}, bf16[3072,256]{1,0:T(8,128)(2,1)}, u32[]{:S(2)}, u32[]{:S(2)}) collective-permute-start(bf16[3072,256]{1,0:T(8,128)(2,1)} %bitcast.27), channel_id=1, source_target_pairs={{0,1},{1,0},{2,3},{3,2},{4,5},{5,4},{6,7},{7,6},{8,9},{9,8},{10,11... | collective-permute-start | bytes 4718600 | tf_op jit(solution)/shard_map/ppermute | solution.py:455
  126.3 24.1 %all-to-all-start.5 = ((bf16[64,8,512]{2,1,0:T(8,128)(2,1)}), bf16[64,8,512]{2,1,0:T(8,128)(2,1)}, u32[]{:S(2)}, u32[]{:S(2)}) async-start(bf16[64,8,512]{2,1,0:T(8,128)(2,1)} %bitcast.30), calls=%async_computation.5 | async-start | bytes 1048576 | tf_op jit(solution)/shard_map/all_to_all | solution.py:368
  132.7 35.8 %collective-permute-start.1 = (bf16[512,1024]{1,0:T(8,128)(2,1)S(1)}, bf16[512,1024]{1,0:T(8,128)(2,1)}, u32[]{:S(2)}, u32[]{:S(2)}) collective-permute-start(bf16[512,1024]{1,0:T(8,128)(2,1)S(1)} %bitcast.25), channel_id=1, source_target_pairs={{1,2},{2,1},{3,0},{0,3},{5,6},{6,5},{7,4},{4,7},{9,10},{10,9},{11,... | collective-permute-start | bytes 3145736 | tf_op jit(solution)/shard_map/ppermute | solution.py:477
  150.3 29.4 %collective-permute-start = (bf16[512,512]{1,0:T(8,128)(2,1)}, bf16[512,512]{1,0:T(8,128)(2,1)}, u32[]{:S(2)}, u32[]{:S(2)}) collective-permute-start(bf16[512,512]{1,0:T(8,128)(2,1)} %bitcast.12.refs_0_), channel_id=1, source_target_pairs={{1,2},{2,1},{3,0},{0,3},{5,6},{6,5},{7,4},{4,7},{9,10},{10,9},{11,... | collective-permute-start | bytes 1572872 | tf_op jit(solution)/shard_map/ppermute | solution.py:477
  168.5 1.9 copy-start.3
  170.4 1.4 copy-start.8
  177.0 1.3 copy-start.4
  178.3 1.4 copy-start.6
  179.7 1.6 copy-start.5
  181.3 1.6 copy-start.7
  185.9 7.9 %collective-permute-start.3 = (bf16[256,512]{1,0:T(8,128)(2,1)S(1)}, bf16[256,512]{1,0:T(8,128)(2,1)S(1)}, u32[]{:S(2)}, u32[]{:S(2)}) collective-permute-start(bf16[256,512]{1,0:T(8,128)(2,1)S(1)} %get-tuple-element.30), channel_id=1, source_target_pairs={{1,2},{2,1},{3,0},{0,3},{5,6},{6,5},{7,4},{4,7},{9,10},{10,9},{11,... | collective-permute-start | bytes 786440 | tf_op jit(solution)/shard_map/ppermute | solution.py:503
  193.8 2.8 %copy-start.2 = (bf16[4,256,3072]{2,1,0:T(8,128)(2,1)S(1)}, bf16[4,256,3072]{2,1,0:T(8,128)(2,1)}, u32[]{:S(2)}) copy-start(bf16[4,256,3072]{2,1,0:T(8,128)(2,1)} %all-gather.5.cloned.1.call-done.refs_3_) | copy-start | bytes 18874372
  200.7 1.2 copy-start.1
  201.8 12.5 %copy-start.23 = (f32[64,2]{0,1:T(2,128)S(1)}, f32[64,2]{0,1:T(2,128)}, u32[]{:S(2)}) copy-start(f32[64,2]{0,1:T(2,128)} %param.26) | copy-start | bytes 1540
  201.8 51.5 %copy-start.11 = (f32[64,3072]{1,0:T(8,128)S(1)}, f32[64,3072]{1,0:T(8,128)}, u32[]{:S(2)}) copy-start(f32[64,3072]{1,0:T(8,128)} %copy-done.10) | copy-start | bytes 2359300
  201.8 51.5 %all-to-all-start.7 = ((bf16[64,8,1536]{2,1,0:T(8,128)(2,1)}), bf16[64,8,1536]{2,1,0:T(8,128)(2,1)}, u32[]{:S(2)}, u32[]{:S(2)}) async-start(bf16[64,8,1536]{2,1,0:T(8,128)(2,1)} %bitcast.24), calls=%async_computation.7 | async-start | bytes 3145728 | tf_op jit(solution)/shard_map/all_to_all | solution.py:368
Sparse Core Ops, SparseCore 0:
  9.2 57.3 all-gather.2
  68.4 107.1 all-gather.4

commit v3 on v2

--- a/solution.py
+++ b/solution.py
@@ -19,6 +19,7 @@
 ROW_PAIRS = ((1, 2), (2, 1), (3, 0), (0, 3))
 WEIGHT_PAIRS = ((0, 1), (1, 0), (2, 3), (3, 2))
 FIRST_SHARE = (2, 3)
+
 
 f32 = jnp.float32
 bf16 = jnp.bfloat16
@@ -291,10 +292,9 @@
 
 
 def first_kernel(
-    capacity, own_ref, others_ref, gate_ref, gate_too_ref, up_pair_ref, parts_ref, acts_ref, kept_ref
+    capacity, own_ref, others_ref, gate_ref, up_ref, gate_too_ref, up_too_ref, acts_ref, kept_ref
 ):
-    place = parts_ref[0] % 2
-    weight_refs = (gate_ref, up_pair_ref.at[place], gate_too_ref, up_pair_ref.at[1 - place])
+    weight_refs = (gate_ref, up_ref, gate_too_ref, up_too_ref)
     for i, j, product in gate_up(own_ref, others_ref, weight_refs, capacity):
         acts_ref[i, j] = product
     left = kept_ref.shape[1]
@@ -316,34 +316,35 @@
             outs[i][:, lanes] = (gates[i] * product).astype(bf16)
 
 
-def down_kernel(capacity, parts_ref, mine_ref, rest_ref, weights_ref, out_ref):
-    width = weights_ref.shape[1]
+def down_kernel(capacity, mine_ref, rest_ref, *refs):
+    *weight_refs, out_ref = refs
+    width = weight_refs[0].shape[0]
     inner = [ref[:, k * width : (k + 1) * width] for ref in (mine_ref, rest_ref) for k in range(2)]
     rows = mine_ref.shape[0]
     block = out_ref.shape[1]
-    part = weights_ref.shape[2] // PARTS
+    part = weight_refs[0].shape[1] // PARTS
     out = jnp.zeros(out_ref.shape, f32)
     for q in range(PARTS):
         lanes = pl.ds(pl.multiple_of(q * part + pl.program_id(0) * block, LANES), block)
-        product = dot(inner[0], weights_ref[parts_ref[0], :, lanes])
+        product = dot(inner[0], weight_refs[0][:, lanes])
         for k in range(1, len(inner)):
-            product = product + dot(inner[k], weights_ref[parts_ref[k], :, lanes])
+            product = product + dot(inner[k], weight_refs[k][:, lanes])
         out = out + dot(spread_table(PARTS * rows, rows, capacity, q), product.astype(bf16))
     out_ref[...] = out.astype(bf16)
 
 
-def project_down(capacity, parts, mine, rest, weights):
+def project_down(capacity, mine, rest, weights):
     rows = mine.shape[0]
-    part = weights.shape[2] // PARTS
+    part = weights[0].shape[1] // PARTS
     whole = pl.BlockSpec(memory_space=pltpu.VMEM)
     return pl.pallas_call(
         lambda *refs: down_kernel(capacity, *refs),
         grid=(part // DOWN_LANES,),
         out_shape=jax.ShapeDtypeStruct((PARTS * rows, part), bf16),
-        in_specs=[pl.BlockSpec(memory_space=pltpu.SMEM), whole, whole, whole],
+        in_specs=[whole, whole] + [whole for _ in weights],
         out_specs=pl.BlockSpec((PARTS * rows, DOWN_LANES), lambda k: (0, k)),
         compiler_params=pltpu.CompilerParams(vmem_limit_bytes=12 * 1024 * 1024),
-    )(parts, mine, rest, weights)
+    )(mine, rest, *weights)
 
 
 def combine_kernel(capacity, results_ref, residual_ref, column_ref, row_ref, weight_ref, out_ref):
@@ -395,9 +396,9 @@
     capacity = window_rows // sp_size
     piece = LANES // plane
 
-    down = lax.all_gather(expert_down_weight[0], TP)
-
-    up_pair = lax.all_gather(expert_up_weight[0], "tp_1")
+    down = expert_down_weight[0]
+    down_near = lax.ppermute(down, TP, WEIGHT_PAIRS)
+    down_next = lax.ppermute(down, TP, ROW_PAIRS)
 
     floor = forget_minimum.reshape(1, -1)
     message = jax.ShapeDtypeStruct((plane, heads * piece + 16, LANES), bf16)
@@ -450,9 +451,13 @@
         output_weight.reshape(tp_size, width, -1),
         preferred_element_type=f32,
     ).astype(bf16)
+    gate_weight, up_weight, down_near, projected = lax.optimization_barrier(
+        (expert_gate_weight[0], expert_up_weight[0], down_near, projected)
+    )
     mix = spread(projected.reshape(tp_size, quarter_rows, -1), TP)
-    gate_weight, mix = lax.optimization_barrier((expert_gate_weight[0], mix))
+    down_far = lax.ppermute(down_near, TP, ROW_PAIRS)
     gate_weight_too = lax.ppermute(gate_weight, TP, WEIGHT_PAIRS)
+    up_weight_too = lax.ppermute(up_weight, TP, WEIGHT_PAIRS)
 
     own = lax.dynamic_slice_in_dim(routes, lax.axis_index(TP) * quarter_rows, quarter_rows, 0)
     own_rows = own.T
@@ -475,9 +480,8 @@
     for send in sends:
         received = spread(send.reshape(sp_size, PARTS * capacity, -1), SP).reshape(send.shape)
         rows.append((received, lax.ppermute(received, TP, ROW_PAIRS)))
-    count = 4
-    place = lax.axis_index(TP).astype(jnp.int32)
-    parts = jnp.stack([place, place ^ 1, 3 - place, (3 - place) ^ 1])
+    weights = (gate_weight, up_weight, gate_weight_too, up_weight_too)
+    count = len(weights)
     acts, kept = call(
         lambda *refs: first_kernel(capacity, *refs),
         (
@@ -485,14 +489,12 @@
             jax.ShapeDtypeStruct((count, model_width - first_depth, hidden_part), bf16),
         ),
         *rows[0],
-        gate_weight,
-        gate_weight_too,
-        up_pair,
-        parts,
-        kinds="vvvvvs",
+        *weights,
         mib=16,
     )
-    acts, down = lax.optimization_barrier((acts, down))
+    acts, down_near, down_next, down_far = lax.optimization_barrier(
+        (acts, down_near, down_next, down_far)
+    )
     mine, theirs = call(
         lambda *refs: second_kernel(capacity, *refs),
         (jax.ShapeDtypeStruct((window_rows, 2 * hidden_part), bf16),) * 2,
@@ -502,11 +504,7 @@
     )
     rest = lax.ppermute(theirs, TP, ROW_PAIRS)
     expert_out = project_down(
-        capacity,
-        parts,
-        mine,
-        rest,
-        down,
+        capacity, mine, rest, (down, down_near, down_next, down_far)
     )
     returned = spread(expert_out.reshape(sp_size, PARTS * capacity, -1), SP)
     return call(

time: 265 us -> 265 us (level)
  waiting for transfers between devices: 124 us -> 144 us
  between operations: 13.6 us -> 0.2 us
  blocking collectives: 31.6 us -> 25.3 us
  local copies, waits for them, and re-layouts: 18.1 us -> 12.2 us
  starting transfers between devices: 51.2 us -> 54 us
    ppermute x2, waiting for transfers between devices: 0.01 us -> 27.1 us  [layer(): rows.append((received, lax.ppermute(received, TP, ROW_PAIRS)))]
    ppermute x1, waiting for transfers between devices: 17.2 us -> 0.01 us  [layer(): gate_weight_too = lax.ppermute(gate_weight, TP, WEIGHT_PAIRS)]
    ppermute x0 -> x4, waiting for transfers between devices: none -> 16.2 us  [the longest x1 16.2 us: layer(): up_weight_too = lax.ppermute(up_weight, TP, WEIGHT_PAIRS)]
    unnamed x49 -> x45, local copies, waits for them, and re-layouts: 17.8 us -> 11.3 us
    all_to_all x2, blocking collectives: 31.6 us -> 25.3 us  [spread(): return lax.all_to_all(value, axes, split_axis=0, concat_axis=0, tiled=True)]
    ppermute x0 -> x4, starting transfers between devices: none -> 5.89 us  [the longest x1 2.03 us: layer(): down_near = lax.ppermute(down, TP, WEIGHT_PAIRS)]
    all_to_all x6, waiting for transfers between devices: 98.8 us -> 94.6 us  [spread(): return lax.all_to_all(value, axes, split_axis=0, concat_axis=0, tiled=True)]
  transfers between devices with their start and end apart: 12 -> 14, of which waited for: 8 -> 10; matrix products, arithmetic and copies ran while one was open for 1% -> 1% of each run, Pallas kernels for 5% -> 5%
where the time goes in v3:
time: 265 us; the launch traced here: 264 us
  waiting for transfers between devices  144 us (54%)
  starting transfers between devices  54 us (20%)
  Pallas kernels  26.4 us (10%)
  blocking collectives  25.3 us (10%)
  local copies, waits for them, and re-layouts  12.2 us (5%)
    all_to_all x6, waiting for transfers between devices, spread(): return lax.all_to_all(value, axes, split_axis=0, concat_axis=0, tiled=True)  94.6 us
    all_to_all x6, starting transfers between devices, spread(): return lax.all_to_all(value, axes, split_axis=0, concat_axis=0, tiled=True)  44.9 us
    ppermute x2, waiting for transfers between devices, layer(): rows.append((received, lax.ppermute(received, TP, ROW_PAIRS)))  27.1 us
    all_to_all x2, blocking collectives, spread(): return lax.all_to_all(value, axes, split_axis=0, concat_axis=0, tiled=True)  25.3 us
    pallas_call x9, Pallas kernels, call(): pl.pallas_call(kernel, out_shape=out_shape, in_specs=[spaces[kind] for _,...  20.5 us
    ppermute x1, waiting for transfers between devices, layer(): up_weight_too = lax.ppermute(up_weight, TP, WEIGHT_PAIRS)  16.2 us
    unnamed x45, local copies, waits for them, and re-layouts  11.3 us
    ppermute x1, waiting for transfers between devices, layer(): rest = lax.ppermute(theirs, TP, ROW_PAIRS)  6.19 us
  transfers between devices with their start and end apart: 14, of which 10 were waited for; matrix products, arithmetic and copies ran while one was open for 1% of the time, Pallas kernels for 5%

profile of v3, /device:TPU:1, one launch (start us, length us, event | category | flops | bytes accessed | tf_op | source)
XLA Modules:
  0.0 263.7 jit_solution(12840456926258035379)
XLA Ops:
  0.0 2.0 collective-permute-start
  2.0 0.7 reshape.36.floor_ref
  2.7 0.9 copy-done.8
  3.6 0.9 copy-done.10
  4.6 0.7 copy-done.16
  5.3 1.4 shard_map.146
  6.7 10.5 %all_to_all.40.refs_0_ = bf16[8,64,128]{2,1,0:T(8,128)(2,1)S(1)} all-to-all(bf16[8,64,128]{2,1,0:T(8,128)(2,1)S(1)} %shard_map.146), channel_id=1, replica_groups=mesh['sp_0'=8,'sp_1'=4,'sp_2'=2,'tp_0'=2,'tp_1'=2] {'sp_1','sp_2'}, dimensions={0} | all-to-all | bytes 262144 | tf_op jit(solution)/shard_map/all_to_all | solution.py:369
  17.2 0.7 shard_map.147
  17.9 8.2 %all-to-all-start.1 = ((bf16[8,64,128]{2,1,0:T(8,128)(2,1)}), bf16[8,64,128]{2,1,0:T(8,128)(2,1)S(1)}, u32[]{:S(2)}, u32[]{:S(2)}) async-start(bf16[8,64,128]{2,1,0:T(8,128)(2,1)} %get-tuple-element.23), calls=%async_computation.1 | async-start | bytes 262144 | tf_op jit(solution)/shard_map/all_to_all | solution.py:369
  26.0 7.9 %all-to-all-done.1.refs_1_ = bf16[8,64,128]{2,1,0:T(8,128)(2,1)S(1)} async-done(((bf16[8,64,128]{2,1,0:T(8,128)(2,1)}), bf16[8,64,128]{2,1,0:T(8,128)(2,1)S(1)}, u32[]{:S(2)}, u32[]{:S(2)}) %all-to-all-start.1) | async-done | bytes 131104 | tf_op jit(solution)/shard_map/all_to_all | solution.py:369
  33.9 0.7 shard_map.148
  34.6 6.2 %all-to-all-start.2 = ((bf16[8,48,128]{2,1,0:T(8,128)(2,1)}), bf16[8,48,128]{2,1,0:T(8,128)(2,1)}, u32[]{:S(2)}, u32[]{:S(2)}) async-start(bf16[8,48,128]{2,1,0:T(8,128)(2,1)} %shard_map.148), calls=%async_computation.2 | async-start | bytes 196608 | tf_op jit(solution)/shard_map/all_to_all | solution.py:369
  40.9 0.9 copy-done.14
  41.8 2.9 %shard_map.145.local_ref = f32[2,256,384]{2,1,0:T(8,128)S(1)} custom-call(bf16[256,384]{1,0:T(8,128)(2,1)S(1)} %copy-done.14, bf16[256,384]{1,0:T(8,128)(2,1)S(1)} %copy-done.9, bf16[256,384]{1,0:T(8,128)(2,1)S(1)} %copy-done.11, f32[1,384]{1,0:T(1,128)S(1)} %reshape.36.floor_ref, f32[3,256]{1,0:T(4,128)S(1)} %copy-done.17), custom_call_target="tpu_custom_call" | custom-call | tf_op jit(solution)/shard_map/pallas_call | solution.py:50
  44.7 1.2 all-to-all-done.2.carry_ref
  46.0 0.9 copy-done.15
  46.9 1.3 shard_map.149
  48.1 14.8 %all_to_all.41 = bf16[4,256,384]{2,1,0:T(8,128)(2,1)S(1)} all-to-all(bf16[4,256,384]{2,1,0:T(8,128)(2,1)S(1)} %shard_map.149), channel_id=1, replica_groups=mesh['sp_0'=8,'sp_1'=4,'sp_2'=2,'tp_0'=2,'tp_1'=2] {'tp_0','tp_1'}, dimensions={0} | all-to-all | bytes 1572864 | tf_op jit(solution)/shard_map/all_to_all | solution.py:369
  63.0 1.5 fusion
  64.5 3.5 %all-to-all-start.4 = ((bf16[4,64,768]{2,1,0:T(8,128)(2,1)}), bf16[4,64,768]{2,1,0:T(8,128)(2,1)S(1)}, u32[]{:S(2)}, u32[]{:S(2)}) async-start(bf16[4,64,768]{2,1,0:T(8,128)(2,1)} %bitcast.6), calls=%async_computation.4 | async-start | bytes 786432 | tf_op jit(solution)/shard_map/all_to_all | solution.py:369
  68.2 5.9 %all-to-all-done.4.refs_0_ = bf16[4,64,768]{2,1,0:T(8,128)(2,1)S(1)} async-done(((bf16[4,64,768]{2,1,0:T(8,128)(2,1)}), bf16[4,64,768]{2,1,0:T(8,128)(2,1)S(1)}, u32[]{:S(2)}, u32[]{:S(2)}) %all-to-all-start.4) | async-done | bytes 393248 | tf_op jit(solution)/shard_map/all_to_all | solution.py:369
  74.2 1.2 shard_map.150
  75.4 1.1 copy-done.5
  76.5 0.9 copy-done.6
  77.4 0.8 copy-done.12
  78.2 7.2 %all-to-all-start.6 = ((bf16[64,8,1024]{2,1,0:T(8,128)(2,1)}), bf16[64,8,1024]{2,1,0:T(8,128)(2,1)S(1)}, u32[]{:S(2)}, u32[]{:S(2)}) async-start(bf16[64,8,1024]{2,1,0:T(8,128)(2,1)} %bitcast.32), calls=%async_computation.6 | async-start | bytes 2097152 | tf_op jit(solution)/shard_map/all_to_all | solution.py:369
  85.8 1.2 collective-permute-start.4
  86.9 0.9 collective-permute-start.5
  87.8 1.8 collective-permute-start.6
  89.6 24.1 %all-to-all-done.6 = bf16[64,8,1024]{2,1,0:T(8,128)(2,1)S(1)} async-done(((bf16[64,8,1024]{2,1,0:T(8,128)(2,1)}), bf16[64,8,1024]{2,1,0:T(8,128)(2,1)S(1)}, u32[]{:S(2)}, u32[]{:S(2)}) %all-to-all-start.6) | async-done | bytes 1048608 | tf_op jit(solution)/shard_map/all_to_all | solution.py:369
  113.7 6.5 %all-to-all-start.5 = ((bf16[64,8,512]{2,1,0:T(8,128)(2,1)}), bf16[64,8,512]{2,1,0:T(8,128)(2,1)}, u32[]{:S(2)}, u32[]{:S(2)}) async-start(bf16[64,8,512]{2,1,0:T(8,128)(2,1)} %bitcast.33), calls=%async_computation.5 | async-start | bytes 1048576 | tf_op jit(solution)/shard_map/all_to_all | solution.py:369
  120.2 1.0 collective-permute-start.2
  121.2 16.6 %all-to-all-done.5 = bf16[64,8,512]{2,1,0:T(8,128)(2,1)} async-done(((bf16[64,8,512]{2,1,0:T(8,128)(2,1)}), bf16[64,8,512]{2,1,0:T(8,128)(2,1)}, u32[]{:S(2)}, u32[]{:S(2)}) %all-to-all-start.5) | async-done | bytes 524320 | tf_op jit(solution)/shard_map/all_to_all | solution.py:369
  137.8 0.9 collective-permute-start.1
  138.7 16.2 %collective-permute-done.4.refs_5_ = bf16[3072,256]{1,0:T(8,128)(2,1)} collective-permute-done((bf16[3072,256]{1,0:T(8,128)(2,1)}, bf16[3072,256]{1,0:T(8,128)(2,1)}, u32[]{:S(2)}, u32[]{:S(2)}) %collective-permute-start.4) | collective-permute-done | bytes 1572896 | tf_op jit(solution)/shard_map/ppermute | solution.py:460
  154.9 24.6 %collective-permute-done.2.refs_1_ = bf16[512,1024]{1,0:T(8,128)(2,1)} collective-permute-done((bf16[512,1024]{1,0:T(8,128)(2,1)S(1)}, bf16[512,1024]{1,0:T(8,128)(2,1)}, u32[]{:S(2)}, u32[]{:S(2)}) %collective-permute-start.2) | collective-permute-done | bytes 1048608 | tf_op jit(solution)/shard_map/ppermute | solution.py:482
  179.5 1.4 copy-done.2
  180.9 1.4 copy-done.3
  182.3 5.8 %shard_map.151 = (f32[2,4,256,256]{3,2,1,0:T(8,128)S(1)}, bf16[4,1024,256]{2,1,0:T(8,128)(2,1)S(1)}) custom-call(bf16[512,1024]{1,0:T(8,128)(2,1)S(1)} %bitcast.24, bf16[512,1024]{1,0:T(8,128)(2,1)} %collective-permute-done.2.refs_1_, bf16[3072,256]{1,0:T(8,128)(2,1)S(1)} %bitcast.26, bf16[3072,256]{1,0:T(8,128)(2,1)S(1)} %bitcast.28, ...), custom_call_target="tpu_custom_call" | custom-call | tf_op jit(solution)/shard_map/pallas_call | solution.py:50
  188.1 2.5 collective-permute-done.1.refs_1_
  190.6 3.0 %shard_map.152 = (bf16[256,512]{1,0:T(8,128)(2,1)S(1)}, bf16[256,512]{1,0:T(8,128)(2,1)S(1)}) custom-call(bf16[512,512]{1,0:T(8,128)(2,1)} %bitcast.10.refs_0_, bf16[512,512]{1,0:T(8,128)(2,1)S(1)} %collective-permute-done.1.refs_1_, bf16[4,1024,256]{2,1,0:T(8,128)(2,1)S(1)} %get-tuple-element.31.refs_2_, f32[2,4,256,256]{3,2,1,0:T(8,128)S(1)} %get-tuple-element.34.refs_3_), custom_call_target="tpu_custom_call" | custom-call | tf_op jit(solution)/shard_map/pallas_call | solution.py:50
  193.6 1.0 collective-permute-start.7
  194.6 6.2 %collective-permute-done.7.refs_1_ = bf16[256,512]{1,0:T(8,128)(2,1)S(1)} collective-permute-done((bf16[256,512]{1,0:T(8,128)(2,1)S(1)}, bf16[256,512]{1,0:T(8,128)(2,1)S(1)}, u32[]{:S(2)}, u32[]{:S(2)}) %collective-permute-start.7) | collective-permute-done | bytes 262176 | tf_op jit(solution)/shard_map/ppermute | solution.py:505
  200.8 5.8 %shard_map.153 = bf16[512,1536]{1,0:T(8,128)(2,1)S(1)} custom-call(bf16[256,512]{1,0:T(8,128)(2,1)S(1)} %get-tuple-element.35.refs_0_, bf16[256,512]{1,0:T(8,128)(2,1)S(1)} %collective-permute-done.7.refs_1_, bf16[256,3072]{1,0:T(8,128)(2,1)S(1)} %bitcast.31, bf16[256,3072]{1,0:T(8,128)(2,1)} %collective-permute-done.refs_3_, ...), custom_call_target="tpu_custom_call" | custom-call | tf_op jit(solution)/shard_map/pallas_call | solution.py:340
  206.6 1.2 copy-done.1
  207.7 13.3 %all-to-all-start.7 = ((bf16[64,8,1536]{2,1,0:T(8,128)(2,1)}), bf16[64,8,1536]{2,1,0:T(8,128)(2,1)}, u32[]{:S(2)}, u32[]{:S(2)}) async-start(bf16[64,8,1536]{2,1,0:T(8,128)(2,1)} %bitcast.22), calls=%async_computation.7 | async-start | bytes 3145728 | tf_op jit(solution)/shard_map/all_to_all | solution.py:369
  221.2 38.9 %all-to-all-done.7 = bf16[64,8,1536]{2,1,0:T(8,128)(2,1)} async-done(((bf16[64,8,1536]{2,1,0:T(8,128)(2,1)}), bf16[64,8,1536]{2,1,0:T(8,128)(2,1)}, u32[]{:S(2)}, u32[]{:S(2)}) %all-to-all-start.7) | async-done | bytes 1572896 | tf_op jit(solution)/shard_map/all_to_all | solution.py:369
  260.1 3.6 %shard_map.154 = bf16[64,3072]{1,0:T(8,128)(2,1)} custom-call(bf16[512,1536]{1,0:T(8,128)(2,1)} %bitcast.14.refs_0_, f32[64,3072]{1,0:T(8,128)S(1)} %copy-done.7, s32[64,2]{1,0:T(8,128)S(1)} %copy.16.refs_3_.refs_2_, s32[2,64]{1,0:T(2,128)S(1)} %fusion.3.refs_4_.refs_3_, f32[64,2]{1,0:T(8,128)S(1)} %copy.18.refs_4_), custom_call_target="tpu_custom_call" | custom-call | tf_op jit(solution)/shard_map/pallas_call | solution.py:50
  (43 shorter events, 0.8 us)
Async XLA Ops:
  0.0 62.9 %copy-start = (bf16[1536,768]{1,0:T(8,128)(2,1)S(1)}, bf16[1536,768]{1,0:T(8,128)(2,1)}, u32[]{:S(2)}) copy-start(bf16[1536,768]{1,0:T(8,128)(2,1)} %param.22) | copy-start | bytes 7077892
  0.0 40.8 %copy-start.17 = (f32[3,256]{1,0:T(4,128)S(1)}, f32[3,256]{1,0:T(4,128)}, u32[]{:S(2)}) copy-start(f32[3,256]{1,0:T(4,128)} %extra_ref.3) | copy-start | bytes 9220
  0.0 64.5 %collective-permute-start = (bf16[256,3072]{1,0:T(8,128)(2,1)}, bf16[256,3072]{1,0:T(8,128)(2,1)}, u32[]{:S(2)}, u32[]{:S(2)}) collective-permute-start(bf16[256,3072]{1,0:T(8,128)(2,1)} %bitcast.29), channel_id=1, source_target_pairs={{0,1},{1,0},{2,3},{3,2},{4,5},{5,4},{6,7},{7,6},{8,9},{9,8},{10,11... | collective-permute-start | bytes 4718600 | tf_op jit(solution)/shard_map/ppermute | solution.py:400
  2.7 0.9 copy-start.8
  3.6 0.9 copy-start.10
  4.6 0.7 copy-start.16
  5.3 35.6 %copy-start.9 = (bf16[256,384]{1,0:T(8,128)(2,1)S(1)}, bf16[256,384]{1,0:T(8,128)(2,1)}, u32[]{:S(2)}) copy-start(bf16[256,384]{1,0:T(8,128)(2,1)} %forget_ref.3) | copy-start | bytes 589828
  5.3 35.6 %copy-start.11 = (bf16[256,384]{1,0:T(8,128)(2,1)S(1)}, bf16[256,384]{1,0:T(8,128)(2,1)}, u32[]{:S(2)}) copy-start(bf16[256,384]{1,0:T(8,128)(2,1)} %value_ref.3) | copy-start | bytes 589828
  5.3 39.4 %copy-start.19 = (f32[384]{0:T(512)S(1)}, f32[384]{0:T(512)}, u32[]{:S(2)}) copy-start(f32[384]{0:T(512)} %param.21) | copy-start | bytes 4612
  17.9 16.0 %all-to-all-start.1 = ((bf16[8,64,128]{2,1,0:T(8,128)(2,1)}), bf16[8,64,128]{2,1,0:T(8,128)(2,1)S(1)}, u32[]{:S(2)}, u32[]{:S(2)}) async-start(bf16[8,64,128]{2,1,0:T(8,128)(2,1)} %get-tuple-element.23), calls=%async_computation.1 | async-start | bytes 262144 | tf_op jit(solution)/shard_map/all_to_all | solution.py:369
  34.6 11.3 %all-to-all-start.2 = ((bf16[8,48,128]{2,1,0:T(8,128)(2,1)}), bf16[8,48,128]{2,1,0:T(8,128)(2,1)}, u32[]{:S(2)}, u32[]{:S(2)}) async-start(bf16[8,48,128]{2,1,0:T(8,128)(2,1)} %shard_map.148), calls=%async_computation.2 | async-start | bytes 196608 | tf_op jit(solution)/shard_map/all_to_all | solution.py:369
  40.9 0.9 copy-start.14
  46.0 0.9 copy-start.15
  62.9 5.0 %copy-start.20 = (s32[256,2]{0,1:T(2,128)S(1)}, s32[256,2]{0,1:T(2,128)}, u32[]{:S(2)}) copy-start(s32[256,2]{0,1:T(2,128)} %param.25) | copy-start | bytes 6148
  63.0 11.2 %copy-start.13 = (bf16[64,3072]{1,0:T(8,128)(2,1)S(1)}, bf16[64,3072]{1,0:T(8,128)(2,1)}, u32[]{:S(2)}) copy-start(bf16[64,3072]{1,0:T(8,128)(2,1)} %refs_1_.1) | copy-start | bytes 1179652
  63.0 11.2 %copy-start.18 = (f32[3072]{0:T(1024)S(1)}, f32[3072]{0:T(1024)}, u32[]{:S(2)}) copy-start(f32[3072]{0:T(1024)} %param.24) | copy-start | bytes 36868
  64.5 9.7 %all-to-all-start.4 = ((bf16[4,64,768]{2,1,0:T(8,128)(2,1)}), bf16[4,64,768]{2,1,0:T(8,128)(2,1)S(1)}, u32[]{:S(2)}, u32[]{:S(2)}) async-start(bf16[4,64,768]{2,1,0:T(8,128)(2,1)} %bitcast.6), calls=%async_computation.4 | async-start | bytes 786432 | tf_op jit(solution)/shard_map/all_to_all | solution.py:369
  75.4 1.1 copy-start.5
  76.5 0.9 copy-start.6
  77.4 0.8 copy-start.12
  78.2 35.5 %all-to-all-start.6 = ((bf16[64,8,1024]{2,1,0:T(8,128)(2,1)}), bf16[64,8,1024]{2,1,0:T(8,128)(2,1)S(1)}, u32[]{:S(2)}, u32[]{:S(2)}) async-start(bf16[64,8,1024]{2,1,0:T(8,128)(2,1)} %bitcast.32), calls=%async_computation.6 | async-start | bytes 2097152 | tf_op jit(solution)/shard_map/all_to_all | solution.py:369
  85.4 52.4 %collective-permute-start.3 = (bf16[3072,256]{1,0:T(8,128)(2,1)}, bf16[3072,256]{1,0:T(8,128)(2,1)}, u32[]{:S(2)}, u32[]{:S(2)}) collective-permute-start(bf16[3072,256]{1,0:T(8,128)(2,1)} %bitcast.25), channel_id=1, source_target_pairs={{0,1},{1,0},{2,3},{3,2},{4,5},{5,4},{6,7},{7,6},{8,9},{9,8},{10,11... | collective-permute-start | bytes 4718600 | tf_op jit(solution)/shard_map/ppermute | solution.py:459
  85.8 69.1 %collective-permute-start.4 = (bf16[3072,256]{1,0:T(8,128)(2,1)}, bf16[3072,256]{1,0:T(8,128)(2,1)}, u32[]{:S(2)}, u32[]{:S(2)}) collective-permute-start(bf16[3072,256]{1,0:T(8,128)(2,1)} %bitcast.27), channel_id=1, source_target_pairs={{0,1},{1,0},{2,3},{3,2},{4,5},{5,4},{6,7},{7,6},{8,9},{9,8},{10,11... | collective-permute-start | bytes 4718600 | tf_op jit(solution)/shard_map/ppermute | solution.py:460
  86.9 101.1 %collective-permute-start.5 = (bf16[256,3072]{1,0:T(8,128)(2,1)}, bf16[256,3072]{1,0:T(8,128)(2,1)}, u32[]{:S(2)}, u32[]{:S(2)}) collective-permute-start(bf16[256,3072]{1,0:T(8,128)(2,1)} %bitcast.30), channel_id=1, source_target_pairs={{1,2},{2,1},{3,0},{0,3},{5,6},{6,5},{7,4},{4,7},{9,10},{10,9},{11,... | collective-permute-start | bytes 4718600 | tf_op jit(solution)/shard_map/ppermute | solution.py:401
  87.8 100.2 %collective-permute-start.6 = (bf16[256,3072]{1,0:T(8,128)(2,1)}, bf16[256,3072]{1,0:T(8,128)(2,1)}, u32[]{:S(2)}, u32[]{:S(2)}) collective-permute-start(bf16[256,3072]{1,0:T(8,128)(2,1)} %collective-permute-done.refs_3_), channel_id=1, source_target_pairs={{1,2},{2,1},{3,0},{0,3},{5,6},{6,5},{7,4},{4,7},{9,10},{10,9},{11,... | collective-permute-start | bytes 4718600 | tf_op jit(solution)/shard_map/ppermute | solution.py:458
  113.7 24.1 %all-to-all-start.5 = ((bf16[64,8,512]{2,1,0:T(8,128)(2,1)}), bf16[64,8,512]{2,1,0:T(8,128)(2,1)}, u32[]{:S(2)}, u32[]{:S(2)}) async-start(bf16[64,8,512]{2,1,0:T(8,128)(2,1)} %bitcast.33), calls=%async_computation.5 | async-start | bytes 1048576 | tf_op jit(solution)/shard_map/all_to_all | solution.py:369
  120.2 59.3 %collective-permute-start.2 = (bf16[512,1024]{1,0:T(8,128)(2,1)S(1)}, bf16[512,1024]{1,0:T(8,128)(2,1)}, u32[]{:S(2)}, u32[]{:S(2)}) collective-permute-start(bf16[512,1024]{1,0:T(8,128)(2,1)S(1)} %bitcast.23), channel_id=1, source_target_pairs={{1,2},{2,1},{3,0},{0,3},{5,6},{6,5},{7,4},{4,7},{9,10},{10,9},{11,... | collective-permute-start | bytes 3145736 | tf_op jit(solution)/shard_map/ppermute | solution.py:482
  137.8 52.8 %collective-permute-start.1 = (bf16[512,512]{1,0:T(8,128)(2,1)}, bf16[512,512]{1,0:T(8,128)(2,1)S(1)}, u32[]{:S(2)}, u32[]{:S(2)}) collective-permute-start(bf16[512,512]{1,0:T(8,128)(2,1)} %bitcast.10.refs_0_), channel_id=1, source_target_pairs={{1,2},{2,1},{3,0},{0,3},{5,6},{6,5},{7,4},{4,7},{9,10},{10,9},{11,... | collective-permute-start | bytes 1572872 | tf_op jit(solution)/shard_map/ppermute | solution.py:482
  179.5 1.4 copy-start.2
  180.9 1.4 copy-start.3
  190.6 10.2 %copy-start.4 = (bf16[1,256,3072]{2,1,0:T(8,128)(2,1)S(1)}, bf16[1,256,3072]{2,1,0:T(8,128)(2,1)}, u32[]{:S(2)}) copy-start(bf16[1,256,3072]{2,1,0:T(8,128)(2,1)} %param.29) | copy-start | bytes 4718596
  193.6 7.2 %collective-permute-start.7 = (bf16[256,512]{1,0:T(8,128)(2,1)S(1)}, bf16[256,512]{1,0:T(8,128)(2,1)S(1)}, u32[]{:S(2)}, u32[]{:S(2)}) collective-permute-start(bf16[256,512]{1,0:T(8,128)(2,1)S(1)} %get-tuple-element.36), channel_id=1, source_target_pairs={{1,2},{2,1},{3,0},{0,3},{5,6},{6,5},{7,4},{4,7},{9,10},{10,9},{11,... | collective-permute-start | bytes 786440 | tf_op jit(solution)/shard_map/ppermute | solution.py:505
  206.6 1.2 copy-start.1
  207.7 13.4 %copy-start.21 = (f32[64,2]{0,1:T(2,128)S(1)}, f32[64,2]{0,1:T(2,128)}, u32[]{:S(2)}) copy-start(f32[64,2]{0,1:T(2,128)} %param.26) | copy-start | bytes 1540
  207.7 52.3 %copy-start.7 = (f32[64,3072]{1,0:T(8,128)S(1)}, f32[64,3072]{1,0:T(8,128)}, u32[]{:S(2)}) copy-start(f32[64,3072]{1,0:T(8,128)} %copy-done.6) | copy-start | bytes 2359300
  207.7 52.3 %all-to-all-start.7 = ((bf16[64,8,1536]{2,1,0:T(8,128)(2,1)}), bf16[64,8,1536]{2,1,0:T(8,128)(2,1)}, u32[]{:S(2)}, u32[]{:S(2)}) async-start(bf16[64,8,1536]{2,1,0:T(8,128)(2,1)} %bitcast.22), calls=%async_computation.7 | async-start | bytes 3145728 | tf_op jit(solution)/shard_map/all_to_all | solution.py:369

commit v4 on v3

--- a/solution.py
+++ b/solution.py
@@ -18,7 +18,7 @@
 SP_TP = SP + TP
 ROW_PAIRS = ((1, 2), (2, 1), (3, 0), (0, 3))
 WEIGHT_PAIRS = ((0, 1), (1, 0), (2, 3), (3, 2))
-FIRST_SHARE = (2, 3)
+FIRST_SHARE = (3, 4)
 
 
 f32 = jnp.float32
@@ -58,7 +58,7 @@
 
 
 def decays(forget_ref, floor_ref, extra_ref, table):
-    weight = (1.0 - floor_ref[...]) * jax.nn.sigmoid(-forget_ref[...].astype(f32))
+    weight = (1.0 - floor_ref[...][None, :]) * jax.nn.sigmoid(-forget_ref[...].astype(f32))
     single = jnp.log1p(-weight)
     summed = dot(table, single, precision=exact)
     extra = extra_ref[...]
@@ -143,13 +143,16 @@
             ).astype(bf16)
 
 
-def local_kernel(query_ref, forget_ref, value_ref, floor_ref, extra_ref, out_ref):
+def local_kernel(
+    query_ref, forget_ref, value_ref, gate_ref, floor_ref, extra_ref, gain_ref, out_ref
+):
     rows, width = query_ref.shape
     at = lax.broadcasted_iota(jnp.int32, (rows, rows), 0)
     other = lax.broadcasted_iota(jnp.int32, (rows, rows), 1)
     upto = ((other <= at) & (at // SPAN == other // SPAN)).astype(f32)
     weight, summed, extra_summed = decays(forget_ref, floor_ref, extra_ref, upto)
     query = silu(query_ref[...].astype(f32))
+    out_ref[2] = gain_ref[...][None, :] * silu(gate_ref[...].astype(f32))
     causal = lax.broadcasted_iota(jnp.int32, (SPAN, SPAN), 0) >= lax.broadcasted_iota(
         jnp.int32, (SPAN, SPAN), 1
     )
@@ -178,7 +181,7 @@
             state = state * jnp.exp(final) + dot(value, kept, ((0,), (0,)))
 
 
-def head_kernel(local_ref, carry_ref, gain_ref, gate_ref, out_ref):
+def head_kernel(local_ref, carry_ref, out_ref):
     width = local_ref.shape[2]
     heads = width // LANES
     piece = carry_ref.shape[1] // heads
@@ -190,10 +193,23 @@
         late = local_ref[1, :, lanes].astype(bf16)
         mixed = local_ref[0, :, lanes] + dot(late, carried, ((1,), (1,)))
         scale = lax.rsqrt(jnp.mean(mixed * mixed, axis=-1, keepdims=True) + epsilon)
-        gate = silu(gate_ref[:, lanes].astype(f32))
-        hidden = (mixed * scale * gain_ref[:, lanes] * gate).astype(bf16)
-        for k in range(out_ref.shape[0]):
-            out_ref[k, :, lanes] = hidden
+        out_ref[:, lanes] = (mixed * scale * local_ref[2, :, lanes]).astype(bf16)
+
+
+def project_kernel(place_ref, *refs):
+    count = (len(refs) - 2) // 2
+    hidden_refs, (weight_ref, *out_refs, held_ref) = refs[:count], refs[count:]
+    width = hidden_refs[0].shape[1]
+    place = place_ref[0]
+    projected = jnp.zeros(held_ref.shape, f32)
+    for k, hidden_ref in enumerate(hidden_refs):
+        start = pl.multiple_of((place + count - k) % count * width, width)
+        projected = projected + dot(hidden_ref[...], weight_ref[pl.ds(start, width), :])
+    held_ref[...] = projected
+    for k, out_ref in enumerate(out_refs):
+        tokens = out_ref.shape[0]
+        start = pl.multiple_of((place + k) % count * tokens, tokens)
+        out_ref[...] = held_ref[pl.ds(start, tokens), :].astype(bf16)
 
 
 def slots_in_row(column_ref, row_ref, capacity):
@@ -248,9 +264,13 @@
     return (column == wanted).astype(f32).astype(bf16)
 
 
-def dispatch_kernel(capacity, mix_ref, stream_ref, gain_ref, column_ref, row_ref, residual_ref, *send_refs):
+def dispatch_kernel(capacity, place_ref, *refs):
+    *refs, mix_ref = refs
+    blocks, _, block = mix_ref.shape
+    for k in range(blocks):
+        mix_ref[(place_ref[0] + blocks - k) % blocks] = refs[k][...]
+    stream_ref, gain_ref, column_ref, row_ref, residual_ref, *send_refs = refs[blocks:]
     tokens, width = stream_ref.shape
-    blocks, _, block = mix_ref.shape
     square = jnp.zeros((tokens, 1), f32)
     for k in range(blocks):
         lanes = slice(k * block, (k + 1) * block)
@@ -278,95 +298,111 @@
         send_ref[...] = send.astype(bf16)
 
 
-def gate_up(own_ref, others_ref, weight_refs, capacity):
-    rows, part = own_ref.shape
-    tables = [gather_table(rows // PARTS, rows, capacity, q) for q in range(PARTS)]
-    laid = [
-        jnp.concatenate([dot(table, ref[...]).astype(bf16) for table in tables], axis=1)
-        for ref in (own_ref, others_ref)
-    ]
-    for j, weight_ref in enumerate(weight_refs):
-        weight = weight_ref[: PARTS * part, :]
-        for i in range(2):
-            yield i, j, dot(laid[i], weight)
-
-
 def first_kernel(
     capacity, own_ref, others_ref, gate_ref, up_ref, gate_too_ref, up_too_ref, acts_ref, kept_ref
 ):
     weight_refs = (gate_ref, up_ref, gate_too_ref, up_too_ref)
-    for i, j, product in gate_up(own_ref, others_ref, weight_refs, capacity):
-        acts_ref[i, j] = product
     left = kept_ref.shape[1]
+    for i, ref in enumerate((own_ref, others_ref)):
+        rows = laid_out(ref, capacity)
+        for j, weight_ref in enumerate(weight_refs):
+            acts_ref[i, j] = dot(rows, weight_ref[: weight_ref.shape[0] - left, :])
     for j, weight_ref in enumerate(weight_refs):
         kept_ref[j] = weight_ref[weight_ref.shape[0] - left :, :]
 
 
-def second_kernel(capacity, own_ref, others_ref, kept_ref, acts_ref, mine_ref, theirs_ref):
-    outs = (mine_ref, theirs_ref)
+def laid_out(received_ref, capacity):
+    rows = received_ref.shape[0]
+    tables = [gather_table(rows // PARTS, rows, capacity, q) for q in range(PARTS)]
+    received = received_ref[...]
+    return jnp.concatenate([dot(table, received).astype(bf16) for table in tables], axis=1)
+
+
+def inner_of(rows, kept_ref, acts_ref, out_ref):
     width = kept_ref.shape[2]
-    gates = {}
-    weight_refs = [kept_ref.at[j] for j in range(kept_ref.shape[0])]
-    for i, j, product in gate_up(own_ref, others_ref, weight_refs, capacity):
-        product = product + acts_ref[i, j]
-        if j % 2 == 0:
-            gates[i] = silu(product)
-        else:
-            lanes = slice(j // 2 * width, (j // 2 + 1) * width)
-            outs[i][:, lanes] = (gates[i] * product).astype(bf16)
-
-
-def down_kernel(capacity, mine_ref, rest_ref, *refs):
-    *weight_refs, out_ref = refs
-    width = weight_refs[0].shape[0]
-    inner = [ref[:, k * width : (k + 1) * width] for ref in (mine_ref, rest_ref) for k in range(2)]
-    rows = mine_ref.shape[0]
+    for j in range(kept_ref.shape[0] // 2):
+        gate = acts_ref[2 * j] + dot(rows, kept_ref[2 * j])
+        up = acts_ref[2 * j + 1] + dot(rows, kept_ref[2 * j + 1])
+        out_ref[:, j * width : (j + 1) * width] = (silu(gate) * up).astype(bf16)
+
+
+def others_kernel(capacity, others_ref, kept_ref, acts_ref, out_ref):
+    inner_of(laid_out(others_ref, capacity), kept_ref, acts_ref.at[1], out_ref)
+
+
+def own_kernel(capacity, own_ref, kept_ref, acts_ref, down_ref, near_ref, out_ref, inner_ref):
+    inner_of(laid_out(own_ref, capacity), kept_ref, acts_ref.at[0], inner_ref)
+    width = down_ref.shape[0]
+    out_ref[...] = dot(inner_ref[:, :width], down_ref[...]) + dot(inner_ref[:, width:], near_ref[...])
+
+
+def down_kernel(capacity, partial_ref, rest_ref, next_ref, far_ref, out_ref):
+    rows, depth = rest_ref.shape
     block = out_ref.shape[1]
-    part = weight_refs[0].shape[1] // PARTS
+    part = next_ref.shape[1] // PARTS
     out = jnp.zeros(out_ref.shape, f32)
     for q in range(PARTS):
         lanes = pl.ds(pl.multiple_of(q * part + pl.program_id(0) * block, LANES), block)
-        product = dot(inner[0], weight_refs[0][:, lanes])
-        for k in range(1, len(inner)):
-            product = product + dot(inner[k], weight_refs[k][:, lanes])
+        product = partial_ref[:, lanes] + dot(rest_ref[:, : depth // 2], next_ref[:, lanes])
+        product = product + dot(rest_ref[:, depth // 2 :], far_ref[:, lanes])
         out = out + dot(spread_table(PARTS * rows, rows, capacity, q), product.astype(bf16))
     out_ref[...] = out.astype(bf16)
 
 
-def project_down(capacity, mine, rest, weights):
-    rows = mine.shape[0]
-    part = weights[0].shape[1] // PARTS
+def project_down(capacity, partial, rest, weights):
+    rows, width = partial.shape
     whole = pl.BlockSpec(memory_space=pltpu.VMEM)
     return pl.pallas_call(
         lambda *refs: down_kernel(capacity, *refs),
-        grid=(part // DOWN_LANES,),
-        out_shape=jax.ShapeDtypeStruct((PARTS * rows, part), bf16),
+        grid=(width // PARTS // DOWN_LANES,),
+        out_shape=jax.ShapeDtypeStruct((PARTS * rows, width // PARTS), bf16),
         in_specs=[whole, whole] + [whole for _ in weights],
         out_specs=pl.BlockSpec((PARTS * rows, DOWN_LANES), lambda k: (0, k)),
         compiler_params=pltpu.CompilerParams(vmem_limit_bytes=12 * 1024 * 1024),
-    )(mine, rest, *weights)
-
-
-def combine_kernel(capacity, results_ref, residual_ref, column_ref, row_ref, weight_ref, out_ref):
+    )(partial, rest, *weights)
+
+
+def combine_kernel(
+    capacity, results_ref, residual_ref, column_ref, row_ref, weight_ref, out_ref, held_ref, arrived
+):
+    pieces, count, width = held_ref.shape
+    copies = [
+        pltpu.make_async_copy(
+            results_ref.at[:, k * width : (k + 1) * width], held_ref.at[k], arrived.at[k]
+        )
+        for k in range(pieces)
+    ]
+    for copy in copies:
+        copy.start()
     tokens = residual_ref.shape[0]
     slots = slots_in_column(column_ref, row_ref, capacity)
     weight = weight_ref[...]
     weight = weight / jnp.sum(weight, axis=1, keepdims=True)
-    count, part = results_ref.shape
+    tables = []
     for q in range(PARTS):
         slot_at = lax.broadcasted_iota(jnp.int32, (tokens, count), 1) - q * capacity
         table = jnp.zeros((tokens, count), f32)
         for j in range(TOPK):
             table = table + jnp.where(slot_at == slots[j], weight[:, j : j + 1], 0.0)
-        high, low = split(table)
-        results = results_ref[...]
-        lanes = slice(q * part, (q + 1) * part)
-        routed = dot(high, results) + dot(low, results)
-        out_ref[:, lanes] = (residual_ref[:, lanes] + routed).astype(bf16)
+        tables.extend(split(table))
+    table = jnp.concatenate(tables, axis=0)
+    for k, copy in enumerate(copies):
+        copy.wait()
+        routed = dot(table, held_ref[k])
+        for q in range(PARTS):
+            start = (q * pieces + k) * width
+            lanes = slice(start, start + width)
+            high, low = (routed[(2 * q + i) * tokens : (2 * q + i + 1) * tokens] for i in range(2))
+            out_ref[:, lanes] = (residual_ref[:, lanes] + (high + low)).astype(bf16)
 
 
 def spread(value, axes):
     return lax.all_to_all(value, axes, split_axis=0, concat_axis=0, tiled=True)
+
+
+def shifted(value, k):
+    count = lax.axis_size(TP)
+    return lax.ppermute(value, TP, [(i, (i + k) % count) for i in range(count)])
 
 
 def layer(
@@ -396,11 +432,17 @@
     capacity = window_rows // sp_size
     piece = LANES // plane
 
-    down = expert_down_weight[0]
+    place, tp_place, down = lax.optimization_barrier(
+        (
+            lax.axis_index("sp_0").astype(jnp.int32).reshape(1),
+            lax.axis_index(TP).astype(jnp.int32).reshape(1),
+            expert_down_weight[0],
+        )
+    )
     down_near = lax.ppermute(down, TP, WEIGHT_PAIRS)
     down_next = lax.ppermute(down, TP, ROW_PAIRS)
 
-    floor = forget_minimum.reshape(1, -1)
+    floor = forget_minimum
     message = jax.ShapeDtypeStruct((plane, heads * piece + 16, LANES), bf16)
     states = call(
         state_kernel, message, forget_preact, value_input, floor, extra_log_decay
@@ -418,14 +460,15 @@
     totals = spread(totals, "sp_0")
     local = call(
         local_kernel,
-        jax.ShapeDtypeStruct((2, window_rows, width), f32),
+        jax.ShapeDtypeStruct((3, window_rows, width), f32),
         query,
         forget_preact,
         value_input,
+        output_gate,
         floor,
         extra_log_decay,
-    )
-    place = lax.axis_index("sp_0").astype(jnp.int32).reshape(1)
+        head_norm_gain,
+    )
     carried = call(
         lambda *refs: carry_kernel(heads, *refs),
         jax.ShapeDtypeStruct((plane, heads * piece, LANES), bf16),
@@ -438,23 +481,27 @@
     carried = spread(carried, PLANE)
     hidden = call(
         head_kernel,
-        jax.ShapeDtypeStruct((tp_size, window_rows, width), bf16),
+        jax.ShapeDtypeStruct((window_rows, width), bf16),
         local,
         carried,
-        head_norm_gain.reshape(1, -1),
-        output_gate,
-    )
-    hidden = spread(hidden, TP)
-    projected = jnp.einsum(
-        "ptc,pcd->td",
-        hidden,
-        output_weight.reshape(tp_size, width, -1),
-        preferred_element_type=f32,
-    ).astype(bf16)
+    )
+    hidden = [hidden] + [shifted(hidden, k) for k in range(1, tp_size)]
+    columns = output_weight.shape[1]
+    projected = call(
+        project_kernel,
+        (jax.ShapeDtypeStruct((quarter_rows, columns), bf16),) * tp_size,
+        tp_place,
+        *hidden,
+        output_weight,
+        kinds="s" + "v" * (tp_size + 1),
+        scratch=(pltpu.VMEM((window_rows, columns), f32),),
+    )
     gate_weight, up_weight, down_near, projected = lax.optimization_barrier(
         (expert_gate_weight[0], expert_up_weight[0], down_near, projected)
     )
-    mix = spread(projected.reshape(tp_size, quarter_rows, -1), TP)
+    mix = [projected[0]]
+    for k in range(1, tp_size):
+        mix.append(shifted(projected[k], k))
     down_far = lax.ppermute(down_near, TP, ROW_PAIRS)
     gate_weight_too = lax.ppermute(gate_weight, TP, WEIGHT_PAIRS)
     up_weight_too = lax.ppermute(up_weight, TP, WEIGHT_PAIRS)
@@ -469,11 +516,14 @@
     residual, *sends = call(
         lambda *refs: dispatch_kernel(capacity, *refs),
         (jax.ShapeDtypeStruct((quarter_rows, model_width), f32), *packed),
-        mix,
+        tp_place,
+        *mix,
         stream,
         feedforward_gain.reshape(1, -1),
         own,
         own_rows,
+        kinds="s" + "v" * (tp_size + 4),
+        scratch=(pltpu.VMEM((tp_size, quarter_rows, columns), bf16),),
     )
     hidden_part = expert_gate_weight.shape[2]
     rows = []
@@ -482,30 +532,36 @@
         rows.append((received, lax.ppermute(received, TP, ROW_PAIRS)))
     weights = (gate_weight, up_weight, gate_weight_too, up_weight_too)
     count = len(weights)
+    first_rows, down_next, down_far = lax.optimization_barrier((rows[0], down_next, down_far))
     acts, kept = call(
         lambda *refs: first_kernel(capacity, *refs),
         (
             jax.ShapeDtypeStruct((2, count, window_rows, hidden_part), f32),
             jax.ShapeDtypeStruct((count, model_width - first_depth, hidden_part), bf16),
         ),
-        *rows[0],
+        *first_rows,
         *weights,
         mib=16,
     )
-    acts, down_near, down_next, down_far = lax.optimization_barrier(
-        (acts, down_near, down_next, down_far)
-    )
-    mine, theirs = call(
-        lambda *refs: second_kernel(capacity, *refs),
-        (jax.ShapeDtypeStruct((window_rows, 2 * hidden_part), bf16),) * 2,
-        *rows[1],
+    theirs = call(
+        lambda *refs: others_kernel(capacity, *refs),
+        jax.ShapeDtypeStruct((window_rows, 2 * hidden_part), bf16),
+        rows[1][1],
         kept,
         acts,
     )
     rest = lax.ppermute(theirs, TP, ROW_PAIRS)
-    expert_out = project_down(
-        capacity, mine, rest, (down, down_near, down_next, down_far)
-    )
+    partial = call(
+        lambda *refs: own_kernel(capacity, *refs),
+        jax.ShapeDtypeStruct((window_rows, model_width), f32),
+        rows[1][0],
+        kept,
+        acts,
+        down,
+        down_near,
+        scratch=(pltpu.VMEM((window_rows, 2 * hidden_part), bf16),),
+    )
+    expert_out = project_down(capacity, partial, rest, (down_next, down_far))
     returned = spread(expert_out.reshape(sp_size, PARTS * capacity, -1), SP)
     return call(
         lambda *refs: combine_kernel(capacity, *refs),
@@ -515,6 +571,11 @@
         own,
         own_rows,
         router_weight,
+        kinds="hvvvv",
+        scratch=(
+            pltpu.VMEM((4, expert_out.shape[0], expert_out.shape[1] // 4), bf16),
+            pltpu.SemaphoreType.DMA((4,)),
+        ),
     )
 
 

time: 265 us -> 256 us (0.966)
  waiting for transfers between devices: 144 us -> 134 us
  Pallas kernels: 26.4 us -> 29.2 us
    ppermute x1, waiting for transfers between devices: 16.2 us -> 0.01 us  [layer(): up_weight_too = lax.ppermute(up_weight, TP, WEIGHT_PAIRS)]
    ppermute x1, waiting for transfers between devices: 0.01 us -> 15.4 us  [layer(): down_far = lax.ppermute(down_near, TP, ROW_PAIRS)]
    all_to_all x6 -> x4, waiting for transfers between devices: 94.6 us -> 80.3 us  [spread(): return lax.all_to_all(value, axes, split_axis=0, concat_axis=0, tiled=True)]
    all_to_all x6 -> x4, starting transfers between devices: 44.9 us -> 32.6 us  [spread(): return lax.all_to_all(value, axes, split_axis=0, concat_axis=0, tiled=True)]
    ppermute x0 -> x6, waiting for transfers between devices: none -> 11.8 us  [shifted(): return lax.ppermute(value, TP, [(i, (i + k) % count) for i in range(count)])]
    ppermute x0 -> x6, starting transfers between devices: none -> 9.14 us  [shifted(): return lax.ppermute(value, TP, [(i, (i + k) % count) for i in range(count)])]
    ppermute x1, waiting for transfers between devices: 6.19 us -> 1.66 us  [layer(): rest = lax.ppermute(theirs, TP, ROW_PAIRS)]
    pallas_call x9 -> x11, Pallas kernels: 20.5 us -> 23.9 us  [call(): pl.pallas_call(kernel, out_shape=out_shape, in_specs=[spaces[kind] for _,...]
  transfers between devices with their start and end apart: 14 -> 18, of which waited for: 10 -> 10; matrix products, arithmetic and copies ran while one was open for 1% -> 0% of each run, Pallas kernels for 5% -> 7%
where the time goes in v4:
time: 256 us
  waiting for transfers between devices  134 us (52%)
  starting transfers between devices  53.1 us (21%)
  Pallas kernels  29.2 us (11%)
  blocking collectives  26.3 us (10%)
  local copies, waits for them, and re-layouts  12.1 us (5%)
    all_to_all x4, waiting for transfers between devices, spread(): return lax.all_to_all(value, axes, split_axis=0, concat_axis=0, tiled=True)  80.3 us
    all_to_all x4, starting transfers between devices, spread(): return lax.all_to_all(value, axes, split_axis=0, concat_axis=0, tiled=True)  32.6 us
    all_to_all x2, blocking collectives, spread(): return lax.all_to_all(value, axes, split_axis=0, concat_axis=0, tiled=True)  26.3 us
    ppermute x2, waiting for transfers between devices, layer(): rows.append((received, lax.ppermute(received, TP, ROW_PAIRS)))  25.3 us
    pallas_call x11, Pallas kernels, call(): pl.pallas_call(kernel, out_shape=out_shape, in_specs=[spaces[kind] for _,...  23.9 us
    ppermute x1, waiting for transfers between devices, layer(): down_far = lax.ppermute(down_near, TP, ROW_PAIRS)  15.4 us
    unnamed x45, local copies, waits for them, and re-layouts  11.8 us
    ppermute x6, waiting for transfers between devices, shifted(): return lax.ppermute(value, TP, [(i, (i + k) % count) for i in range(count)])  11.8 us
  transfers between devices with their start and end apart: 18, of which 10 were waited for; matrix products, arithmetic and copies ran while one was open for 0% of the time, Pallas kernels for 7%

profile of v4, /device:TPU:1, one launch (start us, length us, event | category | flops | bytes accessed | tf_op | source)
XLA Modules:
  0.0 255.5 jit_solution(5724718322489682902)
XLA Ops:
  0.0 2.1 collective-permute-start
  2.1 0.9 copy-done.8
  3.1 0.9 copy-done.10
  4.0 0.7 copy-done.15
  4.7 0.7 copy-done.18
  5.4 1.4 shard_map.146
  6.8 10.5 %all_to_all.30.refs_0_ = bf16[8,64,128]{2,1,0:T(8,128)(2,1)S(1)} all-to-all(bf16[8,64,128]{2,1,0:T(8,128)(2,1)S(1)} %shard_map.146), channel_id=1, replica_groups=mesh['sp_0'=8,'sp_1'=4,'sp_2'=2,'tp_0'=2,'tp_1'=2] {'sp_1','sp_2'}, dimensions={0} | all-to-all | bytes 262144 | tf_op jit(solution)/shard_map/all_to_all | solution.py:400
  17.3 15.8 %all_to_all.31.refs_1_ = bf16[8,64,128]{2,1,0:T(8,128)(2,1)S(1)} all-to-all(bf16[8,64,128]{2,1,0:T(8,128)(2,1)S(1)} %get-tuple-element.34), channel_id=1, replica_groups=mesh['sp_0'=8,'sp_1'=4,'sp_2'=2,'tp_0'=2,'tp_1'=2] {'sp_0'}, dimensions={0} | all-to-all | bytes 262144 | tf_op jit(solution)/shard_map/all_to_all | solution.py:400
  33.1 0.7 shard_map.148
  33.9 6.2 %all-to-all-start.2 = ((bf16[8,48,128]{2,1,0:T(8,128)(2,1)}), bf16[8,48,128]{2,1,0:T(8,128)(2,1)}, u32[]{:S(2)}, u32[]{:S(2)}) async-start(bf16[8,48,128]{2,1,0:T(8,128)(2,1)} %shard_map.148), calls=%async_computation.2 | async-start | bytes 196608 | tf_op jit(solution)/shard_map/all_to_all | solution.py:400
  40.1 0.9 copy-done.9
  41.0 0.9 copy-done.11
  42.0 0.9 copy-done.13
  42.9 0.9 copy-done.14
  43.8 3.0 %shard_map.145.local_ref = f32[3,256,384]{2,1,0:T(8,128)S(1)} custom-call(bf16[256,384]{1,0:T(8,128)(2,1)S(1)} %copy-done.13, bf16[256,384]{1,0:T(8,128)(2,1)S(1)} %copy-done.9, bf16[256,384]{1,0:T(8,128)(2,1)S(1)} %copy-done.11, bf16[256,384]{1,0:T(8,128)(2,1)S(1)} %copy-done.14, f32[384]{0:T(512)S(1)} %copy-done.19, f32[3,256]{1,0:T(4,128)S(1)} %copy-done.16, ...), custom_call_target="tpu_custom_call" | custom-call | tf_op jit(solution)/shard_map/pallas_call | solution.py:50
  46.8 1.9 shard_map.149.refs_0_
  49.0 2.7 %collective-permute-start.2 = (bf16[256,384]{1,0:T(8,128)(2,1)}, bf16[256,384]{1,0:T(8,128)(2,1)S(1)}, u32[]{:S(2)}, u32[]{:S(2)}) collective-permute-start(bf16[256,384]{1,0:T(8,128)(2,1)} %shard_map.149.refs_0_), channel_id=1, source_target_pairs={{0,2},{1,3},{2,0},{3,1},{4,6},{5,7},{6,4},{7,5},{8,10},{9,11},{10,... | collective-permute-start | bytes 589832 | tf_op jit(solution)/shard_map/ppermute | solution.py:405
  51.7 1.5 collective-permute-start.3
  53.4 3.0 %collective-permute-done.1.refs_1_ = bf16[256,384]{1,0:T(8,128)(2,1)S(1)} collective-permute-done((bf16[256,384]{1,0:T(8,128)(2,1)}, bf16[256,384]{1,0:T(8,128)(2,1)S(1)}, u32[]{:S(2)}, u32[]{:S(2)}) %collective-permute-start.1) | collective-permute-done | bytes 196640 | tf_op jit(solution)/shard_map/ppermute | solution.py:405
  56.5 4.5 %collective-permute-done.2.refs_2_ = bf16[256,384]{1,0:T(8,128)(2,1)S(1)} collective-permute-done((bf16[256,384]{1,0:T(8,128)(2,1)}, bf16[256,384]{1,0:T(8,128)(2,1)S(1)}, u32[]{:S(2)}, u32[]{:S(2)}) %collective-permute-start.2) | collective-permute-done | bytes 196640 | tf_op jit(solution)/shard_map/ppermute | solution.py:405
  61.0 1.9 shard_map.150
  63.0 1.9 collective-permute-start.4
  64.9 2.5 collective-permute-start.5
  68.2 3.7 %collective-permute-done.5.refs_3_ = bf16[64,768]{1,0:T(8,128)(2,1)S(1)} collective-permute-done((bf16[64,768]{1,0:T(8,128)(2,1)S(1)}, bf16[64,768]{1,0:T(8,128)(2,1)S(1)}, u32[]{:S(2)}, u32[]{:S(2)}) %collective-permute-start.5) | collective-permute-done | bytes 98336 | tf_op jit(solution)/shard_map/ppermute | solution.py:405
  71.9 2.0 shard_map.151
  73.9 1.1 copy-done.5
  75.0 0.9 copy-done.6
  75.9 6.3 %all-to-all-start.4 = ((bf16[64,8,1152]{2,1,0:T(8,128)(2,1)}), bf16[64,8,1152]{2,1,0:T(8,128)(2,1)S(1)}, u32[]{:S(2)}, u32[]{:S(2)}) async-start(bf16[64,8,1152]{2,1,0:T(8,128)(2,1)} %bitcast.26), calls=%async_computation.4 | async-start | bytes 2359296 | tf_op jit(solution)/shard_map/all_to_all | solution.py:400
  82.3 2.3 collective-permute-start.8
  84.5 0.7 collective-permute-start.9
  85.2 1.5 collective-permute-start.11
  86.7 26.2 %all-to-all-done.4 = bf16[64,8,1152]{2,1,0:T(8,128)(2,1)S(1)} async-done(((bf16[64,8,1152]{2,1,0:T(8,128)(2,1)}), bf16[64,8,1152]{2,1,0:T(8,128)(2,1)S(1)}, u32[]{:S(2)}, u32[]{:S(2)}) %all-to-all-start.4) | async-done | bytes 1179680 | tf_op jit(solution)/shard_map/all_to_all | solution.py:400
  112.9 2.0 collective-permute-start.7
  114.9 6.9 %all-to-all-start.3 = ((bf16[64,8,384]{2,1,0:T(8,128)(2,1)}), bf16[64,8,384]{2,1,0:T(8,128)(2,1)S(1)}, u32[]{:S(2)}, u32[]{:S(2)}) async-start(bf16[64,8,384]{2,1,0:T(8,128)(2,1)} %bitcast.7), calls=%async_computation.3 | async-start | bytes 786432 | tf_op jit(solution)/shard_map/all_to_all | solution.py:400
  121.8 15.2 %all-to-all-done.3 = bf16[64,8,384]{2,1,0:T(8,128)(2,1)S(1)} async-done(((bf16[64,8,384]{2,1,0:T(8,128)(2,1)}), bf16[64,8,384]{2,1,0:T(8,128)(2,1)S(1)}, u32[]{:S(2)}, u32[]{:S(2)}) %all-to-all-start.3) | async-done | bytes 393248 | tf_op jit(solution)/shard_map/all_to_all | solution.py:400
  137.6 15.4 %collective-permute-done.9.refs_3_ = bf16[256,3072]{1,0:T(8,128)(2,1)} collective-permute-done((bf16[256,3072]{1,0:T(8,128)(2,1)}, bf16[256,3072]{1,0:T(8,128)(2,1)}, u32[]{:S(2)}, u32[]{:S(2)}) %collective-permute-start.9) | collective-permute-done | bytes 1572896 | tf_op jit(solution)/shard_map/ppermute | solution.py:505
  153.0 25.3 %collective-permute-done.7.refs_1_ = bf16[512,1152]{1,0:T(8,128)(2,1)} collective-permute-done((bf16[512,1152]{1,0:T(8,128)(2,1)S(1)}, bf16[512,1152]{1,0:T(8,128)(2,1)}, u32[]{:S(2)}, u32[]{:S(2)}) %collective-permute-start.7) | collective-permute-done | bytes 1179680 | tf_op jit(solution)/shard_map/ppermute | solution.py:532
  178.3 1.4 copy-done.3
  179.7 1.4 copy-done.4
  181.1 6.3 %shard_map.152 = (f32[2,4,256,256]{3,2,1,0:T(8,128)S(1)}, bf16[4,768,256]{2,1,0:T(8,128)(2,1)S(1)}) custom-call(bf16[512,1152]{1,0:T(8,128)(2,1)S(1)} %bitcast.16, bf16[512,1152]{1,0:T(8,128)(2,1)} %collective-permute-done.7.refs_1_, bf16[3072,256]{1,0:T(8,128)(2,1)S(1)} %bitcast.23, bf16[3072,256]{1,0:T(8,128)(2,1)S(1)} %bitcast.25, ...), custom_call_target="tpu_custom_call" | custom-call | tf_op jit(solution)/shard_map/pallas_call | solution.py:50
  187.5 0.9 shard_map.154
  188.4 2.1 collective-permute-start.13
  190.4 3.2 %shard_map.153.refs_0_ = f32[256,3072]{1,0:T(8,128)S(1)} custom-call(bf16[512,384]{1,0:T(8,128)(2,1)S(1)} %bitcast.18, bf16[4,768,256]{2,1,0:T(8,128)(2,1)S(1)} %get-tuple-element.52.refs_1_, f32[2,4,256,256]{3,2,1,0:T(8,128)S(1)} %get-tuple-element.53.refs_2_, bf16[256,3072]{1,0:T(8,128)(2,1)S(1)} %bitcast.21, bf16[256,3072]{1,0:T(8,128)(2,1)} %collective-permute-done.refs_4_), custom_call_target="tpu_custom_call" | custom-call | tf_op jit(solution)/shard_map/pallas_call | solution.py:50
  193.6 1.7 collective-permute-done.13.refs_1_
  195.3 5.3 %shard_map.155 = bf16[512,1536]{1,0:T(8,128)(2,1)} custom-call(f32[256,3072]{1,0:T(8,128)S(1)} %shard_map.153.refs_0_, bf16[256,512]{1,0:T(8,128)(2,1)S(1)} %collective-permute-done.13.refs_1_, bf16[256,3072]{1,0:T(8,128)(2,1)} %collective-permute-done.8.refs_2_, bf16[256,3072]{1,0:T(8,128)(2,1)} %collective-permute-done.9.refs_3_), custom_call_target="tpu_custom_call" | custom-call | tf_op jit(solution)/shard_map/pallas_call | solution.py:355
  200.6 13.2 %all-to-all-start.5 = ((bf16[64,8,1536]{2,1,0:T(8,128)(2,1)}), bf16[64,8,1536]{2,1,0:T(8,128)(2,1)S(1)}, u32[]{:S(2)}, u32[]{:S(2)}) async-start(bf16[64,8,1536]{2,1,0:T(8,128)(2,1)} %bitcast.11), calls=%async_computation.5 | async-start | bytes 3145728 | tf_op jit(solution)/shard_map/all_to_all | solution.py:400
  213.9 39.0 %all-to-all-done.5 = bf16[64,8,1536]{2,1,0:T(8,128)(2,1)S(1)} async-done(((bf16[64,8,1536]{2,1,0:T(8,128)(2,1)}), bf16[64,8,1536]{2,1,0:T(8,128)(2,1)S(1)}, u32[]{:S(2)}, u32[]{:S(2)}) %all-to-all-start.5) | async-done | bytes 1572896 | tf_op jit(solution)/shard_map/all_to_all | solution.py:400
  252.8 2.5 shard_map.156
  (50 shorter events, 2.2 us)
Async XLA Ops:
  0.0 53.3 %copy-start = (s32[256,2]{0,1:T(2,128)S(1)}, s32[256,2]{0,1:T(2,128)}, u32[]{:S(2)}) copy-start(s32[256,2]{0,1:T(2,128)} %param.25) | copy-start | bytes 6148
  0.0 40.1 %copy-start.19 = (f32[384]{0:T(512)S(1)}, f32[384]{0:T(512)}, u32[]{:S(2)}) copy-start(f32[384]{0:T(512)} %floor_ref.3) | copy-start | bytes 4612
  0.0 40.1 %copy-start.16 = (f32[3,256]{1,0:T(4,128)S(1)}, f32[3,256]{1,0:T(4,128)}, u32[]{:S(2)}) copy-start(f32[3,256]{1,0:T(4,128)} %extra_ref.3) | copy-start | bytes 9220
  0.0 40.1 %copy-start.20 = (f32[384]{0:T(512)S(1)}, f32[384]{0:T(512)}, u32[]{:S(2)}) copy-start(f32[384]{0:T(512)} %gain_ref.1) | copy-start | bytes 4612
  0.0 62.9 %collective-permute-start = (bf16[256,3072]{1,0:T(8,128)(2,1)}, bf16[256,3072]{1,0:T(8,128)(2,1)}, u32[]{:S(2)}, u32[]{:S(2)}) collective-permute-start(bf16[256,3072]{1,0:T(8,128)(2,1)} %bitcast.19), channel_id=1, source_target_pairs={{0,1},{1,0},{2,3},{3,2},{4,5},{5,4},{6,7},{7,6},{8,9},{9,8},{10,11... | collective-permute-start | bytes 4718600 | tf_op jit(solution)/shard_map/ppermute | solution.py:442
  2.1 0.9 copy-start.8
  3.1 0.9 copy-start.10
  4.0 0.7 copy-start.15
  4.7 0.7 copy-start.18
  33.9 12.9 %all-to-all-start.2 = ((bf16[8,48,128]{2,1,0:T(8,128)(2,1)}), bf16[8,48,128]{2,1,0:T(8,128)(2,1)}, u32[]{:S(2)}, u32[]{:S(2)}) async-start(bf16[8,48,128]{2,1,0:T(8,128)(2,1)} %shard_map.148), calls=%async_computation.2 | async-start | bytes 196608 | tf_op jit(solution)/shard_map/all_to_all | solution.py:400
  40.1 0.9 copy-start.9
  41.0 0.9 copy-start.11
  42.0 0.9 copy-start.13
  42.9 0.9 copy-start.14
  43.8 17.2 %copy-start.1 = (bf16[1536,768]{1,0:T(8,128)(2,1)S(1)}, bf16[1536,768]{1,0:T(8,128)(2,1)}, u32[]{:S(2)}) copy-start(bf16[1536,768]{1,0:T(8,128)(2,1)} %refs_4_.2) | copy-start | bytes 7077892
  48.7 7.7 %collective-permute-start.1 = (bf16[256,384]{1,0:T(8,128)(2,1)}, bf16[256,384]{1,0:T(8,128)(2,1)S(1)}, u32[]{:S(2)}, u32[]{:S(2)}) collective-permute-start(bf16[256,384]{1,0:T(8,128)(2,1)} %shard_map.149.refs_0_), channel_id=1, source_target_pairs={{0,1},{1,2},{2,3},{3,0},{4,5},{5,6},{6,7},{7,4},{8,9},{9,10},{10,1... | collective-permute-start | bytes 589832 | tf_op jit(solution)/shard_map/ppermute | solution.py:405
  49.0 12.0 %collective-permute-start.2 = (bf16[256,384]{1,0:T(8,128)(2,1)}, bf16[256,384]{1,0:T(8,128)(2,1)S(1)}, u32[]{:S(2)}, u32[]{:S(2)}) collective-permute-start(bf16[256,384]{1,0:T(8,128)(2,1)} %shard_map.149.refs_0_), channel_id=1, source_target_pairs={{0,2},{1,3},{2,0},{3,1},{4,6},{5,7},{6,4},{7,5},{8,10},{9,11},{10,... | collective-permute-start | bytes 589832 | tf_op jit(solution)/shard_map/ppermute | solution.py:405
  51.7 9.3 %collective-permute-start.3 = (bf16[256,384]{1,0:T(8,128)(2,1)}, bf16[256,384]{1,0:T(8,128)(2,1)S(1)}, u32[]{:S(2)}, u32[]{:S(2)}) collective-permute-start(bf16[256,384]{1,0:T(8,128)(2,1)} %shard_map.149.refs_0_), channel_id=1, source_target_pairs={{0,3},{1,0},{2,1},{3,2},{4,7},{5,4},{6,5},{7,6},{8,11},{9,8},{10,9... | collective-permute-start | bytes 589832 | tf_op jit(solution)/shard_map/ppermute | solution.py:405
  53.4 18.4 %copy-start.12 = (bf16[64,3072]{1,0:T(8,128)(2,1)S(1)}, bf16[64,3072]{1,0:T(8,128)(2,1)}, u32[]{:S(2)}) copy-start(bf16[64,3072]{1,0:T(8,128)(2,1)} %refs_5_.1) | copy-start | bytes 1179652
  53.4 18.4 %copy-start.17 = (f32[3072]{0:T(1024)S(1)}, f32[3072]{0:T(1024)}, u32[]{:S(2)}) copy-start(f32[3072]{0:T(1024)} %param.24) | copy-start | bytes 36868
  63.0 5.2 %collective-permute-start.4 = (bf16[64,768]{1,0:T(8,128)(2,1)S(1)}, bf16[64,768]{1,0:T(8,128)(2,1)S(1)}, u32[]{:S(2)}, u32[]{:S(2)}) collective-permute-start(bf16[64,768]{1,0:T(8,128)(2,1)S(1)} %get-tuple-element.42), channel_id=1, source_target_pairs={{0,1},{1,2},{2,3},{3,0},{4,5},{5,6},{6,7},{7,4},{8,9},{9,10},{10,1... | collective-permute-start | bytes 294920 | tf_op jit(solution)/shard_map/ppermute | solution.py:405
  64.9 7.0 %collective-permute-start.5 = (bf16[64,768]{1,0:T(8,128)(2,1)S(1)}, bf16[64,768]{1,0:T(8,128)(2,1)S(1)}, u32[]{:S(2)}, u32[]{:S(2)}) collective-permute-start(bf16[64,768]{1,0:T(8,128)(2,1)S(1)} %get-tuple-element.43), channel_id=1, source_target_pairs={{0,2},{1,3},{2,0},{3,1},{4,6},{5,7},{6,4},{7,5},{8,10},{9,11},{10,... | collective-permute-start | bytes 294920 | tf_op jit(solution)/shard_map/ppermute | solution.py:405
  67.4 4.5 %collective-permute-start.6 = (bf16[64,768]{1,0:T(8,128)(2,1)S(1)}, bf16[64,768]{1,0:T(8,128)(2,1)S(1)}, u32[]{:S(2)}, u32[]{:S(2)}) collective-permute-start(bf16[64,768]{1,0:T(8,128)(2,1)S(1)} %get-tuple-element.44), channel_id=1, source_target_pairs={{0,3},{1,0},{2,1},{3,2},{4,7},{5,4},{6,5},{7,6},{8,11},{9,8},{10,9... | collective-permute-start | bytes 294920 | tf_op jit(solution)/shard_map/ppermute | solution.py:405
  71.9 10.4 %copy-start.2 = (bf16[1,256,3072]{2,1,0:T(8,128)(2,1)S(1)}, bf16[1,256,3072]{2,1,0:T(8,128)(2,1)}, u32[]{:S(2)}) copy-start(bf16[1,256,3072]{2,1,0:T(8,128)(2,1)} %param.29) | copy-start | bytes 4718596
  73.9 1.1 copy-start.5
  75.0 0.9 copy-start.6
  75.9 37.0 %all-to-all-start.4 = ((bf16[64,8,1152]{2,1,0:T(8,128)(2,1)}), bf16[64,8,1152]{2,1,0:T(8,128)(2,1)S(1)}, u32[]{:S(2)}, u32[]{:S(2)}) async-start(bf16[64,8,1152]{2,1,0:T(8,128)(2,1)} %bitcast.26), calls=%async_computation.4 | async-start | bytes 2359296 | tf_op jit(solution)/shard_map/all_to_all | solution.py:400
  82.3 39.5 %collective-permute-start.8 = (bf16[256,3072]{1,0:T(8,128)(2,1)S(1)}, bf16[256,3072]{1,0:T(8,128)(2,1)}, u32[]{:S(2)}, u32[]{:S(2)}) collective-permute-start(bf16[256,3072]{1,0:T(8,128)(2,1)S(1)} %bitcast.20), channel_id=1, source_target_pairs={{1,2},{2,1},{3,0},{0,3},{5,6},{6,5},{7,4},{4,7},{9,10},{10,9},{11,... | collective-permute-start | bytes 4718600 | tf_op jit(solution)/shard_map/ppermute | solution.py:443
  84.5 68.5 %collective-permute-start.9 = (bf16[256,3072]{1,0:T(8,128)(2,1)}, bf16[256,3072]{1,0:T(8,128)(2,1)}, u32[]{:S(2)}, u32[]{:S(2)}) collective-permute-start(bf16[256,3072]{1,0:T(8,128)(2,1)} %collective-permute-done.refs_4_), channel_id=1, source_target_pairs={{1,2},{2,1},{3,0},{0,3},{5,6},{6,5},{7,4},{4,7},{9,10},{10,9},{11,... | collective-permute-start | bytes 4718600 | tf_op jit(solution)/shard_map/ppermute | solution.py:505
  85.2 93.1 %collective-permute-start.10 = (bf16[3072,256]{1,0:T(8,128)(2,1)}, bf16[3072,256]{1,0:T(8,128)(2,1)}, u32[]{:S(2)}, u32[]{:S(2)}) collective-permute-start(bf16[3072,256]{1,0:T(8,128)(2,1)} %bitcast.22), channel_id=1, source_target_pairs={{0,1},{1,0},{2,3},{3,2},{4,5},{5,4},{6,7},{7,6},{8,9},{9,8},{10,11... | collective-permute-start | bytes 4718600 | tf_op jit(solution)/shard_map/ppermute | solution.py:506
  85.2 93.1 %collective-permute-start.11 = (bf16[3072,256]{1,0:T(8,128)(2,1)}, bf16[3072,256]{1,0:T(8,128)(2,1)}, u32[]{:S(2)}, u32[]{:S(2)}) collective-permute-start(bf16[3072,256]{1,0:T(8,128)(2,1)} %bitcast.24), channel_id=1, source_target_pairs={{0,1},{1,0},{2,3},{3,2},{4,5},{5,4},{6,7},{7,6},{8,9},{9,8},{10,11... | collective-permute-start | bytes 4718600 | tf_op jit(solution)/shard_map/ppermute | solution.py:507
  112.9 65.5 %collective-permute-start.7 = (bf16[512,1152]{1,0:T(8,128)(2,1)S(1)}, bf16[512,1152]{1,0:T(8,128)(2,1)}, u32[]{:S(2)}, u32[]{:S(2)}) collective-permute-start(bf16[512,1152]{1,0:T(8,128)(2,1)S(1)} %bitcast.15), channel_id=1, source_target_pairs={{1,2},{2,1},{3,0},{0,3},{5,6},{6,5},{7,4},{4,7},{9,10},{10,9},{11,... | collective-permute-start | bytes 3538952 | tf_op jit(solution)/shard_map/ppermute | solution.py:532
  114.9 22.1 %all-to-all-start.3 = ((bf16[64,8,384]{2,1,0:T(8,128)(2,1)}), bf16[64,8,384]{2,1,0:T(8,128)(2,1)S(1)}, u32[]{:S(2)}, u32[]{:S(2)}) async-start(bf16[64,8,384]{2,1,0:T(8,128)(2,1)} %bitcast.7), calls=%async_computation.3 | async-start | bytes 786432 | tf_op jit(solution)/shard_map/all_to_all | solution.py:400
  136.9 50.6 %collective-permute-start.12 = (bf16[512,384]{1,0:T(8,128)(2,1)S(1)}, bf16[512,384]{1,0:T(8,128)(2,1)S(1)}, u32[]{:S(2)}, u32[]{:S(2)}) collective-permute-start(bf16[512,384]{1,0:T(8,128)(2,1)S(1)} %bitcast.17), channel_id=1, source_target_pairs={{1,2},{2,1},{3,0},{0,3},{5,6},{6,5},{7,4},{4,7},{9,10},{10,9},{11,... | collective-permute-start | bytes 1179656 | tf_op jit(solution)/shard_map/ppermute | solution.py:532
  178.3 1.4 copy-start.3
  179.7 1.4 copy-start.4
  188.4 6.9 %collective-permute-start.13 = (bf16[256,512]{1,0:T(8,128)(2,1)S(1)}, bf16[256,512]{1,0:T(8,128)(2,1)S(1)}, u32[]{:S(2)}, u32[]{:S(2)}) collective-permute-start(bf16[256,512]{1,0:T(8,128)(2,1)S(1)} %shard_map.154), channel_id=1, source_target_pairs={{1,2},{2,1},{3,0},{0,3},{5,6},{6,5},{7,4},{4,7},{9,10},{10,9},{11,... | collective-permute-start | bytes 786440 | tf_op jit(solution)/shard_map/ppermute | solution.py:553
  200.6 13.2 %copy-start.21 = (f32[64,2]{0,1:T(2,128)S(1)}, f32[64,2]{0,1:T(2,128)}, u32[]{:S(2)}) copy-start(f32[64,2]{0,1:T(2,128)} %param.26) | copy-start | bytes 1540
  200.6 52.2 %copy-start.7 = (f32[64,3072]{1,0:T(8,128)S(1)}, f32[64,3072]{1,0:T(8,128)}, u32[]{:S(2)}) copy-start(f32[64,3072]{1,0:T(8,128)} %copy-done.6) | copy-start | bytes 2359300
  200.6 52.2 %all-to-all-start.5 = ((bf16[64,8,1536]{2,1,0:T(8,128)(2,1)}), bf16[64,8,1536]{2,1,0:T(8,128)(2,1)S(1)}, u32[]{:S(2)}, u32[]{:S(2)}) async-start(bf16[64,8,1536]{2,1,0:T(8,128)(2,1)} %bitcast.11), calls=%async_computation.5 | async-start | bytes 3145728 | tf_op jit(solution)/shard_map/all_to_all | solution.py:400

commit v5 on v4

--- a/solution.py
+++ b/solution.py
@@ -16,8 +16,17 @@
 SP = ("sp_0", "sp_1", "sp_2")
 TP = ("tp_0", "tp_1")
 SP_TP = SP + TP
-ROW_PAIRS = ((1, 2), (2, 1), (3, 0), (0, 3))
-WEIGHT_PAIRS = ((0, 1), (1, 0), (2, 3), (3, 2))
+CORE_TP = ("sp_2",) + TP
+EVEN_LINKS = ((0, 1), (1, 0), (2, 3), (3, 2))
+ODD_LINKS = ((1, 2), (2, 1), (3, 0), (0, 3))
+
+
+def by_core(first, second):
+    return first + tuple((a + 4, b + 4) for a, b in second)
+
+
+WEIGHT_PAIRS = by_core(EVEN_LINKS, ODD_LINKS)
+ROW_PAIRS = by_core(ODD_LINKS, EVEN_LINKS)
 FIRST_SHARE = (3, 4)
 
 
@@ -298,17 +307,15 @@
         send_ref[...] = send.astype(bf16)
 
 
-def first_kernel(
-    capacity, own_ref, others_ref, gate_ref, up_ref, gate_too_ref, up_too_ref, acts_ref, kept_ref
-):
-    weight_refs = (gate_ref, up_ref, gate_too_ref, up_too_ref)
-    left = kept_ref.shape[1]
+def first_kernel(capacity, own_ref, others_ref, *refs):
+    *weight_refs, acts_ref, kept_ref = refs
+    depth = weight_refs[0].shape[0] - kept_ref.shape[1]
     for i, ref in enumerate((own_ref, others_ref)):
         rows = laid_out(ref, capacity)
         for j, weight_ref in enumerate(weight_refs):
-            acts_ref[i, j] = dot(rows, weight_ref[: weight_ref.shape[0] - left, :])
+            acts_ref[i, j] = dot(rows, weight_ref[:depth, :])
     for j, weight_ref in enumerate(weight_refs):
-        kept_ref[j] = weight_ref[weight_ref.shape[0] - left :, :]
+        kept_ref[j] = weight_ref[depth:, :]
 
 
 def laid_out(received_ref, capacity):
@@ -336,36 +343,51 @@
     out_ref[...] = dot(inner_ref[:, :width], down_ref[...]) + dot(inner_ref[:, width:], near_ref[...])
 
 
-def down_kernel(capacity, partial_ref, rest_ref, next_ref, far_ref, out_ref):
+def down_kernel(capacity, partial_ref, rest_ref, next_ref, far_ref, out_ref, held_ref, arrived):
     rows, depth = rest_ref.shape
-    block = out_ref.shape[1]
-    part = next_ref.shape[1] // PARTS
-    out = jnp.zeros(out_ref.shape, f32)
+    _, pieces, _, block = held_ref.shape
+    each = pieces // PARTS
+    order = [q * each + k for k in range(each) for q in range(PARTS)]
+    copies = {
+        (i, n): pltpu.make_async_copy(
+            ref.at[:, n * block : (n + 1) * block], held_ref.at[i, n], arrived.at[i, n]
+        )
+        for n in order
+        for i, ref in enumerate((next_ref, far_ref))
+    }
+    for copy in copies.values():
+        copy.start()
+    tables = [spread_table(PARTS * rows, rows, capacity, q) for q in range(PARTS)]
+    rest = [rest_ref[:, : depth // 2], rest_ref[:, depth // 2 :]]
+    for k in range(each):
+        out = jnp.zeros((PARTS * rows, block), f32)
+        for q in range(PARTS):
+            n = q * each + k
+            product = partial_ref[:, n * block : (n + 1) * block]
+            for i in range(2):
+                copies[i, n].wait()
+                product = product + dot(rest[i], held_ref[i, n])
+            out = out + dot(tables[q], product.astype(bf16))
+        out_ref[:, k * block : (k + 1) * block] = out.astype(bf16)
+
+
+def tables_kernel(capacity, column_ref, row_ref, weight_ref, out_ref):
+    tokens = column_ref.shape[0]
+    count = out_ref.shape[1]
+    slots = slots_in_column(column_ref, row_ref, capacity)
+    weight = weight_ref[...]
+    weight = weight / jnp.sum(weight, axis=1, keepdims=True)
     for q in range(PARTS):
-        lanes = pl.ds(pl.multiple_of(q * part + pl.program_id(0) * block, LANES), block)
-        product = partial_ref[:, lanes] + dot(rest_ref[:, : depth // 2], next_ref[:, lanes])
-        product = product + dot(rest_ref[:, depth // 2 :], far_ref[:, lanes])
-        out = out + dot(spread_table(PARTS * rows, rows, capacity, q), product.astype(bf16))
-    out_ref[...] = out.astype(bf16)
-
-
-def project_down(capacity, partial, rest, weights):
-    rows, width = partial.shape
-    whole = pl.BlockSpec(memory_space=pltpu.VMEM)
-    return pl.pallas_call(
-        lambda *refs: down_kernel(capacity, *refs),
-        grid=(width // PARTS // DOWN_LANES,),
-        out_shape=jax.ShapeDtypeStruct((PARTS * rows, width // PARTS), bf16),
-        in_specs=[whole, whole] + [whole for _ in weights],
-        out_specs=pl.BlockSpec((PARTS * rows, DOWN_LANES), lambda k: (0, k)),
-        compiler_params=pltpu.CompilerParams(vmem_limit_bytes=12 * 1024 * 1024),
-    )(partial, rest, *weights)
-
-
-def combine_kernel(
-    capacity, results_ref, residual_ref, column_ref, row_ref, weight_ref, out_ref, held_ref, arrived
-):
-    pieces, count, width = held_ref.shape
+        slot_at = lax.broadcasted_iota(jnp.int32, (tokens, count), 1) - q * capacity
+        table = jnp.zeros((tokens, count), f32)
+        for j in range(TOPK):
+            table = table + jnp.where(slot_at == slots[j], weight[:, j : j + 1], 0.0)
+        for i, piece in enumerate(split(table)):
+            out_ref[(2 * q + i) * tokens : (2 * q + i + 1) * tokens, :] = piece
+
+
+def combine_kernel(results_ref, residual_ref, table_ref, out_ref, held_ref, arrived):
+    pieces, _, width = held_ref.shape
     copies = [
         pltpu.make_async_copy(
             results_ref.at[:, k * width : (k + 1) * width], held_ref.at[k], arrived.at[k]
@@ -375,20 +397,9 @@
     for copy in copies:
         copy.start()
     tokens = residual_ref.shape[0]
-    slots = slots_in_column(column_ref, row_ref, capacity)
-    weight = weight_ref[...]
-    weight = weight / jnp.sum(weight, axis=1, keepdims=True)
-    tables = []
-    for q in range(PARTS):
-        slot_at = lax.broadcasted_iota(jnp.int32, (tokens, count), 1) - q * capacity
-        table = jnp.zeros((tokens, count), f32)
-        for j in range(TOPK):
-            table = table + jnp.where(slot_at == slots[j], weight[:, j : j + 1], 0.0)
-        tables.extend(split(table))
-    table = jnp.concatenate(tables, axis=0)
     for k, copy in enumerate(copies):
         copy.wait()
-        routed = dot(table, held_ref[k])
+        routed = dot(table_ref[...], held_ref[k])
         for q in range(PARTS):
             start = (q * pieces + k) * width
             lanes = slice(start, start + width)
@@ -439,8 +450,8 @@
             expert_down_weight[0],
         )
     )
-    down_near = lax.ppermute(down, TP, WEIGHT_PAIRS)
-    down_next = lax.ppermute(down, TP, ROW_PAIRS)
+    down_near = lax.ppermute(down, CORE_TP, WEIGHT_PAIRS)
+    down_next = lax.ppermute(down, CORE_TP, ROW_PAIRS)
 
     floor = forget_minimum
     message = jax.ShapeDtypeStruct((plane, heads * piece + 16, LANES), bf16)
@@ -485,7 +496,18 @@
         local,
         carried,
     )
-    hidden = [hidden] + [shifted(hidden, k) for k in range(1, tp_size)]
+    own = lax.dynamic_slice_in_dim(routes, lax.axis_index(TP) * quarter_rows, quarter_rows, 0)
+    own_rows = own.T
+    tables = call(
+        lambda *refs: tables_kernel(capacity, *refs),
+        jax.ShapeDtypeStruct((2 * PARTS * quarter_rows, PARTS * window_rows), bf16),
+        own,
+        own_rows,
+        router_weight,
+    )
+    hidden = [hidden]
+    for k in range(1, tp_size):
+        hidden.append(shifted(hidden[0], k))
     columns = output_weight.shape[1]
     projected = call(
         project_kernel,
@@ -502,12 +524,10 @@
     mix = [projected[0]]
     for k in range(1, tp_size):
         mix.append(shifted(projected[k], k))
-    down_far = lax.ppermute(down_near, TP, ROW_PAIRS)
-    gate_weight_too = lax.ppermute(gate_weight, TP, WEIGHT_PAIRS)
-    up_weight_too = lax.ppermute(up_weight, TP, WEIGHT_PAIRS)
-
-    own = lax.dynamic_slice_in_dim(routes, lax.axis_index(TP) * quarter_rows, quarter_rows, 0)
-    own_rows = own.T
+    down_far = lax.ppermute(down_near, CORE_TP, ROW_PAIRS)
+    gate_weight_too = lax.ppermute(gate_weight, CORE_TP, WEIGHT_PAIRS)
+    up_weight_too = lax.ppermute(up_weight, CORE_TP, WEIGHT_PAIRS)
+
     first_depth = model_width * FIRST_SHARE[0] // FIRST_SHARE[1]
     packed = [
         jax.ShapeDtypeStruct((window_rows * PARTS, depth // PARTS), bf16)
@@ -529,7 +549,7 @@
     rows = []
     for send in sends:
         received = spread(send.reshape(sp_size, PARTS * capacity, -1), SP).reshape(send.shape)
-        rows.append((received, lax.ppermute(received, TP, ROW_PAIRS)))
+        rows.append((received, lax.ppermute(received, CORE_TP, ROW_PAIRS)))
     weights = (gate_weight, up_weight, gate_weight_too, up_weight_too)
     count = len(weights)
     first_rows, down_next, down_far = lax.optimization_barrier((rows[0], down_next, down_far))
@@ -550,7 +570,7 @@
         kept,
         acts,
     )
-    rest = lax.ppermute(theirs, TP, ROW_PAIRS)
+    rest = lax.ppermute(theirs, CORE_TP, ROW_PAIRS)
     partial = call(
         lambda *refs: own_kernel(capacity, *refs),
         jax.ShapeDtypeStruct((window_rows, model_width), f32),
@@ -561,17 +581,28 @@
         down_near,
         scratch=(pltpu.VMEM((window_rows, 2 * hidden_part), bf16),),
     )
-    expert_out = project_down(capacity, partial, rest, (down_next, down_far))
+    pieces = model_width // DOWN_LANES
+    expert_out = call(
+        lambda *refs: down_kernel(capacity, *refs),
+        jax.ShapeDtypeStruct((PARTS * window_rows, model_width // PARTS), bf16),
+        partial,
+        rest,
+        down_next,
+        down_far,
+        kinds="vvhh",
+        scratch=(
+            pltpu.VMEM((2, pieces, hidden_part, DOWN_LANES), bf16),
+            pltpu.SemaphoreType.DMA((2, pieces)),
+        ),
+    )
     returned = spread(expert_out.reshape(sp_size, PARTS * capacity, -1), SP)
     return call(
-        lambda *refs: combine_kernel(capacity, *refs),
+        combine_kernel,
         jax.ShapeDtypeStruct((quarter_rows, model_width), bf16),
         returned.reshape(expert_out.shape),
         residual,
-        own,
-        own_rows,
-        router_weight,
-        kinds="hvvvv",
+        tables,
+        kinds="hvv",
         scratch=(
             pltpu.VMEM((4, expert_out.shape[0], expert_out.shape[1] // 4), bf16),
             pltpu.SemaphoreType.DMA((4,)),

time: 256 us -> 244 us (0.953)
  waiting for transfers between devices: 134 us -> 122 us
    ppermute x8, waiting for transfers between devices: 42.4 us -> 29.7 us  [the longest x2 17 us: layer(): rows.append((received, lax.ppermute(received, CORE_TP, ROW_PAIRS)))]
    pallas_call x11 -> x13, Pallas kernels: 23.9 us -> 29.6 us  [call(): pl.pallas_call(kernel, out_shape=out_shape, in_specs=[spaces[kind] for _,...]
    pallas_call x1 -> x0, Pallas kernels: 5.3 us -> none  [project_down(): pl.pallas_call(lambda *refs: down_kernel(capacity, *refs), grid=(width //...]
    all_to_all x4, starting transfers between devices: 32.6 us -> 35.4 us  [spread(): return lax.all_to_all(value, axes, split_axis=0, concat_axis=0, tiled=True)]
  transfers between devices with their start and end apart: 18 -> 18, of which waited for: 10 -> 11; matrix products, arithmetic and copies ran while one was open for 0% -> 0% of each run, Pallas kernels for 7% -> 8%
where the time goes in v5:
time: 244 us; the launch traced here: 243 us
  waiting for transfers between devices  122 us (50%)
  starting transfers between devices  53.9 us (22%)
  Pallas kernels  29.6 us (12%)
  blocking collectives  25.5 us (10%)
  local copies, waits for them, and re-layouts  12.1 us (5%)
    all_to_all x4, waiting for transfers between devices, spread(): return lax.all_to_all(value, axes, split_axis=0, concat_axis=0, tiled=True)  80 us
    all_to_all x4, starting transfers between devices, spread(): return lax.all_to_all(value, axes, split_axis=0, concat_axis=0, tiled=True)  35.4 us
    pallas_call x13, Pallas kernels, call(): pl.pallas_call(kernel, out_shape=out_shape, in_specs=[spaces[kind] for _,...  29.6 us
    all_to_all x2, blocking collectives, spread(): return lax.all_to_all(value, axes, split_axis=0, concat_axis=0, tiled=True)  25.5 us
    ppermute x2, waiting for transfers between devices, layer(): rows.append((received, lax.ppermute(received, CORE_TP, ROW_PAIRS)))  17 us
    ppermute x6, waiting for transfers between devices, shifted(): return lax.ppermute(value, TP, [(i, (i + k) % count) for i in range(count)])  12.1 us
    unnamed x45, local copies, waits for them, and re-layouts  11.8 us
    ppermute x1, waiting for transfers between devices, layer(): down_far = lax.ppermute(down_near, CORE_TP, ROW_PAIRS)  11.5 us
  transfers between devices with their start and end apart: 18, of which 11 were waited for; matrix products, arithmetic and copies ran while one was open for 0% of the time, Pallas kernels for 8%

profile of v5, /device:TPU:1, one launch (start us, length us, event | category | flops | bytes accessed | tf_op | source)
XLA Modules:
  0.0 243.1 jit_solution(15016476840049007117)
XLA Ops:
  0.0 3.4 %collective-permute-start = (bf16[256,3072]{1,0:T(8,128)(2,1)}, bf16[256,3072]{1,0:T(8,128)(2,1)}, u32[]{:S(2)}, u32[]{:S(2)}) collective-permute-start(bf16[256,3072]{1,0:T(8,128)(2,1)} %bitcast.19), channel_id=1, source_target_pairs={{0,1},{1,0},{2,3},{3,2},{5,6},{6,5},{7,4},{4,7},{8,9},{9,8},{10,11... | collective-permute-start | bytes 4718600 | tf_op jit(solution)/shard_map/ppermute | solution.py:453
  3.4 0.9 copy-done.8
  4.3 0.9 copy-done.10
  5.3 0.7 copy-done.15
  6.0 0.7 copy-done.18
  6.6 1.4 shard_map.146
  8.1 9.6 %all_to_all.30.refs_0_ = bf16[8,64,128]{2,1,0:T(8,128)(2,1)S(1)} all-to-all(bf16[8,64,128]{2,1,0:T(8,128)(2,1)S(1)} %shard_map.146), channel_id=1, replica_groups=mesh['sp_0'=8,'sp_1'=4,'sp_2'=2,'tp_0'=2,'tp_1'=2] {'sp_1','sp_2'}, dimensions={0} | all-to-all | bytes 262144 | tf_op jit(solution)/shard_map/all_to_all | solution.py:411
  17.7 15.8 %all_to_all.31.refs_1_ = bf16[8,64,128]{2,1,0:T(8,128)(2,1)S(1)} all-to-all(bf16[8,64,128]{2,1,0:T(8,128)(2,1)S(1)} %get-tuple-element.34), channel_id=1, replica_groups=mesh['sp_0'=8,'sp_1'=4,'sp_2'=2,'tp_0'=2,'tp_1'=2] {'sp_0'}, dimensions={0} | all-to-all | bytes 262144 | tf_op jit(solution)/shard_map/all_to_all | solution.py:411
  33.6 0.7 shard_map.148
  34.3 6.2 %all-to-all-start.2 = ((bf16[8,48,128]{2,1,0:T(8,128)(2,1)}), bf16[8,48,128]{2,1,0:T(8,128)(2,1)}, u32[]{:S(2)}, u32[]{:S(2)}) async-start(bf16[8,48,128]{2,1,0:T(8,128)(2,1)} %shard_map.148), calls=%async_computation.2 | async-start | bytes 196608 | tf_op jit(solution)/shard_map/all_to_all | solution.py:411
  40.5 0.9 copy-done.9
  41.5 0.9 copy-done.11
  42.4 0.9 copy-done.13
  43.3 0.9 copy-done.14
  44.2 3.0 %shard_map.145.local_ref = f32[3,256,384]{2,1,0:T(8,128)S(1)} custom-call(bf16[256,384]{1,0:T(8,128)(2,1)S(1)} %copy-done.13, bf16[256,384]{1,0:T(8,128)(2,1)S(1)} %copy-done.9, bf16[256,384]{1,0:T(8,128)(2,1)S(1)} %copy-done.11, bf16[256,384]{1,0:T(8,128)(2,1)S(1)} %copy-done.14, f32[384]{0:T(512)S(1)} %copy-done.19, f32[3,256]{1,0:T(4,128)S(1)} %copy-done.16, ...), custom_call_target="tpu_custom_call" | custom-call | tf_op jit(solution)/shard_map/pallas_call | solution.py:59
  47.2 1.9 shard_map.149.refs_0_
  49.2 2.6 %collective-permute-start.2 = (bf16[256,384]{1,0:T(8,128)(2,1)}, bf16[256,384]{1,0:T(8,128)(2,1)S(1)}, u32[]{:S(2)}, u32[]{:S(2)}) collective-permute-start(bf16[256,384]{1,0:T(8,128)(2,1)} %shard_map.149.refs_0_), channel_id=1, source_target_pairs={{0,2},{1,3},{2,0},{3,1},{4,6},{5,7},{6,4},{7,5},{8,10},{9,11},{10,... | collective-permute-start | bytes 589832 | tf_op jit(solution)/shard_map/ppermute | solution.py:416
  51.7 1.5 collective-permute-start.3
  53.4 3.6 %collective-permute-done.1.refs_1_ = bf16[256,384]{1,0:T(8,128)(2,1)S(1)} collective-permute-done((bf16[256,384]{1,0:T(8,128)(2,1)}, bf16[256,384]{1,0:T(8,128)(2,1)S(1)}, u32[]{:S(2)}, u32[]{:S(2)}) %collective-permute-start.1) | collective-permute-done | bytes 196640 | tf_op jit(solution)/shard_map/ppermute | solution.py:416
  57.0 4.0 %collective-permute-done.2.refs_2_ = bf16[256,384]{1,0:T(8,128)(2,1)S(1)} collective-permute-done((bf16[256,384]{1,0:T(8,128)(2,1)}, bf16[256,384]{1,0:T(8,128)(2,1)S(1)}, u32[]{:S(2)}, u32[]{:S(2)}) %collective-permute-start.2) | collective-permute-done | bytes 196640 | tf_op jit(solution)/shard_map/ppermute | solution.py:416
  61.5 1.9 shard_map.150
  63.4 2.2 collective-permute-start.4
  65.6 2.2 collective-permute-start.5
  68.6 3.7 %collective-permute-done.5.refs_3_ = bf16[64,768]{1,0:T(8,128)(2,1)S(1)} collective-permute-done((bf16[64,768]{1,0:T(8,128)(2,1)S(1)}, bf16[64,768]{1,0:T(8,128)(2,1)S(1)}, u32[]{:S(2)}, u32[]{:S(2)}) %collective-permute-start.5) | collective-permute-done | bytes 98336 | tf_op jit(solution)/shard_map/ppermute | solution.py:416
  72.3 2.0 shard_map.151
  74.4 1.1 copy-done.5
  75.4 0.9 copy-done.6
  76.3 6.3 %all-to-all-start.4 = ((bf16[64,8,1152]{2,1,0:T(8,128)(2,1)}), bf16[64,8,1152]{2,1,0:T(8,128)(2,1)S(1)}, u32[]{:S(2)}, u32[]{:S(2)}) async-start(bf16[64,8,1152]{2,1,0:T(8,128)(2,1)} %bitcast.26), calls=%async_computation.4 | async-start | bytes 2359296 | tf_op jit(solution)/shard_map/all_to_all | solution.py:411
  82.7 1.2 collective-permute-start.8
  84.4 1.9 collective-permute-start.10
  86.4 0.7 collective-permute-start.11
  87.1 26.2 %all-to-all-done.4 = bf16[64,8,1152]{2,1,0:T(8,128)(2,1)S(1)} async-done(((bf16[64,8,1152]{2,1,0:T(8,128)(2,1)}), bf16[64,8,1152]{2,1,0:T(8,128)(2,1)S(1)}, u32[]{:S(2)}, u32[]{:S(2)}) %all-to-all-start.4) | async-done | bytes 1179680 | tf_op jit(solution)/shard_map/all_to_all | solution.py:411
  113.3 0.9 collective-permute-start.7
  114.2 7.9 %all-to-all-start.3 = ((bf16[64,8,384]{2,1,0:T(8,128)(2,1)}), bf16[64,8,384]{2,1,0:T(8,128)(2,1)S(1)}, u32[]{:S(2)}, u32[]{:S(2)}) async-start(bf16[64,8,384]{2,1,0:T(8,128)(2,1)} %bitcast.7), calls=%async_computation.3 | async-start | bytes 786432 | tf_op jit(solution)/shard_map/all_to_all | solution.py:411
  122.1 15.2 %all-to-all-done.3 = bf16[64,8,384]{2,1,0:T(8,128)(2,1)S(1)} async-done(((bf16[64,8,384]{2,1,0:T(8,128)(2,1)}), bf16[64,8,384]{2,1,0:T(8,128)(2,1)S(1)}, u32[]{:S(2)}, u32[]{:S(2)}) %all-to-all-start.3) | async-done | bytes 393248 | tf_op jit(solution)/shard_map/all_to_all | solution.py:411
  137.3 11.5 %collective-permute-done.9.refs_3_ = bf16[256,3072]{1,0:T(8,128)(2,1)} collective-permute-done((bf16[256,3072]{1,0:T(8,128)(2,1)}, bf16[256,3072]{1,0:T(8,128)(2,1)}, u32[]{:S(2)}, u32[]{:S(2)}) %collective-permute-start.9) | collective-permute-done | bytes 1572896 | tf_op jit(solution)/shard_map/ppermute | solution.py:527
  148.8 17.0 %collective-permute-done.7.refs_1_ = bf16[512,1152]{1,0:T(8,128)(2,1)} collective-permute-done((bf16[512,1152]{1,0:T(8,128)(2,1)S(1)}, bf16[512,1152]{1,0:T(8,128)(2,1)}, u32[]{:S(2)}, u32[]{:S(2)}) %collective-permute-start.7) | collective-permute-done | bytes 1179680 | tf_op jit(solution)/shard_map/ppermute | solution.py:552
  165.8 1.4 copy-done.3
  167.2 1.4 copy-done.4
  168.6 6.3 %shard_map.152 = (f32[2,4,256,256]{3,2,1,0:T(8,128)S(1)}, bf16[4,768,256]{2,1,0:T(8,128)(2,1)S(1)}) custom-call(bf16[512,1152]{1,0:T(8,128)(2,1)S(1)} %bitcast.16, bf16[512,1152]{1,0:T(8,128)(2,1)} %collective-permute-done.7.refs_1_, bf16[3072,256]{1,0:T(8,128)(2,1)S(1)} %bitcast.23, bf16[3072,256]{1,0:T(8,128)(2,1)S(1)} %bitcast.25, ...), custom_call_target="tpu_custom_call" | custom-call | tf_op jit(solution)/shard_map/pallas_call | solution.py:59
  175.0 0.9 shard_map.154
  175.8 1.0 collective-permute-start.13
  176.8 3.2 %shard_map.153.refs_0_ = f32[256,3072]{1,0:T(8,128)S(1)} custom-call(bf16[512,384]{1,0:T(8,128)(2,1)S(1)} %bitcast.18, bf16[4,768,256]{2,1,0:T(8,128)(2,1)S(1)} %get-tuple-element.52.refs_1_, f32[2,4,256,256]{3,2,1,0:T(8,128)S(1)} %get-tuple-element.53.refs_2_, bf16[256,3072]{1,0:T(8,128)(2,1)S(1)} %bitcast.21, bf16[256,3072]{1,0:T(8,128)(2,1)} %collective-permute-done.refs_4_), custom_call_target="tpu_custom_call" | custom-call | tf_op jit(solution)/shard_map/pallas_call | solution.py:59
  180.0 1.1 collective-permute-done.13.refs_1_
  181.1 5.7 %shard_map.155 = bf16[512,1536]{1,0:T(8,128)(2,1)} custom-call(f32[256,3072]{1,0:T(8,128)S(1)} %shard_map.153.refs_0_, bf16[256,512]{1,0:T(8,128)(2,1)S(1)} %collective-permute-done.13.refs_1_, bf16[256,3072]{1,0:T(8,128)(2,1)} %collective-permute-done.8.refs_2_, bf16[256,3072]{1,0:T(8,128)(2,1)} %collective-permute-done.9.refs_3_), custom_call_target="tpu_custom_call" | custom-call | tf_op jit(solution)/shard_map/pallas_call | solution.py:59
  186.9 14.9 %all-to-all-start.5 = ((bf16[64,8,1536]{2,1,0:T(8,128)(2,1)}), bf16[64,8,1536]{2,1,0:T(8,128)(2,1)S(1)}, u32[]{:S(2)}, u32[]{:S(2)}) async-start(bf16[64,8,1536]{2,1,0:T(8,128)(2,1)} %bitcast.11), calls=%async_computation.5 | async-start | bytes 3145728 | tf_op jit(solution)/shard_map/all_to_all | solution.py:411
  202.2 38.6 %all-to-all-done.5 = bf16[64,8,1536]{2,1,0:T(8,128)(2,1)S(1)} async-done(((bf16[64,8,1536]{2,1,0:T(8,128)(2,1)}), bf16[64,8,1536]{2,1,0:T(8,128)(2,1)S(1)}, u32[]{:S(2)}, u32[]{:S(2)}) %all-to-all-start.5) | async-done | bytes 1572896 | tf_op jit(solution)/shard_map/all_to_all | solution.py:411
  240.8 2.2 shard_map.157
  (51 shorter events, 2.5 us)
Async XLA Ops:
  0.0 53.3 %copy-start = (s32[256,2]{0,1:T(2,128)S(1)}, s32[256,2]{0,1:T(2,128)}, u32[]{:S(2)}) copy-start(s32[256,2]{0,1:T(2,128)} %param.25) | copy-start | bytes 6148
  0.0 40.5 %copy-start.19 = (f32[384]{0:T(512)S(1)}, f32[384]{0:T(512)}, u32[]{:S(2)}) copy-start(f32[384]{0:T(512)} %floor_ref.3) | copy-start | bytes 4612
  0.0 40.5 %copy-start.16 = (f32[3,256]{1,0:T(4,128)S(1)}, f32[3,256]{1,0:T(4,128)}, u32[]{:S(2)}) copy-start(f32[3,256]{1,0:T(4,128)} %extra_ref.3) | copy-start | bytes 9220
  0.0 40.5 %copy-start.20 = (f32[384]{0:T(512)S(1)}, f32[384]{0:T(512)}, u32[]{:S(2)}) copy-start(f32[384]{0:T(512)} %gain_ref.1) | copy-start | bytes 4612
  0.0 63.4 %collective-permute-start = (bf16[256,3072]{1,0:T(8,128)(2,1)}, bf16[256,3072]{1,0:T(8,128)(2,1)}, u32[]{:S(2)}, u32[]{:S(2)}) collective-permute-start(bf16[256,3072]{1,0:T(8,128)(2,1)} %bitcast.19), channel_id=1, source_target_pairs={{0,1},{1,0},{2,3},{3,2},{5,6},{6,5},{7,4},{4,7},{8,9},{9,8},{10,11... | collective-permute-start | bytes 4718600 | tf_op jit(solution)/shard_map/ppermute | solution.py:453
  3.4 0.9 copy-start.8
  4.3 0.9 copy-start.10
  5.3 0.7 copy-start.15
  6.0 0.7 copy-start.18
  34.3 12.9 %all-to-all-start.2 = ((bf16[8,48,128]{2,1,0:T(8,128)(2,1)}), bf16[8,48,128]{2,1,0:T(8,128)(2,1)}, u32[]{:S(2)}, u32[]{:S(2)}) async-start(bf16[8,48,128]{2,1,0:T(8,128)(2,1)} %shard_map.148), calls=%async_computation.2 | async-start | bytes 196608 | tf_op jit(solution)/shard_map/all_to_all | solution.py:411
  40.5 0.9 copy-start.9
  41.5 0.9 copy-start.11
  42.4 0.9 copy-start.13
  43.3 0.9 copy-start.14
  44.2 17.2 %copy-start.1 = (bf16[1536,768]{1,0:T(8,128)(2,1)S(1)}, bf16[1536,768]{1,0:T(8,128)(2,1)}, u32[]{:S(2)}) copy-start(bf16[1536,768]{1,0:T(8,128)(2,1)} %refs_4_.1) | copy-start | bytes 7077892
  49.2 7.8 %collective-permute-start.1 = (bf16[256,384]{1,0:T(8,128)(2,1)}, bf16[256,384]{1,0:T(8,128)(2,1)S(1)}, u32[]{:S(2)}, u32[]{:S(2)}) collective-permute-start(bf16[256,384]{1,0:T(8,128)(2,1)} %shard_map.149.refs_0_), channel_id=1, source_target_pairs={{0,1},{1,2},{2,3},{3,0},{4,5},{5,6},{6,7},{7,4},{8,9},{9,10},{10,1... | collective-permute-start | bytes 589832 | tf_op jit(solution)/shard_map/ppermute | solution.py:416
  49.2 11.9 %collective-permute-start.2 = (bf16[256,384]{1,0:T(8,128)(2,1)}, bf16[256,384]{1,0:T(8,128)(2,1)S(1)}, u32[]{:S(2)}, u32[]{:S(2)}) collective-permute-start(bf16[256,384]{1,0:T(8,128)(2,1)} %shard_map.149.refs_0_), channel_id=1, source_target_pairs={{0,2},{1,3},{2,0},{3,1},{4,6},{5,7},{6,4},{7,5},{8,10},{9,11},{10,... | collective-permute-start | bytes 589832 | tf_op jit(solution)/shard_map/ppermute | solution.py:416
  51.7 9.7 %collective-permute-start.3 = (bf16[256,384]{1,0:T(8,128)(2,1)}, bf16[256,384]{1,0:T(8,128)(2,1)S(1)}, u32[]{:S(2)}, u32[]{:S(2)}) collective-permute-start(bf16[256,384]{1,0:T(8,128)(2,1)} %shard_map.149.refs_0_), channel_id=1, source_target_pairs={{0,3},{1,0},{2,1},{3,2},{4,7},{5,4},{6,5},{7,6},{8,11},{9,8},{10,9... | collective-permute-start | bytes 589832 | tf_op jit(solution)/shard_map/ppermute | solution.py:416
  53.4 18.9 %copy-start.12 = (bf16[64,3072]{1,0:T(8,128)(2,1)S(1)}, bf16[64,3072]{1,0:T(8,128)(2,1)}, u32[]{:S(2)}) copy-start(bf16[64,3072]{1,0:T(8,128)(2,1)} %refs_5_.1) | copy-start | bytes 1179652
  53.4 18.9 %copy-start.17 = (f32[3072]{0:T(1024)S(1)}, f32[3072]{0:T(1024)}, u32[]{:S(2)}) copy-start(f32[3072]{0:T(1024)} %param.24) | copy-start | bytes 36868
  63.4 5.2 %collective-permute-start.4 = (bf16[64,768]{1,0:T(8,128)(2,1)S(1)}, bf16[64,768]{1,0:T(8,128)(2,1)S(1)}, u32[]{:S(2)}, u32[]{:S(2)}) collective-permute-start(bf16[64,768]{1,0:T(8,128)(2,1)S(1)} %get-tuple-element.42), channel_id=1, source_target_pairs={{0,1},{1,2},{2,3},{3,0},{4,5},{5,6},{6,7},{7,4},{8,9},{9,10},{10,1... | collective-permute-start | bytes 294920 | tf_op jit(solution)/shard_map/ppermute | solution.py:416
  65.6 6.7 %collective-permute-start.5 = (bf16[64,768]{1,0:T(8,128)(2,1)S(1)}, bf16[64,768]{1,0:T(8,128)(2,1)S(1)}, u32[]{:S(2)}, u32[]{:S(2)}) collective-permute-start(bf16[64,768]{1,0:T(8,128)(2,1)S(1)} %get-tuple-element.43), channel_id=1, source_target_pairs={{0,2},{1,3},{2,0},{3,1},{4,6},{5,7},{6,4},{7,5},{8,10},{9,11},{10,... | collective-permute-start | bytes 294920 | tf_op jit(solution)/shard_map/ppermute | solution.py:416
  67.8 4.5 %collective-permute-start.6 = (bf16[64,768]{1,0:T(8,128)(2,1)S(1)}, bf16[64,768]{1,0:T(8,128)(2,1)S(1)}, u32[]{:S(2)}, u32[]{:S(2)}) collective-permute-start(bf16[64,768]{1,0:T(8,128)(2,1)S(1)} %get-tuple-element.44), channel_id=1, source_target_pairs={{0,3},{1,0},{2,1},{3,2},{4,7},{5,4},{6,5},{7,6},{8,11},{9,8},{10,9... | collective-permute-start | bytes 294920 | tf_op jit(solution)/shard_map/ppermute | solution.py:416
  72.3 10.4 %copy-start.2 = (bf16[1,256,3072]{2,1,0:T(8,128)(2,1)S(1)}, bf16[1,256,3072]{2,1,0:T(8,128)(2,1)}, u32[]{:S(2)}) copy-start(bf16[1,256,3072]{2,1,0:T(8,128)(2,1)} %param.29) | copy-start | bytes 4718596
  74.3 1.1 copy-start.5
  75.4 0.9 copy-start.6
  76.3 37.0 %all-to-all-start.4 = ((bf16[64,8,1152]{2,1,0:T(8,128)(2,1)}), bf16[64,8,1152]{2,1,0:T(8,128)(2,1)S(1)}, u32[]{:S(2)}, u32[]{:S(2)}) async-start(bf16[64,8,1152]{2,1,0:T(8,128)(2,1)} %bitcast.26), calls=%async_computation.4 | async-start | bytes 2359296 | tf_op jit(solution)/shard_map/all_to_all | solution.py:411
  82.7 39.4 %collective-permute-start.8 = (bf16[256,3072]{1,0:T(8,128)(2,1)S(1)}, bf16[256,3072]{1,0:T(8,128)(2,1)}, u32[]{:S(2)}, u32[]{:S(2)}) collective-permute-start(bf16[256,3072]{1,0:T(8,128)(2,1)S(1)} %bitcast.20), channel_id=1, source_target_pairs={{1,2},{2,1},{3,0},{0,3},{4,5},{5,4},{6,7},{7,6},{9,10},{10,9},{11,... | collective-permute-start | bytes 4718600 | tf_op jit(solution)/shard_map/ppermute | solution.py:454
  83.8 65.0 %collective-permute-start.9 = (bf16[256,3072]{1,0:T(8,128)(2,1)}, bf16[256,3072]{1,0:T(8,128)(2,1)}, u32[]{:S(2)}, u32[]{:S(2)}) collective-permute-start(bf16[256,3072]{1,0:T(8,128)(2,1)} %collective-permute-done.refs_4_), channel_id=1, source_target_pairs={{1,2},{2,1},{3,0},{0,3},{4,5},{5,4},{6,7},{7,6},{9,10},{10,9},{11,... | collective-permute-start | bytes 4718600 | tf_op jit(solution)/shard_map/ppermute | solution.py:527
  84.4 81.4 %collective-permute-start.10 = (bf16[3072,256]{1,0:T(8,128)(2,1)}, bf16[3072,256]{1,0:T(8,128)(2,1)}, u32[]{:S(2)}, u32[]{:S(2)}) collective-permute-start(bf16[3072,256]{1,0:T(8,128)(2,1)} %bitcast.22), channel_id=1, source_target_pairs={{0,1},{1,0},{2,3},{3,2},{5,6},{6,5},{7,4},{4,7},{8,9},{9,8},{10,11... | collective-permute-start | bytes 4718600 | tf_op jit(solution)/shard_map/ppermute | solution.py:528
  86.4 79.5 %collective-permute-start.11 = (bf16[3072,256]{1,0:T(8,128)(2,1)}, bf16[3072,256]{1,0:T(8,128)(2,1)}, u32[]{:S(2)}, u32[]{:S(2)}) collective-permute-start(bf16[3072,256]{1,0:T(8,128)(2,1)} %bitcast.24), channel_id=1, source_target_pairs={{0,1},{1,0},{2,3},{3,2},{5,6},{6,5},{7,4},{4,7},{8,9},{9,8},{10,11... | collective-permute-start | bytes 4718600 | tf_op jit(solution)/shard_map/ppermute | solution.py:529
  113.3 52.5 %collective-permute-start.7 = (bf16[512,1152]{1,0:T(8,128)(2,1)S(1)}, bf16[512,1152]{1,0:T(8,128)(2,1)}, u32[]{:S(2)}, u32[]{:S(2)}) collective-permute-start(bf16[512,1152]{1,0:T(8,128)(2,1)S(1)} %bitcast.15), channel_id=1, source_target_pairs={{1,2},{2,1},{3,0},{0,3},{4,5},{5,4},{6,7},{7,6},{9,10},{10,9},{11,... | collective-permute-start | bytes 3538952 | tf_op jit(solution)/shard_map/ppermute | solution.py:552
  114.2 23.1 %all-to-all-start.3 = ((bf16[64,8,384]{2,1,0:T(8,128)(2,1)}), bf16[64,8,384]{2,1,0:T(8,128)(2,1)S(1)}, u32[]{:S(2)}, u32[]{:S(2)}) async-start(bf16[64,8,384]{2,1,0:T(8,128)(2,1)} %bitcast.7), calls=%async_computation.3 | async-start | bytes 786432 | tf_op jit(solution)/shard_map/all_to_all | solution.py:411
  137.3 37.7 %collective-permute-start.12 = (bf16[512,384]{1,0:T(8,128)(2,1)S(1)}, bf16[512,384]{1,0:T(8,128)(2,1)S(1)}, u32[]{:S(2)}, u32[]{:S(2)}) collective-permute-start(bf16[512,384]{1,0:T(8,128)(2,1)S(1)} %bitcast.17), channel_id=1, source_target_pairs={{1,2},{2,1},{3,0},{0,3},{4,5},{5,4},{6,7},{7,6},{9,10},{10,9},{11,... | collective-permute-start | bytes 1179656 | tf_op jit(solution)/shard_map/ppermute | solution.py:552
  165.8 1.4 copy-start.3
  167.2 1.4 copy-start.4
  175.8 5.3 %collective-permute-start.13 = (bf16[256,512]{1,0:T(8,128)(2,1)S(1)}, bf16[256,512]{1,0:T(8,128)(2,1)S(1)}, u32[]{:S(2)}, u32[]{:S(2)}) collective-permute-start(bf16[256,512]{1,0:T(8,128)(2,1)S(1)} %shard_map.154), channel_id=1, source_target_pairs={{1,2},{2,1},{3,0},{0,3},{4,5},{5,4},{6,7},{7,6},{9,10},{10,9},{11,... | collective-permute-start | bytes 786440 | tf_op jit(solution)/shard_map/ppermute | solution.py:573
  186.8 14.9 %copy-start.21 = (f32[64,2]{0,1:T(2,128)S(1)}, f32[64,2]{0,1:T(2,128)}, u32[]{:S(2)}) copy-start(f32[64,2]{0,1:T(2,128)} %param.26) | copy-start | bytes 1540
  186.9 54.0 %copy-start.7 = (f32[64,3072]{1,0:T(8,128)S(1)}, f32[64,3072]{1,0:T(8,128)}, u32[]{:S(2)}) copy-start(f32[64,3072]{1,0:T(8,128)} %copy-done.6) | copy-start | bytes 2359300
  186.9 53.9 %all-to-all-start.5 = ((bf16[64,8,1536]{2,1,0:T(8,128)(2,1)}), bf16[64,8,1536]{2,1,0:T(8,128)(2,1)S(1)}, u32[]{:S(2)}, u32[]{:S(2)}) async-start(bf16[64,8,1536]{2,1,0:T(8,128)(2,1)} %bitcast.11), calls=%async_computation.5 | async-start | bytes 3145728 | tf_op jit(solution)/shard_map/all_to_all | solution.py:411

commit v6 on v5

--- a/solution.py
+++ b/solution.py
@@ -27,7 +27,7 @@
 
 WEIGHT_PAIRS = by_core(EVEN_LINKS, ODD_LINKS)
 ROW_PAIRS = by_core(ODD_LINKS, EVEN_LINKS)
-FIRST_SHARE = (3, 4)
+FIRST_SHARE = (5, 6)
 
 
 f32 = jnp.float32
@@ -343,32 +343,30 @@
     out_ref[...] = dot(inner_ref[:, :width], down_ref[...]) + dot(inner_ref[:, width:], near_ref[...])
 
 
-def down_kernel(capacity, partial_ref, rest_ref, next_ref, far_ref, out_ref, held_ref, arrived):
+def down_kernel(capacity, partial_ref, rest_ref, next_ref, far_ref, out_ref):
     rows, depth = rest_ref.shape
-    _, pieces, _, block = held_ref.shape
-    each = pieces // PARTS
-    order = [q * each + k for k in range(each) for q in range(PARTS)]
-    copies = {
-        (i, n): pltpu.make_async_copy(
-            ref.at[:, n * block : (n + 1) * block], held_ref.at[i, n], arrived.at[i, n]
-        )
-        for n in order
-        for i, ref in enumerate((next_ref, far_ref))
-    }
-    for copy in copies.values():
-        copy.start()
-    tables = [spread_table(PARTS * rows, rows, capacity, q) for q in range(PARTS)]
-    rest = [rest_ref[:, : depth // 2], rest_ref[:, depth // 2 :]]
-    for k in range(each):
-        out = jnp.zeros((PARTS * rows, block), f32)
-        for q in range(PARTS):
-            n = q * each + k
-            product = partial_ref[:, n * block : (n + 1) * block]
-            for i in range(2):
-                copies[i, n].wait()
-                product = product + dot(rest[i], held_ref[i, n])
-            out = out + dot(tables[q], product.astype(bf16))
-        out_ref[:, k * block : (k + 1) * block] = out.astype(bf16)
+    block = out_ref.shape[1]
+    part = next_ref.shape[1] // PARTS
+    out = jnp.zeros(out_ref.shape, f32)
+    for q in range(PARTS):
+        lanes = pl.ds(pl.multiple_of(q * part + pl.program_id(0) * block, LANES), block)
+        product = partial_ref[:, lanes] + dot(rest_ref[:, : depth // 2], next_ref[:, lanes])
+        product = product + dot(rest_ref[:, depth // 2 :], far_ref[:, lanes])
+        out = out + dot(spread_table(PARTS * rows, rows, capacity, q), product.astype(bf16))
+    out_ref[...] = out.astype(bf16)
+
+
+def project_down(capacity, partial, rest, weights):
+    rows, width = partial.shape
+    whole = pl.BlockSpec(memory_space=pltpu.VMEM)
+    return pl.pallas_call(
+        lambda *refs: down_kernel(capacity, *refs),
+        grid=(width // PARTS // DOWN_LANES,),
+        out_shape=jax.ShapeDtypeStruct((PARTS * rows, width // PARTS), bf16),
+        in_specs=[whole, whole] + [whole for _ in weights],
+        out_specs=pl.BlockSpec((PARTS * rows, DOWN_LANES), lambda k: (0, k)),
+        compiler_params=pltpu.CompilerParams(vmem_limit_bytes=12 * 1024 * 1024),
+    )(partial, rest, *weights)
 
 
 def tables_kernel(capacity, column_ref, row_ref, weight_ref, out_ref):
@@ -581,20 +579,7 @@
         down_near,
         scratch=(pltpu.VMEM((window_rows, 2 * hidden_part), bf16),),
     )
-    pieces = model_width // DOWN_LANES
-    expert_out = call(
-        lambda *refs: down_kernel(capacity, *refs),
-        jax.ShapeDtypeStruct((PARTS * window_rows, model_width // PARTS), bf16),
-        partial,
-        rest,
-        down_next,
-        down_far,
-        kinds="vvhh",
-        scratch=(
-            pltpu.VMEM((2, pieces, hidden_part, DOWN_LANES), bf16),
-            pltpu.SemaphoreType.DMA((2, pieces)),
-        ),
-    )
+    expert_out = project_down(capacity, partial, rest, (down_next, down_far))
     returned = spread(expert_out.reshape(sp_size, PARTS * capacity, -1), SP)
     return call(
         combine_kernel,

time: 244 us -> 245 us (level)
    pallas_call x13 -> x12, Pallas kernels: 29.6 us -> 23.8 us  [call(): pl.pallas_call(kernel, out_shape=out_shape, in_specs=[spaces[kind] for _,...]
    pallas_call x0 -> x1, Pallas kernels: none -> 5.3 us  [project_down(): pl.pallas_call(lambda *refs: down_kernel(capacity, *refs), grid=(width //...]
where the time goes in v6:
time: 245 us; the launch traced here: 244 us
  waiting for transfers between devices  124 us (51%)
  starting transfers between devices  53.6 us (22%)
  Pallas kernels  29.1 us (12%)
  blocking collectives  25.5 us (10%)
  local copies, waits for them, and re-layouts  12.1 us (5%)
    all_to_all x4, waiting for transfers between devices, spread(): return lax.all_to_all(value, axes, split_axis=0, concat_axis=0, tiled=True)  80.9 us
    all_to_all x4, starting transfers between devices, spread(): return lax.all_to_all(value, axes, split_axis=0, concat_axis=0, tiled=True)  35.1 us
    all_to_all x2, blocking collectives, spread(): return lax.all_to_all(value, axes, split_axis=0, concat_axis=0, tiled=True)  25.5 us
    pallas_call x12, Pallas kernels, call(): pl.pallas_call(kernel, out_shape=out_shape, in_specs=[spaces[kind] for _,...  23.8 us
    ppermute x2, waiting for transfers between devices, layer(): rows.append((received, lax.ppermute(received, CORE_TP, ROW_PAIRS)))  18.4 us
    ppermute x6, waiting for transfers between devices, shifted(): return lax.ppermute(value, TP, [(i, (i + k) % count) for i in range(count)])  12.1 us
    unnamed x45, local copies, waits for them, and re-layouts  11.9 us
    ppermute x1, waiting for transfers between devices, layer(): down_far = lax.ppermute(down_near, CORE_TP, ROW_PAIRS)  10.9 us
  transfers between devices with their start and end apart: 18, of which 11 were waited for; matrix products, arithmetic and copies ran while one was open for 0% of the time, Pallas kernels for 8%

profile of v6, /device:TPU:1, one launch (start us, length us, event | category | flops | bytes accessed | tf_op | source)
XLA Modules:
  0.0 244.2 jit_solution(17126221283774996304)
XLA Ops:
  0.0 3.4 %collective-permute-start = (bf16[256,3072]{1,0:T(8,128)(2,1)}, bf16[256,3072]{1,0:T(8,128)(2,1)}, u32[]{:S(2)}, u32[]{:S(2)}) collective-permute-start(bf16[256,3072]{1,0:T(8,128)(2,1)} %bitcast.17), channel_id=1, source_target_pairs={{0,1},{1,0},{2,3},{3,2},{5,6},{6,5},{7,4},{4,7},{8,9},{9,8},{10,11... | collective-permute-start | bytes 4718600 | tf_op jit(solution)/shard_map/ppermute | solution.py:451
  3.4 0.9 copy-done.8
  4.3 0.9 copy-done.10
  5.3 0.7 copy-done.15
  6.0 0.7 copy-done.18
  6.6 1.4 shard_map.146
  8.1 9.6 %all_to_all.30.refs_0_ = bf16[8,64,128]{2,1,0:T(8,128)(2,1)S(1)} all-to-all(bf16[8,64,128]{2,1,0:T(8,128)(2,1)S(1)} %shard_map.146), channel_id=1, replica_groups=mesh['sp_0'=8,'sp_1'=4,'sp_2'=2,'tp_0'=2,'tp_1'=2] {'sp_1','sp_2'}, dimensions={0} | all-to-all | bytes 262144 | tf_op jit(solution)/shard_map/all_to_all | solution.py:409
  17.7 15.8 %all_to_all.31.refs_1_ = bf16[8,64,128]{2,1,0:T(8,128)(2,1)S(1)} all-to-all(bf16[8,64,128]{2,1,0:T(8,128)(2,1)S(1)} %get-tuple-element.34), channel_id=1, replica_groups=mesh['sp_0'=8,'sp_1'=4,'sp_2'=2,'tp_0'=2,'tp_1'=2] {'sp_0'}, dimensions={0} | all-to-all | bytes 262144 | tf_op jit(solution)/shard_map/all_to_all | solution.py:409
  33.6 0.7 shard_map.148
  34.3 6.2 %all-to-all-start.2 = ((bf16[8,48,128]{2,1,0:T(8,128)(2,1)}), bf16[8,48,128]{2,1,0:T(8,128)(2,1)}, u32[]{:S(2)}, u32[]{:S(2)}) async-start(bf16[8,48,128]{2,1,0:T(8,128)(2,1)} %shard_map.148), calls=%async_computation.2 | async-start | bytes 196608 | tf_op jit(solution)/shard_map/all_to_all | solution.py:409
  40.5 0.9 copy-done.9
  41.5 0.9 copy-done.11
  42.4 0.9 copy-done.13
  43.3 0.9 copy-done.14
  44.2 3.0 %shard_map.145.local_ref = f32[3,256,384]{2,1,0:T(8,128)S(1)} custom-call(bf16[256,384]{1,0:T(8,128)(2,1)S(1)} %copy-done.13, bf16[256,384]{1,0:T(8,128)(2,1)S(1)} %copy-done.9, bf16[256,384]{1,0:T(8,128)(2,1)S(1)} %copy-done.11, bf16[256,384]{1,0:T(8,128)(2,1)S(1)} %copy-done.14, f32[384]{0:T(512)S(1)} %copy-done.19, f32[3,256]{1,0:T(4,128)S(1)} %copy-done.16, ...), custom_call_target="tpu_custom_call" | custom-call | tf_op jit(solution)/shard_map/pallas_call | solution.py:59
  47.2 1.9 shard_map.149.refs_0_
  49.2 2.6 %collective-permute-start.2 = (bf16[256,384]{1,0:T(8,128)(2,1)}, bf16[256,384]{1,0:T(8,128)(2,1)S(1)}, u32[]{:S(2)}, u32[]{:S(2)}) collective-permute-start(bf16[256,384]{1,0:T(8,128)(2,1)} %shard_map.149.refs_0_), channel_id=1, source_target_pairs={{0,2},{1,3},{2,0},{3,1},{4,6},{5,7},{6,4},{7,5},{8,10},{9,11},{10,... | collective-permute-start | bytes 589832 | tf_op jit(solution)/shard_map/ppermute | solution.py:414
  51.7 1.5 collective-permute-start.3
  53.4 3.6 %collective-permute-done.1.refs_1_ = bf16[256,384]{1,0:T(8,128)(2,1)S(1)} collective-permute-done((bf16[256,384]{1,0:T(8,128)(2,1)}, bf16[256,384]{1,0:T(8,128)(2,1)S(1)}, u32[]{:S(2)}, u32[]{:S(2)}) %collective-permute-start.1) | collective-permute-done | bytes 196640 | tf_op jit(solution)/shard_map/ppermute | solution.py:414
  57.0 4.0 %collective-permute-done.2.refs_2_ = bf16[256,384]{1,0:T(8,128)(2,1)S(1)} collective-permute-done((bf16[256,384]{1,0:T(8,128)(2,1)}, bf16[256,384]{1,0:T(8,128)(2,1)S(1)}, u32[]{:S(2)}, u32[]{:S(2)}) %collective-permute-start.2) | collective-permute-done | bytes 196640 | tf_op jit(solution)/shard_map/ppermute | solution.py:414
  61.5 1.9 shard_map.150
  63.4 2.2 collective-permute-start.4
  65.6 2.2 collective-permute-start.5
  68.6 3.7 %collective-permute-done.5.refs_3_ = bf16[64,768]{1,0:T(8,128)(2,1)S(1)} collective-permute-done((bf16[64,768]{1,0:T(8,128)(2,1)S(1)}, bf16[64,768]{1,0:T(8,128)(2,1)S(1)}, u32[]{:S(2)}, u32[]{:S(2)}) %collective-permute-start.5) | collective-permute-done | bytes 98336 | tf_op jit(solution)/shard_map/ppermute | solution.py:414
  72.3 2.0 shard_map.151
  74.3 1.1 copy-done.5
  75.4 0.9 copy-done.6
  76.3 6.3 %all-to-all-start.4 = ((bf16[64,8,1280]{2,1,0:T(8,128)(2,1)}), bf16[64,8,1280]{2,1,0:T(8,128)(2,1)S(1)}, u32[]{:S(2)}, u32[]{:S(2)}) async-start(bf16[64,8,1280]{2,1,0:T(8,128)(2,1)} %bitcast.24), calls=%async_computation.4 | async-start | bytes 2621440 | tf_op jit(solution)/shard_map/all_to_all | solution.py:409
  82.7 1.2 collective-permute-start.8
  84.4 1.9 collective-permute-start.10
  86.4 0.7 collective-permute-start.11
  87.1 29.2 %all-to-all-done.4 = bf16[64,8,1280]{2,1,0:T(8,128)(2,1)S(1)} async-done(((bf16[64,8,1280]{2,1,0:T(8,128)(2,1)}), bf16[64,8,1280]{2,1,0:T(8,128)(2,1)S(1)}, u32[]{:S(2)}, u32[]{:S(2)}) %all-to-all-start.4) | async-done | bytes 1310752 | tf_op jit(solution)/shard_map/all_to_all | solution.py:409
  116.3 0.9 collective-permute-start.7
  117.2 7.6 %all-to-all-start.3 = ((bf16[64,8,256]{2,1,0:T(8,128)(2,1)}), bf16[64,8,256]{2,1,0:T(8,128)(2,1)S(1)}, u32[]{:S(2)}, u32[]{:S(2)}) async-start(bf16[64,8,256]{2,1,0:T(8,128)(2,1)} %bitcast.7), calls=%async_computation.3 | async-start | bytes 524288 | tf_op jit(solution)/shard_map/all_to_all | solution.py:409
  124.9 13.1 %all-to-all-done.3 = bf16[64,8,256]{2,1,0:T(8,128)(2,1)S(1)} async-done(((bf16[64,8,256]{2,1,0:T(8,128)(2,1)}), bf16[64,8,256]{2,1,0:T(8,128)(2,1)S(1)}, u32[]{:S(2)}, u32[]{:S(2)}) %all-to-all-start.3) | async-done | bytes 262176 | tf_op jit(solution)/shard_map/all_to_all | solution.py:409
  137.9 10.9 %collective-permute-done.9.refs_3_ = bf16[256,3072]{1,0:T(8,128)(2,1)} collective-permute-done((bf16[256,3072]{1,0:T(8,128)(2,1)}, bf16[256,3072]{1,0:T(8,128)(2,1)}, u32[]{:S(2)}, u32[]{:S(2)}) %collective-permute-start.9) | collective-permute-done | bytes 1572896 | tf_op jit(solution)/shard_map/ppermute | solution.py:525
  148.8 18.4 %collective-permute-done.7.refs_1_ = bf16[512,1280]{1,0:T(8,128)(2,1)} collective-permute-done((bf16[512,1280]{1,0:T(8,128)(2,1)S(1)}, bf16[512,1280]{1,0:T(8,128)(2,1)}, u32[]{:S(2)}, u32[]{:S(2)}) %collective-permute-start.7) | collective-permute-done | bytes 1310752 | tf_op jit(solution)/shard_map/ppermute | solution.py:550
  167.2 1.4 copy-done.3
  168.6 1.4 copy-done.4
  170.1 6.6 %shard_map.152 = (f32[2,4,256,256]{3,2,1,0:T(8,128)S(1)}, bf16[4,512,256]{2,1,0:T(8,128)(2,1)S(1)}) custom-call(bf16[512,1280]{1,0:T(8,128)(2,1)S(1)} %bitcast.16, bf16[512,1280]{1,0:T(8,128)(2,1)} %collective-permute-done.7.refs_1_, bf16[3072,256]{1,0:T(8,128)(2,1)S(1)} %bitcast.21, bf16[3072,256]{1,0:T(8,128)(2,1)S(1)} %bitcast.23, ...), custom_call_target="tpu_custom_call" | custom-call | tf_op jit(solution)/shard_map/pallas_call | solution.py:59
  176.7 0.7 shard_map.154
  177.3 1.0 collective-permute-start.13
  178.3 3.0 %shard_map.153.refs_0_ = f32[256,3072]{1,0:T(8,128)S(1)} custom-call(bf16[512,256]{1,0:T(8,128)(2,1)S(1)} %bitcast.26, bf16[4,512,256]{2,1,0:T(8,128)(2,1)S(1)} %get-tuple-element.52.refs_1_, f32[2,4,256,256]{3,2,1,0:T(8,128)S(1)} %get-tuple-element.53.refs_2_, bf16[256,3072]{1,0:T(8,128)(2,1)S(1)} %bitcast.19, bf16[256,3072]{1,0:T(8,128)(2,1)} %collective-permute-done.refs_4_), custom_call_target="tpu_custom_call" | custom-call | tf_op jit(solution)/shard_map/pallas_call | solution.py:59
  181.3 1.3 collective-permute-done.13.refs_1_
  182.6 5.3 %shard_map.155 = bf16[512,1536]{1,0:T(8,128)(2,1)} custom-call(f32[256,3072]{1,0:T(8,128)S(1)} %shard_map.153.refs_0_, bf16[256,512]{1,0:T(8,128)(2,1)S(1)} %collective-permute-done.13.refs_1_, bf16[256,3072]{1,0:T(8,128)(2,1)} %collective-permute-done.8.refs_2_, bf16[256,3072]{1,0:T(8,128)(2,1)} %collective-permute-done.9.refs_3_), custom_call_target="tpu_custom_call" | custom-call | tf_op jit(solution)/shard_map/pallas_call | solution.py:362
  187.9 14.9 %all-to-all-start.5 = ((bf16[64,8,1536]{2,1,0:T(8,128)(2,1)}), bf16[64,8,1536]{2,1,0:T(8,128)(2,1)S(1)}, u32[]{:S(2)}, u32[]{:S(2)}) async-start(bf16[64,8,1536]{2,1,0:T(8,128)(2,1)} %bitcast.11), calls=%async_computation.5 | async-start | bytes 3145728 | tf_op jit(solution)/shard_map/all_to_all | solution.py:409
  203.3 38.6 %all-to-all-done.5 = bf16[64,8,1536]{2,1,0:T(8,128)(2,1)S(1)} async-done(((bf16[64,8,1536]{2,1,0:T(8,128)(2,1)}), bf16[64,8,1536]{2,1,0:T(8,128)(2,1)S(1)}, u32[]{:S(2)}, u32[]{:S(2)}) %all-to-all-start.5) | async-done | bytes 1572896 | tf_op jit(solution)/shard_map/all_to_all | solution.py:409
  241.9 2.2 shard_map.157
  (51 shorter events, 2.5 us)
Async XLA Ops:
  0.0 53.3 %copy-start = (s32[256,2]{0,1:T(2,128)S(1)}, s32[256,2]{0,1:T(2,128)}, u32[]{:S(2)}) copy-start(s32[256,2]{0,1:T(2,128)} %param.25) | copy-start | bytes 6148
  0.0 40.5 %copy-start.19 = (f32[384]{0:T(512)S(1)}, f32[384]{0:T(512)}, u32[]{:S(2)}) copy-start(f32[384]{0:T(512)} %floor_ref.3) | copy-start | bytes 4612
  0.0 40.5 %copy-start.16 = (f32[3,256]{1,0:T(4,128)S(1)}, f32[3,256]{1,0:T(4,128)}, u32[]{:S(2)}) copy-start(f32[3,256]{1,0:T(4,128)} %extra_ref.3) | copy-start | bytes 9220
  0.0 40.5 %copy-start.20 = (f32[384]{0:T(512)S(1)}, f32[384]{0:T(512)}, u32[]{:S(2)}) copy-start(f32[384]{0:T(512)} %gain_ref.1) | copy-start | bytes 4612
  0.0 63.4 %collective-permute-start = (bf16[256,3072]{1,0:T(8,128)(2,1)}, bf16[256,3072]{1,0:T(8,128)(2,1)}, u32[]{:S(2)}, u32[]{:S(2)}) collective-permute-start(bf16[256,3072]{1,0:T(8,128)(2,1)} %bitcast.17), channel_id=1, source_target_pairs={{0,1},{1,0},{2,3},{3,2},{5,6},{6,5},{7,4},{4,7},{8,9},{9,8},{10,11... | collective-permute-start | bytes 4718600 | tf_op jit(solution)/shard_map/ppermute | solution.py:451
  3.4 0.9 copy-start.8
  4.3 0.9 copy-start.10
  5.3 0.7 copy-start.15
  6.0 0.7 copy-start.18
  34.3 12.9 %all-to-all-start.2 = ((bf16[8,48,128]{2,1,0:T(8,128)(2,1)}), bf16[8,48,128]{2,1,0:T(8,128)(2,1)}, u32[]{:S(2)}, u32[]{:S(2)}) async-start(bf16[8,48,128]{2,1,0:T(8,128)(2,1)} %shard_map.148), calls=%async_computation.2 | async-start | bytes 196608 | tf_op jit(solution)/shard_map/all_to_all | solution.py:409
  40.5 0.9 copy-start.9
  41.5 0.9 copy-start.11
  42.4 0.9 copy-start.13
  43.3 0.9 copy-start.14
  44.2 17.2 %copy-start.1 = (bf16[1536,768]{1,0:T(8,128)(2,1)S(1)}, bf16[1536,768]{1,0:T(8,128)(2,1)}, u32[]{:S(2)}) copy-start(bf16[1536,768]{1,0:T(8,128)(2,1)} %refs_4_.1) | copy-start | bytes 7077892
  49.2 7.8 %collective-permute-start.1 = (bf16[256,384]{1,0:T(8,128)(2,1)}, bf16[256,384]{1,0:T(8,128)(2,1)S(1)}, u32[]{:S(2)}, u32[]{:S(2)}) collective-permute-start(bf16[256,384]{1,0:T(8,128)(2,1)} %shard_map.149.refs_0_), channel_id=1, source_target_pairs={{0,1},{1,2},{2,3},{3,0},{4,5},{5,6},{6,7},{7,4},{8,9},{9,10},{10,1... | collective-permute-start | bytes 589832 | tf_op jit(solution)/shard_map/ppermute | solution.py:414
  49.2 11.9 %collective-permute-start.2 = (bf16[256,384]{1,0:T(8,128)(2,1)}, bf16[256,384]{1,0:T(8,128)(2,1)S(1)}, u32[]{:S(2)}, u32[]{:S(2)}) collective-permute-start(bf16[256,384]{1,0:T(8,128)(2,1)} %shard_map.149.refs_0_), channel_id=1, source_target_pairs={{0,2},{1,3},{2,0},{3,1},{4,6},{5,7},{6,4},{7,5},{8,10},{9,11},{10,... | collective-permute-start | bytes 589832 | tf_op jit(solution)/shard_map/ppermute | solution.py:414
  51.7 9.7 %collective-permute-start.3 = (bf16[256,384]{1,0:T(8,128)(2,1)}, bf16[256,384]{1,0:T(8,128)(2,1)S(1)}, u32[]{:S(2)}, u32[]{:S(2)}) collective-permute-start(bf16[256,384]{1,0:T(8,128)(2,1)} %shard_map.149.refs_0_), channel_id=1, source_target_pairs={{0,3},{1,0},{2,1},{3,2},{4,7},{5,4},{6,5},{7,6},{8,11},{9,8},{10,9... | collective-permute-start | bytes 589832 | tf_op jit(solution)/shard_map/ppermute | solution.py:414
  53.4 18.9 %copy-start.12 = (bf16[64,3072]{1,0:T(8,128)(2,1)S(1)}, bf16[64,3072]{1,0:T(8,128)(2,1)}, u32[]{:S(2)}) copy-start(bf16[64,3072]{1,0:T(8,128)(2,1)} %refs_5_.1) | copy-start | bytes 1179652
  53.4 18.9 %copy-start.17 = (f32[3072]{0:T(1024)S(1)}, f32[3072]{0:T(1024)}, u32[]{:S(2)}) copy-start(f32[3072]{0:T(1024)} %param.24) | copy-start | bytes 36868
  63.4 5.2 %collective-permute-start.4 = (bf16[64,768]{1,0:T(8,128)(2,1)S(1)}, bf16[64,768]{1,0:T(8,128)(2,1)S(1)}, u32[]{:S(2)}, u32[]{:S(2)}) collective-permute-start(bf16[64,768]{1,0:T(8,128)(2,1)S(1)} %get-tuple-element.42), channel_id=1, source_target_pairs={{0,1},{1,2},{2,3},{3,0},{4,5},{5,6},{6,7},{7,4},{8,9},{9,10},{10,1... | collective-permute-start | bytes 294920 | tf_op jit(solution)/shard_map/ppermute | solution.py:414
  65.6 6.7 %collective-permute-start.5 = (bf16[64,768]{1,0:T(8,128)(2,1)S(1)}, bf16[64,768]{1,0:T(8,128)(2,1)S(1)}, u32[]{:S(2)}, u32[]{:S(2)}) collective-permute-start(bf16[64,768]{1,0:T(8,128)(2,1)S(1)} %get-tuple-element.43), channel_id=1, source_target_pairs={{0,2},{1,3},{2,0},{3,1},{4,6},{5,7},{6,4},{7,5},{8,10},{9,11},{10,... | collective-permute-start | bytes 294920 | tf_op jit(solution)/shard_map/ppermute | solution.py:414
  67.8 4.5 %collective-permute-start.6 = (bf16[64,768]{1,0:T(8,128)(2,1)S(1)}, bf16[64,768]{1,0:T(8,128)(2,1)S(1)}, u32[]{:S(2)}, u32[]{:S(2)}) collective-permute-start(bf16[64,768]{1,0:T(8,128)(2,1)S(1)} %get-tuple-element.44), channel_id=1, source_target_pairs={{0,3},{1,0},{2,1},{3,2},{4,7},{5,4},{6,5},{7,6},{8,11},{9,8},{10,9... | collective-permute-start | bytes 294920 | tf_op jit(solution)/shard_map/ppermute | solution.py:414
  72.3 10.4 %copy-start.2 = (bf16[1,256,3072]{2,1,0:T(8,128)(2,1)S(1)}, bf16[1,256,3072]{2,1,0:T(8,128)(2,1)}, u32[]{:S(2)}) copy-start(bf16[1,256,3072]{2,1,0:T(8,128)(2,1)} %param.29) | copy-start | bytes 4718596
  74.3 1.1 copy-start.5
  75.4 0.9 copy-start.6
  76.3 40.0 %all-to-all-start.4 = ((bf16[64,8,1280]{2,1,0:T(8,128)(2,1)}), bf16[64,8,1280]{2,1,0:T(8,128)(2,1)S(1)}, u32[]{:S(2)}, u32[]{:S(2)}) async-start(bf16[64,8,1280]{2,1,0:T(8,128)(2,1)} %bitcast.24), calls=%async_computation.4 | async-start | bytes 2621440 | tf_op jit(solution)/shard_map/all_to_all | solution.py:409
  82.7 42.2 %collective-permute-start.8 = (bf16[256,3072]{1,0:T(8,128)(2,1)S(1)}, bf16[256,3072]{1,0:T(8,128)(2,1)}, u32[]{:S(2)}, u32[]{:S(2)}) collective-permute-start(bf16[256,3072]{1,0:T(8,128)(2,1)S(1)} %bitcast.18), channel_id=1, source_target_pairs={{1,2},{2,1},{3,0},{0,3},{4,5},{5,4},{6,7},{7,6},{9,10},{10,9},{11,... | collective-permute-start | bytes 4718600 | tf_op jit(solution)/shard_map/ppermute | solution.py:452
  83.9 65.0 %collective-permute-start.9 = (bf16[256,3072]{1,0:T(8,128)(2,1)}, bf16[256,3072]{1,0:T(8,128)(2,1)}, u32[]{:S(2)}, u32[]{:S(2)}) collective-permute-start(bf16[256,3072]{1,0:T(8,128)(2,1)} %collective-permute-done.refs_4_), channel_id=1, source_target_pairs={{1,2},{2,1},{3,0},{0,3},{4,5},{5,4},{6,7},{7,6},{9,10},{10,9},{11,... | collective-permute-start | bytes 4718600 | tf_op jit(solution)/shard_map/ppermute | solution.py:525
  84.4 82.8 %collective-permute-start.10 = (bf16[3072,256]{1,0:T(8,128)(2,1)}, bf16[3072,256]{1,0:T(8,128)(2,1)}, u32[]{:S(2)}, u32[]{:S(2)}) collective-permute-start(bf16[3072,256]{1,0:T(8,128)(2,1)} %bitcast.20), channel_id=1, source_target_pairs={{0,1},{1,0},{2,3},{3,2},{5,6},{6,5},{7,4},{4,7},{8,9},{9,8},{10,11... | collective-permute-start | bytes 4718600 | tf_op jit(solution)/shard_map/ppermute | solution.py:526
  86.4 80.9 %collective-permute-start.11 = (bf16[3072,256]{1,0:T(8,128)(2,1)}, bf16[3072,256]{1,0:T(8,128)(2,1)}, u32[]{:S(2)}, u32[]{:S(2)}) collective-permute-start(bf16[3072,256]{1,0:T(8,128)(2,1)} %bitcast.22), channel_id=1, source_target_pairs={{0,1},{1,0},{2,3},{3,2},{5,6},{6,5},{7,4},{4,7},{8,9},{9,8},{10,11... | collective-permute-start | bytes 4718600 | tf_op jit(solution)/shard_map/ppermute | solution.py:527
  116.3 50.9 %collective-permute-start.7 = (bf16[512,1280]{1,0:T(8,128)(2,1)S(1)}, bf16[512,1280]{1,0:T(8,128)(2,1)}, u32[]{:S(2)}, u32[]{:S(2)}) collective-permute-start(bf16[512,1280]{1,0:T(8,128)(2,1)S(1)} %bitcast.15), channel_id=1, source_target_pairs={{1,2},{2,1},{3,0},{0,3},{4,5},{5,4},{6,7},{7,6},{9,10},{10,9},{11,... | collective-permute-start | bytes 3932168 | tf_op jit(solution)/shard_map/ppermute | solution.py:550
  117.2 20.7 %all-to-all-start.3 = ((bf16[64,8,256]{2,1,0:T(8,128)(2,1)}), bf16[64,8,256]{2,1,0:T(8,128)(2,1)S(1)}, u32[]{:S(2)}, u32[]{:S(2)}) async-start(bf16[64,8,256]{2,1,0:T(8,128)(2,1)} %bitcast.7), calls=%async_computation.3 | async-start | bytes 524288 | tf_op jit(solution)/shard_map/all_to_all | solution.py:409
  137.9 38.7 %collective-permute-start.12 = (bf16[512,256]{1,0:T(8,128)(2,1)S(1)}, bf16[512,256]{1,0:T(8,128)(2,1)S(1)}, u32[]{:S(2)}, u32[]{:S(2)}) collective-permute-start(bf16[512,256]{1,0:T(8,128)(2,1)S(1)} %bitcast.25), channel_id=1, source_target_pairs={{1,2},{2,1},{3,0},{0,3},{4,5},{5,4},{6,7},{7,6},{9,10},{10,9},{11,... | collective-permute-start | bytes 786440 | tf_op jit(solution)/shard_map/ppermute | solution.py:550
  167.2 1.4 copy-start.3
  168.6 1.4 copy-start.4
  177.3 5.3 %collective-permute-start.13 = (bf16[256,512]{1,0:T(8,128)(2,1)S(1)}, bf16[256,512]{1,0:T(8,128)(2,1)S(1)}, u32[]{:S(2)}, u32[]{:S(2)}) collective-permute-start(bf16[256,512]{1,0:T(8,128)(2,1)S(1)} %shard_map.154), channel_id=1, source_target_pairs={{1,2},{2,1},{3,0},{0,3},{4,5},{5,4},{6,7},{7,6},{9,10},{10,9},{11,... | collective-permute-start | bytes 786440 | tf_op jit(solution)/shard_map/ppermute | solution.py:571
  187.9 14.9 %copy-start.21 = (f32[64,2]{0,1:T(2,128)S(1)}, f32[64,2]{0,1:T(2,128)}, u32[]{:S(2)}) copy-start(f32[64,2]{0,1:T(2,128)} %param.26) | copy-start | bytes 1540
  187.9 53.9 %copy-start.7 = (f32[64,3072]{1,0:T(8,128)S(1)}, f32[64,3072]{1,0:T(8,128)}, u32[]{:S(2)}) copy-start(f32[64,3072]{1,0:T(8,128)} %copy-done.6) | copy-start | bytes 2359300
  187.9 53.9 %all-to-all-start.5 = ((bf16[64,8,1536]{2,1,0:T(8,128)(2,1)}), bf16[64,8,1536]{2,1,0:T(8,128)(2,1)S(1)}, u32[]{:S(2)}, u32[]{:S(2)}) async-start(bf16[64,8,1536]{2,1,0:T(8,128)(2,1)} %bitcast.11), calls=%async_computation.5 | async-start | bytes 3145728 | tf_op jit(solution)/shard_map/all_to_all | solution.py:409
